TPU v7x, 256 devices: a 4x2x16 block of a 4x16x16 slice. The times are simulated.
256 devices in a mesh: grp: 2 (over y), fs: 16 (over z), tp: 8 (over x, core).
Axes of the slice: x: 4, y: 2, z: 16, core: 2. Of those that a mesh axis runs over, the one named last changes fastest.
The devices are a block of a 4x16x16 slice.
Arguments:
- tokens: bfloat16 [8192, 2048], P(('grp', 'fs')), parts along dimension 0, may hold values from -6 to 6
- route_ids: int32 [8192, 2], P(('grp', 'fs')), parts along dimension 0, may hold values from 0 to 31, as said below
- route_weights: float32 [8192, 2], P(('grp', 'fs')), parts along dimension 0, may hold values from 0.2 to 1
- ffn_gain: float32 [2048], P('fs'), may hold values from 0.1 to 1.9
- gate_master: float32 [32, 2048, 1024], P(None, 'fs', 'tp'), may hold values from -0.125 to 0.125
- up_master: float32 [32, 2048, 1024], P(None, 'fs', 'tp'), may hold values from -0.125 to 0.125
- down_master: float32 [32, 1024, 2048], P(None, 'fs', 'tp'), may hold values from -0.1875 to 0.1875
Outputs:
- gate_serve: bfloat16 [64, 2048, 1024], P(('grp', 'fs'), None, 'tp'), parts along dimension 0
- up_serve: bfloat16 [64, 2048, 1024], P(('grp', 'fs'), None, 'tp'), parts along dimension 0
- down_serve: bfloat16 [64, 1024, 2048], P(('grp', 'fs'), None, 'tp'), parts along dimension 0
- mixed: bfloat16 [8192, 2048], P(('grp', 'fs'), 'tp'), parts along dimension 0
There are 2 independent parts, one for each index of `grp`. A program takes and returns all parts, laid end to end along the dimension named above; an argument that names none is the same for every part. Nothing has to cross between parts.
Inputs may be any that keep to these rules, and one draw needn't show every extreme that they name: `route_ids`: each row names two different experts of one group of 8 consecutive experts. Among the tokens of one index of fs, each group is named by exactly 64 tokens and no expert by more than 32; in every group one expert, the same for every index of fs, is named by exactly 32, and so is one other expert of the group, which may change from one index of fs to the next.
All inputs are finite; a program needn't handle non-finite values.
Results may differ from a plain program's by a relative error of at most 0.0087.
Values may be sent and summed in bfloat16 or wider, within the bound.
No kernel may reach another device: no remote copies, remote signals or barrier semaphores. Data moves between devices by JAX's collectives and lax.ppermute only.
A program may use at most 64 MiB of HBM per device.

v0:
```python
import jax
import jax.numpy as jnp
from jax import lax
from jax.sharding import Mesh
from jax.sharding import PartitionSpec as P

GROUP_SIZE = 8
TP = ("tp_0", "tp_1")


def in_one_piece(arrays, axis, split_dim, concat_dim, along):
    ends, at = ([], 0)
    for a in arrays[:-1]:
        at += a.shape[along]
        ends.append(at)
    both = jnp.concatenate(arrays, axis=along)
    return tuple(
        jnp.split(
            lax.all_to_all(both, axis, split_axis=split_dim, concat_axis=concat_dim, tiled=True),
            ends,
            axis=along,
        )
    )


def laid_out(blocks, dim):
    dims = list(blocks.shape[1:])
    dims[dim] *= blocks.shape[0]
    return jnp.moveaxis(blocks, 0, dim).reshape(dims)


def gather_in_order(x, axes, turns):
    blocks = x[None]
    for k in turns:
        blocks = lax.all_gather(blocks, axes[k], axis=0, tiled=True)
    carried = [lax.axis_size(axes[k]) for k in reversed(turns)]
    blocks = blocks.reshape(*carried, *x.shape)
    turned = sorted(range(len(turns)), key=lambda place: turns[len(turns) - 1 - place])
    return blocks.transpose(*turned, *range(len(turns), blocks.ndim)).reshape(-1, *x.shape)


def gathered_by_axis(x, axes, turns, dim):
    return laid_out(gather_in_order(x, axes, turns), dim)


def slot_targets(route_ids, experts, capacity):
    flat_ids = route_ids.reshape(-1)
    member = (flat_ids[:, None] == jnp.arange(experts, dtype=jnp.int32)[None, :]).astype(jnp.int32)
    before = jnp.cumsum(member, axis=0) - member
    slot_index = jnp.sum(before * member, axis=1)
    return flat_ids * capacity + slot_index


def fill_slots(source, targets, experts, capacity):
    doubled = jnp.repeat(source, 2, axis=0)
    buffer = jnp.zeros((experts * capacity, source.shape[1]), source.dtype).at[targets].set(doubled)
    return buffer.reshape(experts, capacity, source.shape[1])


def on_device(tokens, route_ids, route_weights, ffn_gain, gate_master, up_master, down_master):
    row_gain = ffn_gain[None, :, None]
    gate_local = (gate_master * row_gain).astype(jnp.bfloat16)
    up_local = (up_master * row_gain).astype(jnp.bfloat16)
    down_local = down_master.astype(jnp.bfloat16)
    gate_serve, up_serve, down_serve = (
        *in_one_piece((gate_local, up_local), "fs", 0, 1, 2),
        lax.all_to_all(down_local, "fs", split_axis=0, concat_axis=1, tiled=True),
    )
    experts = gate_local.shape[0]
    capacity = tokens.shape[0] // (2 * (experts // GROUP_SIZE))
    token_rows = tokens.astype(jnp.float32)
    normed = (
        token_rows * lax.rsqrt(jnp.mean(token_rows * token_rows, axis=1, keepdims=True) + 1e-06)
    ).astype(jnp.bfloat16)
    targets = slot_targets(route_ids, experts, capacity)
    col_width = normed.shape[1] // lax.axis_size(TP)
    own_cols = lax.dynamic_slice_in_dim(normed, lax.axis_index(TP) * col_width, col_width, 1)
    part_rows = lax.all_to_all(
        fill_slots(own_cols, targets, experts, capacity),
        "fs",
        split_axis=0,
        concat_axis=1,
        tiled=True,
    )
    portion = gathered_by_axis(part_rows, TP, (0, 1), 2)
    gate_part = jnp.einsum("erd,edf->erf", portion, gate_serve, preferred_element_type=jnp.float32)
    up_part = jnp.einsum("erd,edf->erf", portion, up_serve, preferred_element_type=jnp.float32)
    hidden = (jax.nn.silu(gate_part) * up_part).astype(jnp.bfloat16)
    expert_out = jnp.einsum(
        "erf,efd->erd",
        gathered_by_axis(hidden, TP, (0, 1), 2),
        down_serve,
        preferred_element_type=jnp.float32,
    ).astype(jnp.bfloat16)
    returned_rows = lax.all_to_all(expert_out, "fs", split_axis=1, concat_axis=0, tiled=True)
    picked = returned_rows.reshape(-1, returned_rows.shape[2])[targets].astype(jnp.float32)
    weighted = picked * route_weights.reshape(-1, 1)
    combined = jnp.sum(weighted.reshape(-1, 2, returned_rows.shape[2]), axis=1).astype(jnp.bfloat16)
    return (gate_serve, up_serve, down_serve, combined)


def solution(mesh):
    split = Mesh(
        mesh.devices.reshape(mesh.shape["grp"], mesh.shape["fs"], 4, 2),
        ("grp", "fs", "tp_0", "tp_1"),
    )
    in_specs = (
        P(("grp", "fs"), None),
        P(("grp", "fs"), None),
        P(("grp", "fs"), None),
        P("fs"),
        P(None, "fs", TP),
        P(None, "fs", TP),
        P(None, "fs", TP),
    )
    out_specs = (
        P(("grp", "fs"), None, TP),
        P(("grp", "fs"), None, TP),
        P(("grp", "fs"), None, TP),
        P(("grp", "fs"), TP),
    )
    return jax.shard_map(
        on_device, mesh=split, in_specs=in_specs, out_specs=out_specs, check_vma=False
    )
```

profile of v0, /device:TPU:34, one launch (start us, length us, event | category | flops | bytes accessed | tf_op | source)
XLA Modules:
  0.0 300.8 jit_solution(5720126012257750511)
XLA Ops:
  7.2 1.5 convert_element_type.43
  11.8 3.1 %scatter_custom_fusion = bf16[1024,256]{1,0:T(8,128)(2,1)} fusion(s32[512]{0:T(512)S(1)} %bitcast.77, bf16[512,256]{1,0:T(8,128)(2,1)S(1)} %reshape.126, bf16[]{:T(256)} %constant.13.clone.1), kind=kCustom, calls=%fused_computation.12 | custom fusion | bytes 524290 | tf_op jit(solution)/shard_map/scatter | solution.py:56
  14.9 24.0 %all-to-all-start.2 = ((bf16[32,32,256]{2,1,0:T(8,128)(2,1)}), bf16[32,32,256]{2,1,0:T(8,128)(2,1)S(1)}, u32[]{:S(2)}, u32[]{:S(2)}) async-start(bf16[32,32,256]{2,1,0:T(8,128)(2,1)} %bitcast.10), calls=%async_computation.2 | async-start | bytes 1048576 | tf_op jit(solution)/shard_map/all_to_all | solution.py:78
  38.9 2.2 multiply_convert_fusion.1
  41.1 1.6 pad_maximum_fusion
  42.7 25.1 %all-to-all-done.2 = bf16[32,32,256]{2,1,0:T(8,128)(2,1)S(1)} async-done(((bf16[32,32,256]{2,1,0:T(8,128)(2,1)}), bf16[32,32,256]{2,1,0:T(8,128)(2,1)S(1)}, u32[]{:S(2)}, u32[]{:S(2)}) %all-to-all-start.2) | async-done | bytes 524320 | tf_op jit(solution)/shard_map/all_to_all | solution.py:78
  68.6 6.6 %all-to-all-start = ((bf16[32,128,256]{2,1,0:T(8,128)(2,1)}), bf16[32,128,256]{2,1,0:T(8,128)(2,1)S(1)}, u32[]{:S(2)}, u32[]{:S(2)}) async-start(bf16[32,128,256]{2,1,0:T(8,128)(2,1)} %pad_maximum_fusion), calls=%async_computation | async-start | bytes 4194304 | tf_op jit(solution)/shard_map/all_to_all | solution.py:19
  75.2 1.9 copy.43
  77.2 38.8 %all-gather.6.cloned.1.call-done = bf16[4,2,512,256]{3,2,1,0:T(8,128)(2,1)} async-done(((bf16[1,2,512,256]{3,2,1,0:T(8,128)(2,1)}), bf16[4,2,512,256]{3,2,1,0:T(8,128)(2,1)}) %all-gather.6.cloned.1.call-update) | async-done | bytes 2097168 | tf_op jit(solution)/shard_map/all_gather | solution.py:35
  116.1 2.7 convert_element_type.40
  118.8 51.4 %all-to-all-done = bf16[32,128,256]{2,1,0:T(8,128)(2,1)S(1)} async-done(((bf16[32,128,256]{2,1,0:T(8,128)(2,1)}), bf16[32,128,256]{2,1,0:T(8,128)(2,1)S(1)}, u32[]{:S(2)}, u32[]{:S(2)}) %all-to-all-start) | async-done | bytes 2097184 | tf_op jit(solution)/shard_map/all_to_all | solution.py:19
  170.2 7.9 %all-to-all-start.1 = ((bf16[32,64,256]{2,1,0:T(8,128)(2,1)}), bf16[32,64,256]{2,1,0:T(8,128)(2,1)S(1)}, u32[]{:S(2)}, u32[]{:S(2)}) async-start(bf16[32,64,256]{2,1,0:T(8,128)(2,1)} %convert_element_type.40), calls=%async_computation.1 | async-start | bytes 2097152 | tf_op jit(solution)/shard_map/all_to_all | solution.py:67
  178.7 3.2 %copy.44 = bf16[4,2,2,512,256]{4,3,2,1,0:T(8,128)(2,1)S(1)} copy(bf16[4,2,2,512,256]{4,3,2,0,1:T(8,128)(2,1)} %bitcast.68) | data formatting | bytes 8388608 | tf_op jit(solution)/shard_map/transpose | solution.py:39
  183.8 2.0 fusion
  186.1 30.3 %all-gather.12.cloned.1.call-done = bf16[8,512,128]{2,1,0:T(8,128)(2,1)} async-done(((bf16[2,512,128]{2,1,0:T(8,128)(2,1)}), bf16[8,512,128]{2,1,0:T(8,128)(2,1)}) %all-gather.12.cloned.1.call-update) | async-done | bytes 1048592 | tf_op jit(solution)/shard_map/all_gather | solution.py:35
  216.4 11.6 %all-to-all-done.1 = bf16[32,64,256]{2,1,0:T(8,128)(2,1)S(1)} async-done(((bf16[32,64,256]{2,1,0:T(8,128)(2,1)}), bf16[32,64,256]{2,1,0:T(8,128)(2,1)S(1)}, u32[]{:S(2)}, u32[]{:S(2)}) %all-to-all-start.1) | async-done | bytes 1048608 | tf_op jit(solution)/shard_map/all_to_all | solution.py:67
  228.1 11.3 %all-gather.10.cloned.1.call-done = bf16[8,2,512,128]{3,2,1,0:T(8,128)(2,1)} async-done(((bf16[4,2,512,128]{3,2,1,0:T(8,128)(2,1)}), bf16[8,2,512,128]{3,2,1,0:T(8,128)(2,1)}) %all-gather.10.cloned.1.call-update) | async-done | bytes 2097168 | tf_op jit(solution)/shard_map/all_gather | solution.py:35
  239.4 3.7 %copy.46 = bf16[4,2,2,512,128]{4,1,0,3,2:T(2,128)(2,1)S(1)} copy(bf16[4,2,2,512,128]{4,3,2,0,1:T(8,128)(2,1)} %bitcast.70) | data formatting | bytes 4194304 | tf_op jit(solution)/shard_map/transpose | solution.py:39
  243.2 2.3 reshape.111
  245.5 2.3 convolution_convert_fusion
  249.1 12.4 %all-to-all-start.3 = ((bf16[2,512,256]{2,0,1:T(2,128)(2,1)}), bf16[2,512,256]{2,0,1:T(2,128)(2,1)S(1)}, u32[]{:S(2)}, u32[]{:S(2)}) async-start(bf16[2,512,256]{2,0,1:T(2,128)(2,1)} %copy.47), calls=%async_computation.3 | async-start | bytes 1048576 | tf_op jit(solution)/shard_map/all_to_all | solution.py:95
  261.6 28.9 %all-to-all-done.3 = bf16[2,512,256]{2,0,1:T(2,128)(2,1)S(1)} async-done(((bf16[2,512,256]{2,0,1:T(2,128)(2,1)}), bf16[2,512,256]{2,0,1:T(2,128)(2,1)S(1)}, u32[]{:S(2)}, u32[]{:S(2)}) %all-to-all-start.3) | async-done | bytes 524320 | tf_op jit(solution)/shard_map/all_to_all | solution.py:95
  290.7 2.0 gather_fusion
  292.9 1.4 multiply_reduce_fusion.1
  (55 shorter events, 8.6 us)
Async XLA Ops:
  7.2 1.6 copy-start
  7.2 1.9 copy-start.6
  9.1 29.8 %copy-start.8 = (f32[128]{0:T(128)S(1)}, f32[128]{0:T(128)}, u32[]{:S(2)}) copy-start(f32[128]{0:T(128)} %param.10) | copy-start | bytes 1540
  9.6 29.3 %copy-start.2 = (f32[32,128,128]{2,1,0:T(8,128)S(1)}, f32[32,128,128]{2,1,0:T(8,128)}, u32[]{:S(2)}) copy-start(f32[32,128,128]{2,1,0:T(8,128)} %param.11) | copy-start | bytes 6291460
  14.9 52.9 %all-to-all-start.2 = ((bf16[32,32,256]{2,1,0:T(8,128)(2,1)}), bf16[32,32,256]{2,1,0:T(8,128)(2,1)S(1)}, u32[]{:S(2)}, u32[]{:S(2)}) async-start(bf16[32,32,256]{2,1,0:T(8,128)(2,1)} %bitcast.10), calls=%async_computation.2 | async-start | bytes 1048576 | tf_op jit(solution)/shard_map/all_to_all | solution.py:78
  67.8 0.8 copy-start.3
  68.6 101.6 %all-to-all-start = ((bf16[32,128,256]{2,1,0:T(8,128)(2,1)}), bf16[32,128,256]{2,1,0:T(8,128)(2,1)S(1)}, u32[]{:S(2)}, u32[]{:S(2)}) async-start(bf16[32,128,256]{2,1,0:T(8,128)(2,1)} %pad_maximum_fusion), calls=%async_computation | async-start | bytes 4194304 | tf_op jit(solution)/shard_map/all_to_all | solution.py:19
  75.2 40.9 %all-gather.6.cloned.1.call-start = ((), (), s32[]{:S(2)}) async-start(), calls=%async_computation.4 | async-start | bytes 2621440 | tf_op jit(solution)/shard_map/all_gather | solution.py:35
  77.2 101.6 %all-gather.8.cloned.1.call-start = ((), (), s32[]{:S(2)}) async-start(), calls=%async_computation.5 | async-start | bytes 6291456 | tf_op jit(solution)/shard_map/all_gather | solution.py:35
  170.2 57.8 %all-to-all-start.1 = ((bf16[32,64,256]{2,1,0:T(8,128)(2,1)}), bf16[32,64,256]{2,1,0:T(8,128)(2,1)S(1)}, u32[]{:S(2)}, u32[]{:S(2)}) async-start(bf16[32,64,256]{2,1,0:T(8,128)(2,1)} %convert_element_type.40), calls=%async_computation.1 | async-start | bytes 2097152 | tf_op jit(solution)/shard_map/all_to_all | solution.py:67
  178.1 38.3 %all-gather.12.cloned.1.call-start = ((), (), s32[]{:S(2)}) async-start(), calls=%async_computation.7 | async-start | bytes 1310720 | tf_op jit(solution)/shard_map/all_gather | solution.py:35
  178.7 3.8 %copy-start.1 = (bf16[2,2048,128]{2,1,0:T(8,128)(2,1)}, bf16[2,2048,128]{2,1,0:T(8,128)(2,1)S(1)}, u32[]{:S(2)}) copy-start(bf16[2,2048,128]{2,1,0:T(8,128)(2,1)S(1)} %get-tuple-element.5) | copy-start | bytes 3145732
  178.7 5.1 %copy-start.5 = (bf16[2,2048,128]{2,1,0:T(8,128)(2,1)}, bf16[2,2048,128]{2,1,0:T(8,128)(2,1)S(1)}, u32[]{:S(2)}) copy-start(bf16[2,2048,128]{2,1,0:T(8,128)(2,1)S(1)} %get-tuple-element.4) | copy-start | bytes 3145732
  185.8 53.6 %all-gather.10.cloned.1.call-start = ((), (), s32[]{:S(2)}) async-start(), calls=%async_computation.6 | async-start | bytes 3145728 | tf_op jit(solution)/shard_map/all_gather | solution.py:35
  228.1 17.3 %copy-start.4 = (bf16[16,2,64,256]{3,2,0,1:T(8,128)(2,1)}, bf16[16,2,64,256]{3,2,0,1:T(8,128)(2,1)S(1)}, u32[]{:S(2)}) copy-start(bf16[16,2,64,256]{3,2,0,1:T(8,128)(2,1)S(1)} %copy.38) | copy-start | bytes 3145732
  245.5 16.0 %copy-start.7 = (f32[256,2]{0,1:T(2,128)S(1)}, f32[256,2]{0,1:T(2,128)}, u32[]{:S(2)}) copy-start(f32[256,2]{0,1:T(2,128)} %param.9) | copy-start | bytes 6148
  249.1 41.5 %all-to-all-start.3 = ((bf16[2,512,256]{2,0,1:T(2,128)(2,1)}), bf16[2,512,256]{2,0,1:T(2,128)(2,1)S(1)}, u32[]{:S(2)}, u32[]{:S(2)}) async-start(bf16[2,512,256]{2,0,1:T(2,128)(2,1)} %copy.47), calls=%async_computation.3 | async-start | bytes 1048576 | tf_op jit(solution)/shard_map/all_to_all | solution.py:95
Sparse Core Ops, SparseCore 0:
  78.4 37.6 all-gather.5
  117.9 23.5 all-gather.7
  185.9 30.3 all-gather.11
  218.1 21.3 all-gather.9
where the time goes:
time: 302 us; the launch traced here: 301 us
  waiting for transfers between devices  198 us (66%)
  starting transfers between devices  51.2 us (17%)
  local copies, waits for them, and re-layouts  21.2 us (7%)
  between operations  14.1 us (5%)
  other arithmetic  11.2 us (4%)
  matrix products  5.54 us (2%)
    all_gather x4, waiting for transfers between devices, gather_in_order(): blocks = lax.all_gather(blocks, axes[k], axis=0, tiled=True)  80.4 us
    all_to_all x1, waiting for transfers between devices, in_one_piece(): lax.all_to_all(both, axis, split_axis=split_dim, concat_axis=concat_dim,...  51.4 us
    all_to_all x1, waiting for transfers between devices, on_device(): lax.all_to_all(expert_out, 'fs', split_axis=1, concat_axis=0, tiled=True)  28.9 us
    all_to_all x1, waiting for transfers between devices, on_device(): lax.all_to_all(fill_slots(own_cols, targets, experts, capacity), 'fs', sp...  25.1 us
    all_to_all x1, starting transfers between devices, on_device(): lax.all_to_all(fill_slots(own_cols, targets, experts, capacity), 'fs', sp...  24 us
    all_to_all x1, starting transfers between devices, on_device(): lax.all_to_all(expert_out, 'fs', split_axis=1, concat_axis=0, tiled=True)  12.4 us
    all_to_all x1, waiting for transfers between devices, on_device(): lax.all_to_all(down_local, 'fs', split_axis=0, concat_axis=1, tiled=True)  11.6 us
    all_to_all x1, starting transfers between devices, on_device(): lax.all_to_all(down_local, 'fs', split_axis=0, concat_axis=1, tiled=True)  7.88 us
  transfers between devices with their start and end apart: 8, of which 7 were waited for; matrix products, arithmetic and copies ran while one was open for 5% of the time, Pallas kernels for 0%

commit v1 on v0

v1 whole, which is shorter than its diff:
```python
import jax
import jax.numpy as jnp
from jax import lax
from jax.experimental import pallas as pl
from jax.experimental.pallas import tpu as pltpu
from jax.sharding import Mesh
from jax.sharding import PartitionSpec as P


GROUP_SIZE = 8
TP = ("tp_0", "tp_1")
BF = jnp.bfloat16
F32 = jnp.float32
LANES = 128

VM = pl.BlockSpec(memory_space=pltpu.VMEM)
ANY = pl.BlockSpec(memory_space=pl.ANY)


def shift(x, axis, k):
    n = lax.axis_size(axis)
    return lax.ppermute(x, axis, [(i, (i + k) % n) for i in range(n)])


def shape(dims, dtype=BF):
    return jax.ShapeDtypeStruct(dims, dtype)


def iota(dims, dim):
    return lax.broadcasted_iota(jnp.int32, dims, dim)


def dot(a, b, dims=((1,), (0,))):
    return lax.dot_general(a, b, (dims, ((), ())), preferred_element_type=F32)


def as_column(row):
    n = row.shape[1]
    same = iota((n, n), 0) == iota((n, n), 1)
    return jnp.sum(jnp.where(same, row, jnp.zeros_like(row)), axis=1, keepdims=True)


def slot_of(ids_ref, capacity):
    rows = ids_ref.shape[1]
    ids = [as_column(ids_ref[r : r + 1, :].astype(F32)) for r in range(2)]
    lane = iota((rows, LANES), 1).astype(F32)
    hits = [lane == i for i in ids]
    before = (iota((rows, rows), 0) > iota((rows, rows), 1)).astype(BF)
    count = dot(before, jnp.where(hits[0] | hits[1], 1.0, 0.0).astype(BF))
    return [
        (i * capacity + jnp.sum(jnp.where(h, count, 0.0), axis=1, keepdims=True)).astype(jnp.int32)
        for i, h in zip(ids, hits)
    ]


def pack_first(tokens, route_ids, gain, gate, n, count, capacity):
    tokens_n, model = tokens.shape
    _, whole, cols = gate.shape
    size = whole // count
    width = model // lax.axis_size(TP)
    slots = n * (whole // gain.shape[1]) * capacity
    each = slots // n
    pieces = width // LANES
    gain_rows = gain.shape[1]

    def body(tok_ref, ids_ref, gain_ref, gate_ref, out_ref, buf_ref, sem):
        start = pl.multiple_of(lax.axis_index("grp") * size, size)
        copy = pltpu.make_async_copy(gate_ref.at[:, pl.ds(start, size), :], buf_ref, sem)
        copy.start()
        tok = tok_ref[...].astype(F32)
        scale = lax.rsqrt(jnp.mean(tok * tok, axis=1, keepdims=True) + 1e-06)
        at = pl.multiple_of(lax.axis_index(TP) * width, width)
        own = (tok_ref[:, pl.ds(at, width)].astype(F32) * scale).astype(BF)
        first, second = slot_of(ids_ref, capacity)
        lane = iota((tokens_n, slots), 1)
        pick = jnp.where((lane == first) | (lane == second), 1.0, 0.0).astype(BF)
        filled = dot(pick, own, ((0,), (0,))).astype(BF)
        for j in range(n):
            for p in range(pieces):
                to = size + p * each
                out_ref[j, to : to + each, :] = filled[j * each : (j + 1) * each, p * LANES : (p + 1) * LANES]
        column = as_column(gain_ref[...])
        if size >= gain_rows:
            column = jnp.concatenate([column] * (size // gain_rows), axis=0)
        else:
            skip = lax.axis_index("grp") * size % gain_rows
            row = iota((size, gain_rows), 1) == iota((size, gain_rows), 0) + skip
            column = jnp.sum(jnp.where(row, gain_ref[...], 0.0), axis=1, keepdims=True)
        copy.wait()
        for j in range(n):
            out_ref[j, :size, :] = (buf_ref[j] * column).astype(BF)

    return pl.pallas_call(
        body,
        out_shape=shape((n, size + pieces * each, cols)),
        in_specs=[VM, VM, VM, ANY],
        out_specs=VM,
        scratch_shapes=[pltpu.VMEM((n, size, cols), F32), pltpu.SemaphoreType.DMA],
    )(tokens, route_ids.T, gain, gate)


def gather_tp(x):
    half = x.shape[0] // 2
    left, right = (shift(x, "tp_0", 1), shift(x, "tp_0", -1))
    across = (shift(left[:half], "tp_0", 1), shift(right[half:], "tp_0", -1))
    mine = (x, left, right, *across)
    return mine + tuple(shift(b, "tp_1", 1) for b in mine)


def pieces_of(refs):
    own, x = (lax.axis_index("tp_1"), lax.axis_index("tp_0"))
    for c in range(2):
        core = own if c == 0 else 1 - own
        for at, back in ((0, 0), (1, 3), (2, 1), (3, 2), (4, 2)):
            yield refs[5 * c + at], ((x + back) % 4) * 2 + core, at - 3 if at >= 3 else None


def span(part, rows):
    return slice(0, rows) if part is None else slice(part * rows // 2, (part + 1) * rows // 2)


def first_matmuls(blocks, gate, up, per_device, capacity):
    n, tall, _ = blocks[0].shape
    each = per_device * capacity
    pieces = tall // each
    cols = gate.shape[2]
    rows = n * capacity

    def body(*refs):
        ins, (gate_ref, up_ref, out_ref, acc_ref) = (refs[:10], refs[10:])
        for e in range(per_device):
            acc_ref[...] = jnp.zeros((rows, 2 * cols), F32)
            for ref, tp, part in pieces_of(ins):
                d = pl.ds(pl.multiple_of(tp * (pieces * LANES), pieces * LANES), pieces * LANES)
                w = jnp.concatenate([gate_ref[e, d, :], up_ref[e, d, :]], axis=1)
                x = [
                    ref[:, p * each + e * capacity : p * each + (e + 1) * capacity, :].reshape(-1, LANES)
                    for p in range(pieces)
                ]
                acc_ref[span(part, rows), :] += dot(jnp.concatenate(x, axis=1), w)
            g = acc_ref[:, :cols]
            out_ref[:, e * cols : (e + 1) * cols] = (g / (1.0 + jnp.exp(-g)) * acc_ref[:, cols:]).astype(BF)

    return pl.pallas_call(
        body,
        out_shape=shape((rows, per_device * cols)),
        in_specs=[VM] * 12,
        out_specs=VM,
        scratch_shapes=[pltpu.VMEM((rows, 2 * cols), F32)],
    )(*blocks, gate, up)


def second_matmul(blocks, down, n):
    rows = blocks[0].shape[0]
    per_device, _, cols = down.shape
    width = blocks[0].shape[1] // per_device
    capacity = rows // n

    def body(*refs):
        ins, (down_ref, out_ref, acc_ref) = (refs[:10], refs[10:])
        for e in range(per_device):
            acc_ref[...] = jnp.zeros((rows, cols), F32)
            for ref, tp, part in pieces_of(ins):
                w = down_ref[e, pl.ds(pl.multiple_of(tp * width, width), width), :]
                acc_ref[span(part, rows), :] += dot(ref[:, e * width : (e + 1) * width], w)
            out_ref[:, e] = acc_ref[...].reshape(n, capacity, cols).astype(BF)

    return pl.pallas_call(
        body,
        out_shape=shape((n, per_device, capacity, cols)),
        in_specs=[VM] * 11,
        out_specs=VM,
        scratch_shapes=[pltpu.VMEM((rows, cols), F32)],
    )(*blocks, down)


def combine(returned, route_ids, route_weights, capacity):
    rows, cols = (route_ids.shape[0], returned.shape[1])
    slots = returned.shape[0]

    def body(ret_ref, ids_ref, w_ref, out_ref):
        total = jnp.zeros((rows, cols), F32)
        for r, slot in enumerate(slot_of(ids_ref, capacity)):
            pick = (iota((rows, slots), 1) == slot).astype(BF)
            total = total + dot(pick, ret_ref[...]) * as_column(w_ref[r : r + 1, :])
        out_ref[...] = total.astype(BF)

    return pl.pallas_call(
        body, out_shape=shape((rows, cols)), in_specs=[VM] * 3, out_specs=VM
    )(returned, route_ids.T, route_weights.T)


def by_target(master, n):
    return master.reshape(n, -1, master.shape[2])


def share(master, index, count, n):
    whole = by_target(master, n)
    size = whole.shape[1] // count
    return lax.dynamic_slice_in_dim(whole, index * size, size, 1)


def ring(x, axis):
    n = lax.axis_size(axis)
    out, ahead, behind = ([(0, x)], x, x)
    for k in range(1, n // 2 + 1):
        ahead = shift(ahead, axis, 1)
        out.append((k, ahead))
        if k <= (n - 1) // 2:
            behind = shift(behind, axis, -1)
            out.append((n - k, behind))
    return out


def assemble(pieces, index, count, per_device):
    n, rows, cols = pieces[0][1].shape
    buffer = jnp.zeros((count, n, rows, cols), BF)
    for back, piece in pieces:
        at = (index - back) % count
        buffer = lax.dynamic_update_slice(buffer, piece[None], (at, 0, 0, 0))
    split = count // per_device
    buffer = buffer.reshape(per_device, split, n, rows, cols).transpose(0, 2, 1, 3, 4)
    return buffer.reshape(per_device, -1, cols)


def on_device(tokens, route_ids, route_weights, ffn_gain, gate_master, up_master, down_master):
    n = lax.axis_size("fs")
    count, index = (lax.axis_size("grp"), lax.axis_index("grp"))
    experts, rows, _ = gate_master.shape
    per_device = experts // n
    capacity = tokens.shape[0] // (2 * (experts // GROUP_SIZE))
    size = per_device * rows // count

    def swap(x):
        return lax.all_to_all(x, "fs", split_axis=0, concat_axis=0, tiled=True)

    packed = pack_first(
        tokens, route_ids, ffn_gain[None, :], by_target(gate_master, n), n, count, capacity
    )
    packed = swap(packed)
    if size < rows:
        gain = lax.dynamic_slice_in_dim(ffn_gain, index * size % rows, size)
    else:
        gain = jnp.concatenate([ffn_gain] * (size // rows))
    up = swap((share(up_master, index, count, n) * gain[None, :, None]).astype(BF))
    blocks = gather_tp(packed[:, size:])
    down = swap(share(down_master, index, count, n).astype(BF))
    gate_serve = assemble(ring(packed[:, :size], "grp"), index, count, per_device)
    up_serve = assemble(ring(up, "grp"), index, count, per_device)
    down_serve = assemble(ring(down, "grp"), index, count, per_device)
    hidden = first_matmuls(blocks, gate_serve, up_serve, per_device, capacity)
    hidden = gather_tp(hidden)
    out = second_matmul(hidden, down_serve, n)
    out = swap(out)
    mixed = combine(out.reshape(-1, out.shape[-1]), route_ids, route_weights, capacity)
    return (gate_serve, up_serve, down_serve, mixed)


def solution(mesh):
    grp, fs, tp = (mesh.shape["grp"], mesh.shape["fs"], mesh.shape["tp"])
    split = Mesh(mesh.devices.reshape(grp, fs, tp // 2, 2), ("grp", "fs", *TP))
    in_specs = (
        P(("grp", "fs"), None),
        P(("grp", "fs"), None),
        P(("grp", "fs"), None),
        P("fs"),
        P(None, "fs", TP),
        P(None, "fs", TP),
        P(None, "fs", TP),
    )
    out_specs = (
        P(("grp", "fs"), None, TP),
        P(("grp", "fs"), None, TP),
        P(("grp", "fs"), None, TP),
        P(("grp", "fs"), TP),
    )
    return jax.shard_map(on_device, mesh=split, in_specs=in_specs, out_specs=out_specs, check_vma=False)
```

time: 302 us -> 232 us (0.77)
  waiting for transfers between devices: 198 us -> 97.5 us
  blocking collectives: 0 us -> 40.9 us
  Pallas kernels: 0 us -> 14.7 us
  between operations: 14.1 us -> 0.83 us
  other arithmetic: 11.2 us -> 2.37 us
  matrix products: 5.54 us -> 0 us
    all_gather x4 -> x0, waiting for transfers between devices: 80.4 us -> none  [gather_in_order(): blocks = lax.all_gather(blocks, axes[k], axis=0, tiled=True)]
    all_to_all x4 -> x3, waiting for transfers between devices: 117 us -> 74.4 us  [swap(): return lax.all_to_all(x, 'fs', split_axis=0, concat_axis=0, tiled=True)]
    all_to_all x0 -> x1, blocking collectives: none -> 40.9 us  [swap(): return lax.all_to_all(x, 'fs', split_axis=0, concat_axis=0, tiled=True)]
    ppermute x0 -> x21, waiting for transfers between devices: none -> 23.1 us  [shift(): return lax.ppermute(x, axis, [(i, (i + k) % n) for i in range(n)])]
    pallas_call x0 -> x4, Pallas kernels: none -> 14.7 us  [the longest x1 4.78 us: first_matmuls(): pl.pallas_call(body, out_shape=shape((rows, per_device * cols)), in_specs...]
    ppermute x0 -> x21, starting transfers between devices: none -> 14.3 us  [shift(): return lax.ppermute(x, axis, [(i, (i + k) % n) for i in range(n)])]
    all_to_all x4 -> x3, starting transfers between devices: 50.8 us -> 38.7 us  [swap(): return lax.all_to_all(x, 'fs', split_axis=0, concat_axis=0, tiled=True)]
    dynamic_update_slice x0 -> x6, local copies, waits for them, and re-layouts: none -> 8.69 us  [assemble(): buffer = lax.dynamic_update_slice(buffer, piece[None], (at, 0, 0, 0))]
  transfers between devices with their start and end apart: 8 -> 24, of which waited for: 7 -> 8; matrix products, arithmetic and copies ran while one was open for 5% -> 7% of each run, Pallas kernels for 0% -> 4%
where the time goes in v1:
time: 232 us; the launch traced here: 229 us
  waiting for transfers between devices  97.5 us (42%)
  starting transfers between devices  52.9 us (23%)
  blocking collectives  40.9 us (18%)
  local copies, waits for them, and re-layouts  19.5 us (8%)
  Pallas kernels  14.7 us (6%)
  other arithmetic  2.37 us (1%)
    all_to_all x3, waiting for transfers between devices, swap(): return lax.all_to_all(x, 'fs', split_axis=0, concat_axis=0, tiled=True)  74.4 us
    all_to_all x1, blocking collectives, swap(): return lax.all_to_all(x, 'fs', split_axis=0, concat_axis=0, tiled=True)  40.9 us
    all_to_all x3, starting transfers between devices, swap(): return lax.all_to_all(x, 'fs', split_axis=0, concat_axis=0, tiled=True)  38.7 us
    ppermute x21, waiting for transfers between devices, shift(): return lax.ppermute(x, axis, [(i, (i + k) % n) for i in range(n)])  23.1 us
    ppermute x21, starting transfers between devices, shift(): return lax.ppermute(x, axis, [(i, (i + k) % n) for i in range(n)])  14.3 us
    dynamic_update_slice x6, local copies, waits for them, and re-layouts, assemble(): buffer = lax.dynamic_update_slice(buffer, piece[None], (at, 0, 0, 0))  8.69 us
    pallas_call x1, Pallas kernels, first_matmuls(): pl.pallas_call(body, out_shape=shape((rows, per_device * cols)), in_specs...  4.78 us
  transfers between devices with their start and end apart: 24, of which 8 were waited for; matrix products, arithmetic and copies ran while one was open for 7% of the time, Pallas kernels for 4%

profile of v1, /device:TPU:34, one launch (start us, length us, event | category | flops | bytes accessed | tf_op | source)
XLA Modules:
  0.0 228.7 jit_solution(7905295306812796047)
XLA Ops:
  0.7 2.4 %multiply_convert_fusion = bf16[16,128,128]{2,1,0:T(8,128)(2,1)} fusion(f32[16,256,128]{2,1,0:T(8,128)} %bitcast.27, s32[]{:T(128)S(6)} %select_n.39, f32[128]{0:T(128)} %param.10), kind=kLoop, calls=%fused_computation.1 | loop fusion | flops 524288 | bytes 1573380 | tf_op jit(solution)/shard_map/convert_element_type | solution.py:245
  3.0 24.0 %all-to-all-start.1 = ((bf16[16,128,128]{2,1,0:T(8,128)(2,1)}), bf16[16,128,128]{2,1,0:T(8,128)(2,1)}, u32[]{:S(2)}, u32[]{:S(2)}) async-start(bf16[16,128,128]{2,1,0:T(8,128)(2,1)} %multiply_convert_fusion), calls=%async_computation.1 | async-start | bytes 1048576 | tf_op jit(solution)/shard_map/all_to_all | solution.py:235
  27.0 3.5 %shard_map.102 = bf16[16,256,128]{2,1,0:T(8,128)(2,1)} custom-call(bf16[256,2048]{1,0:T(8,128)(2,1)} %tok_ref.1, s32[2,256]{1,0:T(2,128)} %bitcast.28, f32[1,128]{1,0:T(1,128)} %bitcast.31, f32[16,256,128]{2,1,0:T(8,128)} %bitcast.26), custom_call_target="tpu_custom_call" | custom-call | tf_op jit(solution)/shard_map/pallas_call | solution.py:93
  30.5 25.5 %all-to-all-done.1 = bf16[16,128,128]{2,1,0:T(8,128)(2,1)} async-done(((bf16[16,128,128]{2,1,0:T(8,128)(2,1)}), bf16[16,128,128]{2,1,0:T(8,128)(2,1)}, u32[]{:S(2)}, u32[]{:S(2)}) %all-to-all-start.1) | async-done | bytes 524320 | tf_op jit(solution)/shard_map/all_to_all | solution.py:235
  56.0 6.6 %all-to-all-start = ((bf16[16,256,128]{2,1,0:T(8,128)(2,1)}), bf16[16,256,128]{2,1,0:T(8,128)(2,1)S(1)}, u32[]{:S(2)}, u32[]{:S(2)}) async-start(bf16[16,256,128]{2,1,0:T(8,128)(2,1)} %shard_map.102), calls=%async_computation | async-start | bytes 2097152 | tf_op jit(solution)/shard_map/all_to_all | solution.py:235
  63.5 48.9 %all-to-all-done = bf16[16,256,128]{2,1,0:T(8,128)(2,1)S(1)} async-done(((bf16[16,256,128]{2,1,0:T(8,128)(2,1)}), bf16[16,256,128]{2,1,0:T(8,128)(2,1)S(1)}, u32[]{:S(2)}, u32[]{:S(2)}) %all-to-all-start) | async-done | bytes 1048608 | tf_op jit(solution)/shard_map/all_to_all | solution.py:235
  112.4 8.1 %all-to-all-start.2 = ((bf16[16,64,256]{2,1,0:T(8,128)(2,1)}), bf16[16,64,256]{2,1,0:T(8,128)(2,1)}, u32[]{:S(2)}, u32[]{:S(2)}) async-start(bf16[16,64,256]{2,1,0:T(8,128)(2,1)} %dynamic-slice_convert_fusion), calls=%async_computation.2 | async-start | bytes 1048576 | tf_op jit(solution)/shard_map/all_to_all | solution.py:235
  121.6 1.6 collective-permute-start.3
  123.6 2.1 collective-permute-start.1
  125.8 9.7 %collective-permute-done.3.refs_1_ = bf16[16,128,128]{2,1,0:T(8,128)(2,1)} collective-permute-done((bf16[16,128,128]{2,1,0:T(8,128)(2,1)}, bf16[16,128,128]{2,1,0:T(8,128)(2,1)}, u32[]{:S(2)}, u32[]{:S(2)}) %collective-permute-start.3) | collective-permute-done | bytes 524320 | tf_op jit(solution)/shard_map/ppermute | solution.py:22
  135.5 1.7 slice.26
  137.2 1.6 collective-permute-start.5
  138.8 1.7 slice.27
  142.1 1.9 bitcast_dynamic-update-slice_fusion.3
  143.9 4.6 %collective-permute-done = bf16[16,128,128]{2,1,0:T(8,128)(2,1)} collective-permute-done((bf16[16,128,128]{2,1,0:T(8,128)(2,1)}, bf16[16,128,128]{2,1,0:T(8,128)(2,1)}, u32[]{:S(2)}, u32[]{:S(2)}) %collective-permute-start) | collective-permute-done | bytes 524320 | tf_op jit(solution)/shard_map/ppermute | solution.py:22
  148.6 1.9 bitcast_dynamic-update-slice_fusion.2
  150.5 1.7 collective-permute-start.2
  154.8 1.9 bitcast_dynamic-update-slice_fusion.4
  158.1 4.8 %shard_map.103.refs_0_ = bf16[512,256]{1,0:T(8,128)(2,1)} custom-call(bf16[16,128,128]{2,1,0:T(8,128)(2,1)} %get-tuple-element.4.refs_0_, bf16[16,128,128]{2,1,0:T(8,128)(2,1)} %collective-permute-done.3.refs_1_, bf16[16,128,128]{2,1,0:T(8,128)(2,1)} %collective-permute-done.4.refs_2_, bf16[8,128,128]{2,1,0:T(8,128)(2,1)} %copy-done.7, ...), custom_call_target="tpu_custom_call" | custom-call | tf_op jit(solution)/shard_map/pallas_call | solution.py:144
  164.9 6.8 %collective-permute-done.12.refs_1_ = bf16[512,256]{1,0:T(8,128)(2,1)S(1)} collective-permute-done((bf16[512,256]{1,0:T(8,128)(2,1)}, bf16[512,256]{1,0:T(8,128)(2,1)S(1)}, u32[]{:S(2)}, u32[]{:S(2)}) %collective-permute-start.12) | collective-permute-done | bytes 262176 | tf_op jit(solution)/shard_map/ppermute | solution.py:22
  171.7 1.7 collective-permute-start.14
  181.4 3.9 %shard_map.104 = bf16[16,2,32,256]{3,2,1,0:T(8,128)(2,1)} custom-call(bf16[512,256]{1,0:T(8,128)(2,1)} %shard_map.103.refs_0_, bf16[512,256]{1,0:T(8,128)(2,1)} %copy-done.2, bf16[512,256]{1,0:T(8,128)(2,1)} %copy-done.3, bf16[256,256]{1,0:T(8,128)(2,1)} %copy-done.10, bf16[256,256]{1,0:T(8,128)(2,1)} %copy-done.11, bf16[512,256]{1,0:T(8,128)(2,1)} %copy-done.4, ...), custom_call_target="tpu_custom_call" | custom-call | tf_op jit(solution)/shard_map/pallas_call | solution.py:168
  185.3 40.9 %all_to_all.20 = bf16[16,2,32,256]{3,2,1,0:T(8,128)(2,1)} all-to-all(bf16[16,2,32,256]{3,2,1,0:T(8,128)(2,1)} %shard_map.104), channel_id=1, replica_groups=mesh['grp'=2,'fs'=16,'tp_0'=4,'tp_1'=2] {'fs'}, dimensions={0} | all-to-all | bytes 1048576 | tf_op jit(solution)/shard_map/all_to_all | solution.py:235
  226.3 2.5 %shard_map.105 = bf16[256,256]{1,0:T(8,128)(2,1)} custom-call(bf16[1024,256]{1,0:T(8,128)(2,1)} %bitcast.25, s32[2,256]{1,0:T(2,128)} %bitcast.29, f32[2,256]{1,0:T(2,128)} %bitcast.30), custom_call_target="tpu_custom_call" | custom-call | tf_op jit(solution)/shard_map/pallas_call | solution.py:188
  (73 shorter events, 18.0 us)
Async XLA Ops:
  3.0 53.0 %all-to-all-start.1 = ((bf16[16,128,128]{2,1,0:T(8,128)(2,1)}), bf16[16,128,128]{2,1,0:T(8,128)(2,1)}, u32[]{:S(2)}, u32[]{:S(2)}) async-start(bf16[16,128,128]{2,1,0:T(8,128)(2,1)} %multiply_convert_fusion), calls=%async_computation.1 | async-start | bytes 1048576 | tf_op jit(solution)/shard_map/all_to_all | solution.py:235
  56.0 56.4 %all-to-all-start = ((bf16[16,256,128]{2,1,0:T(8,128)(2,1)}), bf16[16,256,128]{2,1,0:T(8,128)(2,1)S(1)}, u32[]{:S(2)}, u32[]{:S(2)}) async-start(bf16[16,256,128]{2,1,0:T(8,128)(2,1)} %shard_map.102), calls=%async_computation | async-start | bytes 2097152 | tf_op jit(solution)/shard_map/all_to_all | solution.py:235
  112.4 38.0 %all-to-all-start.2 = ((bf16[16,64,256]{2,1,0:T(8,128)(2,1)}), bf16[16,64,256]{2,1,0:T(8,128)(2,1)}, u32[]{:S(2)}, u32[]{:S(2)}) async-start(bf16[16,64,256]{2,1,0:T(8,128)(2,1)} %dynamic-slice_convert_fusion), calls=%async_computation.2 | async-start | bytes 1048576 | tf_op jit(solution)/shard_map/all_to_all | solution.py:235
  121.6 13.9 %collective-permute-start.3 = (bf16[16,128,128]{2,1,0:T(8,128)(2,1)}, bf16[16,128,128]{2,1,0:T(8,128)(2,1)}, u32[]{:S(2)}, u32[]{:S(2)}) collective-permute-start(bf16[16,128,128]{2,1,0:T(8,128)(2,1)} %get-tuple-element.4.refs_0_), channel_id=1, source_target_pairs={{0,2},{2,4},{4,6},{6,0},{1,3},{3,5},{5,7},{7,1},{8,10},{10,12},{12... | collective-permute-start | bytes 1572872 | tf_op jit(solution)/shard_map/ppermute | solution.py:22
  123.2 15.6 %collective-permute-start.4 = (bf16[16,128,128]{2,1,0:T(8,128)(2,1)}, bf16[16,128,128]{2,1,0:T(8,128)(2,1)}, u32[]{:S(2)}, u32[]{:S(2)}) collective-permute-start(bf16[16,128,128]{2,1,0:T(8,128)(2,1)} %get-tuple-element.4.refs_0_), channel_id=1, source_target_pairs={{0,6},{2,0},{4,2},{6,4},{1,7},{3,1},{5,3},{7,5},{8,14},{10,8},{12,... | collective-permute-start | bytes 1572872 | tf_op jit(solution)/shard_map/ppermute | solution.py:22
  123.6 20.3 %collective-permute-start.1 = (bf16[16,128,128]{2,1,0:T(8,128)(2,1)}, bf16[16,128,128]{2,1,0:T(8,128)(2,1)}, u32[]{:S(2)}, u32[]{:S(2)}) collective-permute-start(bf16[16,128,128]{2,1,0:T(8,128)(2,1)} %all-to-all-done.1), channel_id=1, source_target_pairs={{0,128},{128,0},{1,129},{129,1},{2,130},{130,2},{3,131},{131,3},{4... | collective-permute-start | bytes 1572872 | tf_op jit(solution)/shard_map/ppermute | solution.py:22
  125.7 22.8 %collective-permute-start = (bf16[16,128,128]{2,1,0:T(8,128)(2,1)}, bf16[16,128,128]{2,1,0:T(8,128)(2,1)}, u32[]{:S(2)}, u32[]{:S(2)}) collective-permute-start(bf16[16,128,128]{2,1,0:T(8,128)(2,1)} %get-tuple-element.5), channel_id=1, source_target_pairs={{0,128},{128,0},{1,129},{129,1},{2,130},{130,2},{3,131},{131,3},{4... | collective-permute-start | bytes 1572872 | tf_op jit(solution)/shard_map/ppermute | solution.py:22
  125.8 24.7 %collective-permute-start.7 = (bf16[16,128,128]{2,1,0:T(8,128)(2,1)}, bf16[16,128,128]{2,1,0:T(8,128)(2,1)}, u32[]{:S(2)}, u32[]{:S(2)}) collective-permute-start(bf16[16,128,128]{2,1,0:T(8,128)(2,1)} %get-tuple-element.4.refs_0_), channel_id=1, source_target_pairs={{0,1},{1,0},{2,3},{3,2},{4,5},{5,4},{6,7},{7,6},{8,9},{9,8},{10,11... | collective-permute-start | bytes 1572872 | tf_op jit(solution)/shard_map/ppermute | solution.py:22
  137.2 15.1 %collective-permute-start.5 = (bf16[8,128,128]{2,1,0:T(8,128)(2,1)}, bf16[8,128,128]{2,1,0:T(8,128)(2,1)S(1)}, u32[]{:S(2)}, u32[]{:S(2)}) collective-permute-start(bf16[8,128,128]{2,1,0:T(8,128)(2,1)} %slice.26), channel_id=1, source_target_pairs={{0,2},{2,4},{4,6},{6,0},{1,3},{3,5},{5,7},{7,1},{8,10},{10,12},{12... | collective-permute-start | bytes 786440 | tf_op jit(solution)/shard_map/ppermute | solution.py:22
  140.5 12.0 %collective-permute-start.6 = (bf16[8,128,128]{2,1,0:T(8,128)(2,1)}, bf16[8,128,128]{2,1,0:T(8,128)(2,1)}, u32[]{:S(2)}, u32[]{:S(2)}) collective-permute-start(bf16[8,128,128]{2,1,0:T(8,128)(2,1)} %slice.27), channel_id=1, source_target_pairs={{0,6},{2,0},{4,2},{6,4},{1,7},{3,1},{5,3},{7,5},{8,14},{10,8},{12,... | collective-permute-start | bytes 786440 | tf_op jit(solution)/shard_map/ppermute | solution.py:22
  143.9 12.7 %collective-permute-start.8 = (bf16[16,128,128]{2,1,0:T(8,128)(2,1)}, bf16[16,128,128]{2,1,0:T(8,128)(2,1)}, u32[]{:S(2)}, u32[]{:S(2)}) collective-permute-start(bf16[16,128,128]{2,1,0:T(8,128)(2,1)} %collective-permute-done.3.refs_1_), channel_id=1, source_target_pairs={{0,1},{1,0},{2,3},{3,2},{4,5},{5,4},{6,7},{7,6},{8,9},{9,8},{10,11... | collective-permute-start | bytes 1572872 | tf_op jit(solution)/shard_map/ppermute | solution.py:22
  148.6 8.1 %collective-permute-start.9 = (bf16[16,128,128]{2,1,0:T(8,128)(2,1)}, bf16[16,128,128]{2,1,0:T(8,128)(2,1)}, u32[]{:S(2)}, u32[]{:S(2)}) collective-permute-start(bf16[16,128,128]{2,1,0:T(8,128)(2,1)} %collective-permute-done.4.refs_2_), channel_id=1, source_target_pairs={{0,1},{1,0},{2,3},{3,2},{4,5},{5,4},{6,7},{7,6},{8,9},{9,8},{10,11... | collective-permute-start | bytes 1572872 | tf_op jit(solution)/shard_map/ppermute | solution.py:22
  150.5 24.5 %collective-permute-start.2 = (bf16[16,64,256]{2,1,0:T(8,128)(2,1)}, bf16[16,64,256]{2,1,0:T(8,128)(2,1)}, u32[]{:S(2)}, u32[]{:S(2)}) collective-permute-start(bf16[16,64,256]{2,1,0:T(8,128)(2,1)} %all-to-all-done.2), channel_id=1, source_target_pairs={{0,128},{128,0},{1,129},{129,1},{2,130},{130,2},{3,131},{131,3},{4... | collective-permute-start | bytes 1572872 | tf_op jit(solution)/shard_map/ppermute | solution.py:22
  152.2 4.5 %collective-permute-start.10 = (bf16[8,128,128]{2,1,0:T(8,128)(2,1)S(1)}, bf16[8,128,128]{2,1,0:T(8,128)(2,1)S(1)}, u32[]{:S(2)}, u32[]{:S(2)}) collective-permute-start(bf16[8,128,128]{2,1,0:T(8,128)(2,1)S(1)} %collective-permute-done.5.refs_3_), channel_id=1, source_target_pairs={{0,1},{1,0},{2,3},{3,2},{4,5},{5,4},{6,7},{7,6},{8,9},{9,8},{10,11... | collective-permute-start | bytes 786440 | tf_op jit(solution)/shard_map/ppermute | solution.py:22
  152.4 5.0 %collective-permute-start.11 = (bf16[8,128,128]{2,1,0:T(8,128)(2,1)}, bf16[8,128,128]{2,1,0:T(8,128)(2,1)S(1)}, u32[]{:S(2)}, u32[]{:S(2)}) collective-permute-start(bf16[8,128,128]{2,1,0:T(8,128)(2,1)} %collective-permute-done.6.refs_4_), channel_id=1, source_target_pairs={{0,1},{1,0},{2,3},{3,2},{4,5},{5,4},{6,7},{7,6},{8,9},{9,8},{10,11... | collective-permute-start | bytes 786440 | tf_op jit(solution)/shard_map/ppermute | solution.py:22
  162.9 8.8 %collective-permute-start.12 = (bf16[512,256]{1,0:T(8,128)(2,1)}, bf16[512,256]{1,0:T(8,128)(2,1)S(1)}, u32[]{:S(2)}, u32[]{:S(2)}) collective-permute-start(bf16[512,256]{1,0:T(8,128)(2,1)} %shard_map.103.refs_0_), channel_id=1, source_target_pairs={{0,2},{2,4},{4,6},{6,0},{1,3},{3,5},{5,7},{7,1},{8,10},{10,12},{12... | collective-permute-start | bytes 786440 | tf_op jit(solution)/shard_map/ppermute | solution.py:22
  164.5 8.8 %collective-permute-start.13 = (bf16[512,256]{1,0:T(8,128)(2,1)}, bf16[512,256]{1,0:T(8,128)(2,1)S(1)}, u32[]{:S(2)}, u32[]{:S(2)}) collective-permute-start(bf16[512,256]{1,0:T(8,128)(2,1)} %shard_map.103.refs_0_), channel_id=1, source_target_pairs={{0,6},{2,0},{4,2},{6,4},{1,7},{3,1},{5,3},{7,5},{8,14},{10,8},{12,... | collective-permute-start | bytes 786440 | tf_op jit(solution)/shard_map/ppermute | solution.py:22
  164.9 14.7 %collective-permute-start.16 = (bf16[512,256]{1,0:T(8,128)(2,1)}, bf16[512,256]{1,0:T(8,128)(2,1)S(1)}, u32[]{:S(2)}, u32[]{:S(2)}) collective-permute-start(bf16[512,256]{1,0:T(8,128)(2,1)} %shard_map.103.refs_0_), channel_id=1, source_target_pairs={{0,1},{1,0},{2,3},{3,2},{4,5},{5,4},{6,7},{7,6},{8,9},{9,8},{10,11... | collective-permute-start | bytes 786440 | tf_op jit(solution)/shard_map/ppermute | solution.py:22
  171.7 6.2 %collective-permute-start.14 = (bf16[256,256]{1,0:T(8,128)(2,1)S(1)}, bf16[256,256]{1,0:T(8,128)(2,1)S(1)}, u32[]{:S(2)}, u32[]{:S(2)}) collective-permute-start(bf16[256,256]{1,0:T(8,128)(2,1)S(1)} %slice.28), channel_id=1, source_target_pairs={{0,2},{2,4},{4,6},{6,0},{1,3},{3,5},{5,7},{7,1},{8,10},{10,12},{12... | collective-permute-start | bytes 393224 | tf_op jit(solution)/shard_map/ppermute | solution.py:22
  173.4 5.1 %collective-permute-start.15 = (bf16[256,256]{1,0:T(8,128)(2,1)S(1)}, bf16[256,256]{1,0:T(8,128)(2,1)S(1)}, u32[]{:S(2)}, u32[]{:S(2)}) collective-permute-start(bf16[256,256]{1,0:T(8,128)(2,1)S(1)} %slice.29), channel_id=1, source_target_pairs={{0,6},{2,0},{4,2},{6,4},{1,7},{3,1},{5,3},{7,5},{8,14},{10,8},{12,... | collective-permute-start | bytes 393224 | tf_op jit(solution)/shard_map/ppermute | solution.py:22
  174.9 4.9 %collective-permute-start.17 = (bf16[512,256]{1,0:T(8,128)(2,1)S(1)}, bf16[512,256]{1,0:T(8,128)(2,1)S(1)}, u32[]{:S(2)}, u32[]{:S(2)}) collective-permute-start(bf16[512,256]{1,0:T(8,128)(2,1)S(1)} %collective-permute-done.12.refs_1_), channel_id=1, source_target_pairs={{0,1},{1,0},{2,3},{3,2},{4,5},{5,4},{6,7},{7,6},{8,9},{9,8},{10,11... | collective-permute-start | bytes 786440 | tf_op jit(solution)/shard_map/ppermute | solution.py:22
  174.9 4.9 %collective-permute-start.18 = (bf16[512,256]{1,0:T(8,128)(2,1)S(1)}, bf16[512,256]{1,0:T(8,128)(2,1)S(1)}, u32[]{:S(2)}, u32[]{:S(2)}) collective-permute-start(bf16[512,256]{1,0:T(8,128)(2,1)S(1)} %collective-permute-done.13.refs_2_), channel_id=1, source_target_pairs={{0,1},{1,0},{2,3},{3,2},{4,5},{5,4},{6,7},{7,6},{8,9},{9,8},{10,11... | collective-permute-start | bytes 786440 | tf_op jit(solution)/shard_map/ppermute | solution.py:22
  177.8 1.8 collective-permute-start.19
  178.4 1.3 collective-permute-start.20
  (14 other events, 96.3 us)

commit v2 on v1

v2 whole, which is shorter than its diff:
```python
import jax
import jax.numpy as jnp
from jax import lax
from jax.experimental import pallas as pl
from jax.experimental.pallas import tpu as pltpu
from jax.sharding import Mesh
from jax.sharding import PartitionSpec as P


GROUP_SIZE = 8
TP = ("tp_0", "tp_1")
BF = jnp.bfloat16
F32 = jnp.float32
LANES = 128
META = 8

VM = pl.BlockSpec(memory_space=pltpu.VMEM)
ANY = pl.BlockSpec(memory_space=pl.ANY)


def shift(x, axis, k):
    n = lax.axis_size(axis)
    return lax.ppermute(x, axis, [(i, (i + k) % n) for i in range(n)])


def shape(dims, dtype=BF):
    return jax.ShapeDtypeStruct(dims, dtype)


def iota(dims, dim):
    return lax.broadcasted_iota(jnp.int32, dims, dim)


def dot(a, b, dims=((1,), (0,))):
    return lax.dot_general(a, b, (dims, ((), ())), preferred_element_type=F32)


def as_column(row):
    n = row.shape[1]
    same = iota((n, n), 0) == iota((n, n), 1)
    return jnp.sum(jnp.where(same, row, jnp.zeros_like(row)), axis=1, keepdims=True)


def slot_of(ids_ref, capacity):
    rows = ids_ref.shape[1]
    ids = [as_column(ids_ref[r : r + 1, :].astype(F32)) for r in range(2)]
    lane = iota((rows, LANES), 1).astype(F32)
    hits = [lane == i for i in ids]
    before = (iota((rows, rows), 0) > iota((rows, rows), 1)).astype(BF)
    count = dot(before, jnp.where(hits[0] | hits[1], 1.0, 0.0).astype(BF))
    return [
        (i * capacity + jnp.sum(jnp.where(h, count, 0.0), axis=1, keepdims=True)).astype(jnp.int32)
        for i, h in zip(ids, hits)
    ]


def fetch(pairs, sems):
    copies = [pltpu.make_async_copy(src, dst, sems.at[i]) for i, (src, dst) in enumerate(pairs)]
    for c in copies:
        c.start()
    return [c.wait for c in copies]


def pack_first(tokens, route_ids, gain, gate, n, count, groups):
    tokens_n, model = tokens.shape
    _, whole, cols = gate.shape
    size = whole // count
    width = model // lax.axis_size(TP)
    part = tokens_n // groups
    members = n // groups
    each = part // members
    pieces = width // LANES
    gain_rows = gain.shape[1]

    def body(tok_ref, ids_ref, gain_ref, gate_ref, out_ref, buf_ref, sem):
        start = pl.multiple_of(lax.axis_index("grp") * size, size)
        copy = pltpu.make_async_copy(gate_ref.at[:, pl.ds(start, size), :], buf_ref, sem)
        copy.start()
        tok = tok_ref[...].astype(F32)
        scale = lax.rsqrt(jnp.mean(tok * tok, axis=1, keepdims=True) + 1e-06)
        at = pl.multiple_of(lax.axis_index(TP) * width, width)
        own = (tok_ref[:, pl.ds(at, width)].astype(F32) * scale).astype(BF)
        ids = [as_column(ids_ref[r : r + 1, :].astype(F32)) for r in range(2)]
        group = ids[0].astype(jnp.int32) // GROUP_SIZE
        member = iota((tokens_n, LANES), 1) == group
        before = (iota((tokens_n, tokens_n), 0) > iota((tokens_n, tokens_n), 1)).astype(BF)
        count_before = dot(before, jnp.where(member, 1.0, 0.0).astype(BF))
        rank = jnp.sum(jnp.where(member, count_before, 0.0), axis=1, keepdims=True)
        place = iota((tokens_n, tokens_n), 1) == group * part + rank.astype(jnp.int32)
        ordered = dot(jnp.where(place, 1.0, 0.0).astype(BF), own, ((0,), (0,))).astype(BF)
        local = [i - (group * GROUP_SIZE).astype(F32) for i in ids]
        named = [jnp.sum(jnp.where(place, i, 0.0), axis=0, keepdims=True) for i in local]
        named = jnp.concatenate(named + [jnp.zeros((META - 2, tokens_n), F32)], axis=0)
        for j in range(n):
            first = j * each
            for p in range(pieces):
                to = size + p * each
                out_ref[j, to : to + each, :] = ordered[first : first + each, p * LANES : (p + 1) * LANES]
            a = j // members
            piece = named[:, a * part : (a + 1) * part]
            piece = jnp.concatenate([piece, jnp.zeros((META, LANES - part), F32)], axis=1)
            out_ref[j, size + pieces * each :, :] = piece.astype(BF)
        column = as_column(gain_ref[...])
        if size >= gain_rows:
            column = jnp.concatenate([column] * (size // gain_rows), axis=0)
        else:
            skip = lax.axis_index("grp") * size % gain_rows
            row = iota((size, gain_rows), 1) == iota((size, gain_rows), 0) + skip
            column = jnp.sum(jnp.where(row, gain_ref[...], 0.0), axis=1, keepdims=True)
        copy.wait()
        for j in range(n):
            out_ref[j, :size, :] = (buf_ref[j] * column).astype(BF)

    return pl.pallas_call(
        body,
        out_shape=shape((n, size + pieces * each + META, cols)),
        in_specs=[VM, VM, VM, ANY],
        out_specs=VM,
        scratch_shapes=[pltpu.VMEM((n, size, cols), F32), pltpu.SemaphoreType.DMA],
    )(tokens, route_ids.T, gain, gate)


def select_rows(blocks, named, per_device, capacity):
    members = len(blocks)
    n, tall, _ = blocks[0].shape
    pieces = 2 * LANES // LANES
    each = tall // pieces
    part = members * each

    def body(*refs):
        ins, (named_ref, *outs) = (refs[:members], refs[members : members + 1 + per_device])
        row_ref = refs[-1]
        here = lax.axis_index("fs") % members
        for k in range(members):
            back = here - k
            back = jnp.where(back < 0, back + members, back)
            to = pl.ds(pl.multiple_of(back * each, each), each)
            for p in range(pieces):
                row_ref[:, to, p * LANES : (p + 1) * LANES] = ins[k][:, p * each : (p + 1) * each, :]
        named_rows = named_ref[...].astype(F32)
        one, two = [
            jnp.concatenate([named_rows[j, r : r + 1, :part] for j in range(n)], axis=0) for r in range(2)
        ]
        earlier = (iota((part, part), 0) < iota((part, part), 1)).astype(BF)
        slot = iota((capacity, part), 0).astype(F32)
        ranks = []
        for k in range(per_device):
            e = here * per_device + expert_at(k, per_device)
            hit = (one == e.astype(F32)) | (two == e.astype(F32))
            rank = dot(jnp.where(hit, 1.0, 0.0).astype(BF), earlier)
            ranks.append(jnp.where(hit, rank, -1.0))
        for j in range(n):
            pick = [jnp.where(slot == ranks[k][j : j + 1], 1.0, 0.0) for k in range(per_device)]
            got = dot(jnp.concatenate(pick, axis=0).astype(BF), row_ref[j]).astype(BF)
            for k in range(per_device):
                for p in range(pieces):
                    outs[k][j, p * capacity : (p + 1) * capacity, :] = got[
                        k * capacity : (k + 1) * capacity, p * LANES : (p + 1) * LANES
                    ]

    return pl.pallas_call(
        body,
        out_shape=tuple(shape((n, pieces * capacity, LANES)) for _ in range(per_device)),
        in_specs=[VM] * (members + 1),
        out_specs=tuple(VM for _ in range(per_device)),
        scratch_shapes=[pltpu.VMEM((n, part, pieces * LANES), BF)],
    )(*blocks, named)


def expert_at(k, per_device):
    return (lax.axis_index("grp") + per_device - k) % per_device


def gather_tp(x, back):
    left, right = (shift(x, "tp_0", 1), shift(x, "tp_0", -1))
    across = shift(right, "tp_0", -1) if back else shift(left, "tp_0", 1)
    mine = (x, left, right, across)
    return mine + tuple(shift(b, "tp_1", 1) for b in mine)


def places_of():
    own, x = (lax.axis_index("tp_1"), lax.axis_index("tp_0"))
    return [
        ((x + ahead) % 4) * 2 + core for core in (own, 1 - own) for ahead in (0, 3, 1, 2)
    ]


def first_matmuls(blocks, gate, up, capacity):
    n, tall, _ = blocks[0].shape
    pieces = tall // capacity
    depth, cols = gate.shape
    rows = n * capacity
    count = len(blocks)

    def body(*refs):
        ins, (gate_ref, up_ref, out_ref, in_buf, gate_buf, up_buf, acc_ref, sems) = (
            refs[:count],
            refs[count:],
        )
        waits = fetch(
            [(gate_ref, gate_buf), (up_ref, up_buf)] + [(r, in_buf.at[i]) for i, r in enumerate(ins)], sems
        )
        waits[0]()
        waits[1]()
        for i, tp in enumerate(places_of()):
            d = pl.ds(pl.multiple_of(tp * (pieces * LANES), pieces * LANES), pieces * LANES)
            w = jnp.concatenate([gate_buf[d, :], up_buf[d, :]], axis=1)
            waits[2 + i]()
            x = [
                in_buf[i, :, p * capacity : (p + 1) * capacity, :].reshape(rows, LANES)
                for p in range(pieces)
            ]
            more = dot(jnp.concatenate(x, axis=1), w)
            if i == 0:
                acc_ref[...] = more
            else:
                acc_ref[...] += more
        g = acc_ref[:, :cols]
        out_ref[...] = (g / (1.0 + jnp.exp(-g)) * acc_ref[:, cols:]).astype(BF)

    return pl.pallas_call(
        body,
        out_shape=shape((rows, cols)),
        in_specs=[ANY] * (count + 2),
        out_specs=VM,
        scratch_shapes=[
            pltpu.VMEM((count, n, tall, LANES), BF),
            pltpu.VMEM((depth, cols), BF),
            pltpu.VMEM((depth, cols), BF),
            pltpu.VMEM((rows, 2 * cols), F32),
            pltpu.SemaphoreType.DMA((count + 2,)),
        ],
    )(*blocks, gate, up)


def second_matmul(blocks, down, n, k, per_device, before):
    rows, width = blocks[0].shape
    depth, cols = down.shape
    capacity = rows // n
    count = len(blocks)
    given = 0 if before is None else 1

    def body(*refs):
        ins, rest = (refs[:count], refs[count : count + 1] + refs[count + 1 + given :])
        down_ref, out_ref, in_buf, down_buf, acc_ref, row_ref, sems, sem = rest
        waits = fetch([(down_ref, down_buf)] + [(r, in_buf.at[i]) for i, r in enumerate(ins)], sems)
        waits[0]()
        for i, tp in enumerate(places_of()):
            w = down_buf[pl.ds(pl.multiple_of(tp * width, width), width), :]
            waits[1 + i]()
            more = dot(in_buf[i], w)
            if i == 0:
                acc_ref[...] = more
            else:
                acc_ref[...] += more
        row_ref[...] = acc_ref[...].reshape(n, capacity, cols).astype(BF)
        copy = pltpu.make_async_copy(row_ref, out_ref.at[:, expert_at(k, per_device)], sem)
        copy.start()
        copy.wait()

    return pl.pallas_call(
        body,
        out_shape=shape((n, per_device, capacity, cols)),
        in_specs=[ANY] * (count + 1 + given),
        out_specs=ANY,
        input_output_aliases={count + 1: 0} if given else {},
        scratch_shapes=[
            pltpu.VMEM((count, rows, width), BF),
            pltpu.VMEM((depth, cols), BF),
            pltpu.VMEM((rows, cols), F32),
            pltpu.VMEM((n, capacity, cols), BF),
            pltpu.SemaphoreType.DMA((count + 1,)),
            pltpu.SemaphoreType.DMA,
        ],
    )(*blocks, down, *([] if before is None else [before]))


def combine(returned, route_ids, route_weights, capacity):
    rows, cols = (route_ids.shape[0], returned.shape[1])
    slots = returned.shape[0]

    def body(ret_ref, ids_ref, w_ref, out_ref):
        total = jnp.zeros((rows, cols), F32)
        for r, slot in enumerate(slot_of(ids_ref, capacity)):
            pick = (iota((rows, slots), 1) == slot).astype(BF)
            total = total + dot(pick, ret_ref[...]) * as_column(w_ref[r : r + 1, :])
        out_ref[...] = total.astype(BF)

    return pl.pallas_call(
        body, out_shape=shape((rows, cols)), in_specs=[VM] * 3, out_specs=VM
    )(returned, route_ids.T, route_weights.T)


def by_target(master, n):
    return master.reshape(n, -1, master.shape[2])


def share(master, index, count, n):
    whole = by_target(master, n)
    size = whole.shape[1] // count
    return lax.dynamic_slice_in_dim(whole, index * size, size, 1)


def ring(x, axis):
    n = lax.axis_size(axis)
    out, ahead, behind = ([(0, x)], x, x)
    for k in range(1, n // 2 + 1):
        ahead = shift(ahead, axis, 1)
        out.append((k, ahead))
        if k <= (n - 1) // 2:
            behind = shift(behind, axis, -1)
            out.append((n - k, behind))
    return out


def assemble(pieces, index, count, per_device):
    n, rows, cols = pieces[0][1].shape
    buffer = jnp.zeros((count, n, rows, cols), BF)
    for back, piece in pieces:
        at = (index - back) % count
        buffer = lax.dynamic_update_slice(buffer, piece[None], (at, 0, 0, 0))
    split = count // per_device
    buffer = buffer.reshape(per_device, split, n, rows, cols).transpose(0, 2, 1, 3, 4)
    return buffer.reshape(per_device, -1, cols)


def one_by_one(pieces, served, index, count, per_device):
    if count == per_device:
        return [p.reshape(-1, p.shape[-1]) for _, p in sorted(pieces, key=lambda q: q[0])]
    return [
        lax.dynamic_index_in_dim(served, (index + per_device - k) % per_device, 0, False)
        for k in range(per_device)
    ]


def on_device(tokens, route_ids, route_weights, ffn_gain, gate_master, up_master, down_master):
    n = lax.axis_size("fs")
    count, index = (lax.axis_size("grp"), lax.axis_index("grp"))
    experts, rows, _ = gate_master.shape
    per_device = experts // n
    groups = experts // GROUP_SIZE
    members = n // groups
    capacity = tokens.shape[0] // (2 * groups)
    size = per_device * rows // count

    def swap(x):
        return lax.all_to_all(x, "fs", split_axis=0, concat_axis=0, tiled=True)

    def neighbour(x, k):
        pairs = [(i, i - i % members + (i + k) % members) for i in range(n)]
        return lax.ppermute(x, "fs", pairs)

    packed = pack_first(
        tokens, route_ids, ffn_gain[None, :], by_target(gate_master, n), n, count, groups
    )
    packed = swap(packed)
    gate, near, named = jnp.split(packed, [size, packed.shape[1] - META], axis=1)
    near = [near] + [neighbour(near, k) for k in range(1, members)]
    if size < rows:
        gain = lax.dynamic_slice_in_dim(ffn_gain, index * size % rows, size)
    else:
        gain = jnp.concatenate([ffn_gain] * (size // rows))
    up = swap((share(up_master, index, count, n) * gain[None, :, None]).astype(BF))
    chosen = select_rows(near, named, per_device, capacity)
    down = swap(share(down_master, index, count, n).astype(BF))
    gate = ring(gate, "grp")
    up = ring(up, "grp")
    down = ring(down, "grp")
    gate_serve = assemble(gate, index, count, per_device)
    up_serve = assemble(up, index, count, per_device)
    down_serve = assemble(down, index, count, per_device)
    gates = one_by_one(gate, gate_serve, index, count, per_device)
    ups = one_by_one(up, up_serve, index, count, per_device)
    downs = one_by_one(down, down_serve, index, count, per_device)
    out = None
    for k in range(per_device):
        blocks = gather_tp(chosen[k], k % 2)
        hidden = first_matmuls(blocks, gates[k], ups[k], capacity)
        hidden = gather_tp(hidden, k % 2)
        out = second_matmul(hidden, downs[k], n, k, per_device, out)
    out = swap(out)
    mixed = combine(out.reshape(-1, out.shape[-1]), route_ids, route_weights, capacity)
    return (gate_serve, up_serve, down_serve, mixed)


def solution(mesh):
    grp, fs, tp = (mesh.shape["grp"], mesh.shape["fs"], mesh.shape["tp"])
    split = Mesh(mesh.devices.reshape(grp, fs, tp // 2, 2), ("grp", "fs", *TP))
    in_specs = (
        P(("grp", "fs"), None),
        P(("grp", "fs"), None),
        P(("grp", "fs"), None),
        P("fs"),
        P(None, "fs", TP),
        P(None, "fs", TP),
        P(None, "fs", TP),
    )
    out_specs = (
        P(("grp", "fs"), None, TP),
        P(("grp", "fs"), None, TP),
        P(("grp", "fs"), None, TP),
        P(("grp", "fs"), TP),
    )
    return jax.shard_map(
        on_device, mesh=split, in_specs=in_specs, out_specs=out_specs, check_vma=False
    )
```

time: 232 us -> 247 us (1.065)
  blocking collectives: 40.9 us -> 0 us
  starting transfers between devices: 52.9 us -> 83.6 us
  waiting for transfers between devices: 97.5 us -> 125 us
  local copies, waits for them, and re-layouts: 19.5 us -> 10.5 us
  Pallas kernels: 14.7 us -> 21.9 us
    all_to_all x1 -> x0, blocking collectives: 40.9 us -> none  [swap(): return lax.all_to_all(x, 'fs', split_axis=0, concat_axis=0, tiled=True)]
    ppermute x0 -> x3, waiting for transfers between devices: none -> 26.7 us  [neighbour(): return lax.ppermute(x, 'fs', pairs)]
    ppermute x21 -> x31, starting transfers between devices: 14.3 us -> 27.6 us  [shift(): return lax.ppermute(x, axis, [(i, (i + k) % n) for i in range(n)])]
    all_to_all x3 -> x4, starting transfers between devices: 38.7 us -> 50.5 us  [swap(): return lax.all_to_all(x, 'fs', split_axis=0, concat_axis=0, tiled=True)]
    all_to_all x3 -> x4, waiting for transfers between devices: 74.4 us -> 80.3 us  [swap(): return lax.all_to_all(x, 'fs', split_axis=0, concat_axis=0, tiled=True)]
    ppermute x0 -> x3, starting transfers between devices: none -> 5.53 us  [neighbour(): return lax.ppermute(x, 'fs', pairs)]
    ppermute x21 -> x31, waiting for transfers between devices: 23.1 us -> 17.9 us  [shift(): return lax.ppermute(x, axis, [(i, (i + k) % n) for i in range(n)])]
    pallas_call x2 -> x4, Pallas kernels: 8.29 us -> 12.9 us  [the longest x2 7.18 us: first_matmuls(): pl.pallas_call(body, out_shape=shape((rows, cols)), in_specs=[ANY] * (cou...]
  transfers between devices with their start and end apart: 24 -> 38, of which waited for: 8 -> 13; matrix products, arithmetic and copies ran while one was open for 7% -> 4% of each run, Pallas kernels for 4% -> 7%
where the time goes in v2:
time: 247 us; the launch traced here: 244 us
  waiting for transfers between devices  125 us (51%)
  starting transfers between devices  83.6 us (34%)
  Pallas kernels  21.9 us (9%)
  local copies, waits for them, and re-layouts  10.5 us (4%)
    all_to_all x4, waiting for transfers between devices, swap(): return lax.all_to_all(x, 'fs', split_axis=0, concat_axis=0, tiled=True)  80.3 us
    all_to_all x4, starting transfers between devices, swap(): return lax.all_to_all(x, 'fs', split_axis=0, concat_axis=0, tiled=True)  50.5 us
    ppermute x31, starting transfers between devices, shift(): return lax.ppermute(x, axis, [(i, (i + k) % n) for i in range(n)])  27.6 us
    ppermute x3, waiting for transfers between devices, neighbour(): return lax.ppermute(x, 'fs', pairs)  26.7 us
    ppermute x31, waiting for transfers between devices, shift(): return lax.ppermute(x, axis, [(i, (i + k) % n) for i in range(n)])  17.9 us
    pallas_call x2, Pallas kernels, first_matmuls(): pl.pallas_call(body, out_shape=shape((rows, cols)), in_specs=[ANY] * (cou...  7.18 us
    pallas_call x2, Pallas kernels, second_matmul(): pl.pallas_call(body, out_shape=shape((n, per_device, capacity, cols)), in...  6.55 us
    dynamic_update_slice x6, local copies, waits for them, and re-layouts, assemble(): buffer = lax.dynamic_update_slice(buffer, piece[None], (at, 0, 0, 0))  6.49 us
  transfers between devices with their start and end apart: 38, of which 13 were waited for; matrix products, arithmetic and copies ran while one was open for 4% of the time, Pallas kernels for 7%

profile of v2, /device:TPU:34, one launch (start us, length us, event | category | flops | bytes accessed | tf_op | source)
XLA Modules:
  0.0 244.5 jit_solution(13315936515095902239)
XLA Ops:
  0.7 2.4 multiply_convert_fusion
  3.0 24.0 %all-to-all-start.1 = ((bf16[16,128,128]{2,1,0:T(8,128)(2,1)}), bf16[16,128,128]{2,1,0:T(8,128)(2,1)S(1)}, u32[]{:S(2)}, u32[]{:S(2)}) async-start(bf16[16,128,128]{2,1,0:T(8,128)(2,1)} %multiply_convert_fusion), calls=%async_computation.1 | async-start | bytes 1048576 | tf_op jit(solution)/shard_map/all_to_all | solution.py:347
  27.0 3.4 %shard_map.102 = bf16[16,168,128]{2,1,0:T(8,128)(2,1)} custom-call(bf16[256,2048]{1,0:T(8,128)(2,1)} %tok_ref.1, s32[2,256]{1,0:T(2,128)} %bitcast.35, f32[1,128]{1,0:T(1,128)} %bitcast.38, f32[16,256,128]{2,1,0:T(8,128)} %bitcast.30), custom_call_target="tpu_custom_call" | custom-call | tf_op jit(solution)/shard_map/pallas_call | solution.py:114
  30.4 25.5 %all-to-all-done.1 = bf16[16,128,128]{2,1,0:T(8,128)(2,1)S(1)} async-done(((bf16[16,128,128]{2,1,0:T(8,128)(2,1)}), bf16[16,128,128]{2,1,0:T(8,128)(2,1)S(1)}, u32[]{:S(2)}, u32[]{:S(2)}) %all-to-all-start.1) | async-done | bytes 524320 | tf_op jit(solution)/shard_map/all_to_all | solution.py:347
  55.9 6.6 %all-to-all-start = ((bf16[16,168,128]{2,1,0:T(8,128)(2,1)}), bf16[16,168,128]{2,1,0:T(8,128)(2,1)S(1)}, u32[]{:S(2)}, u32[]{:S(2)}) async-start(bf16[16,168,128]{2,1,0:T(8,128)(2,1)} %shard_map.102), calls=%async_computation | async-start | bytes 1376256 | tf_op jit(solution)/shard_map/all_to_all | solution.py:347
  63.4 33.9 %all-to-all-done = bf16[16,168,128]{2,1,0:T(8,128)(2,1)S(1)} async-done(((bf16[16,168,128]{2,1,0:T(8,128)(2,1)}), bf16[16,168,128]{2,1,0:T(8,128)(2,1)S(1)}, u32[]{:S(2)}, u32[]{:S(2)}) %all-to-all-start) | async-done | bytes 688160 | tf_op jit(solution)/shard_map/all_to_all | solution.py:347
  97.3 7.7 %all-to-all-start.2 = ((bf16[16,64,256]{2,1,0:T(8,128)(2,1)}), bf16[16,64,256]{2,1,0:T(8,128)(2,1)}, u32[]{:S(2)}, u32[]{:S(2)}) async-start(bf16[16,64,256]{2,1,0:T(8,128)(2,1)} %dynamic-slice_convert_fusion), calls=%async_computation.2 | async-start | bytes 1048576 | tf_op jit(solution)/shard_map/all_to_all | solution.py:347
  109.0 2.4 collective-permute-start.4
  113.4 21.9 %collective-permute-done.3.refs_1_ = bf16[16,32,128]{2,1,0:T(8,128)(2,1)S(1)} collective-permute-done((bf16[16,32,128]{2,1,0:T(8,128)(2,1)S(1)}, bf16[16,32,128]{2,1,0:T(8,128)(2,1)S(1)}, u32[]{:S(2)}, u32[]{:S(2)}) %collective-permute-start.3) | collective-permute-done | bytes 131104 | tf_op jit(solution)/shard_map/ppermute | solution.py:351
  135.3 4.8 %collective-permute-done.4.refs_2_ = bf16[16,32,128]{2,1,0:T(8,128)(2,1)S(1)} collective-permute-done((bf16[16,32,128]{2,1,0:T(8,128)(2,1)S(1)}, bf16[16,32,128]{2,1,0:T(8,128)(2,1)S(1)}, u32[]{:S(2)}, u32[]{:S(2)}) %collective-permute-start.4) | collective-permute-done | bytes 131104 | tf_op jit(solution)/shard_map/ppermute | solution.py:351
  147.2 2.9 %collective-permute-done.20.refs_1_ = bf16[16,64,128]{2,1,0:T(8,128)(2,1)S(1)} collective-permute-done((bf16[16,64,128]{2,1,0:T(8,128)(2,1)}, bf16[16,64,128]{2,1,0:T(8,128)(2,1)S(1)}, u32[]{:S(2)}, u32[]{:S(2)}) %collective-permute-start.20) | collective-permute-done | bytes 262176 | tf_op jit(solution)/shard_map/ppermute | solution.py:23
  150.0 2.4 collective-permute-start.22
  157.0 2.4 collective-permute-start.8
  162.1 3.9 %collective-permute-done.8.refs_3_ = bf16[16,64,128]{2,1,0:T(8,128)(2,1)} collective-permute-done((bf16[16,64,128]{2,1,0:T(8,128)(2,1)}, bf16[16,64,128]{2,1,0:T(8,128)(2,1)}, u32[]{:S(2)}, u32[]{:S(2)}) %collective-permute-start.8) | collective-permute-done | bytes 262176 | tf_op jit(solution)/shard_map/ppermute | solution.py:23
  166.7 3.6 %shard_map.105.refs_0_ = bf16[512,128]{1,0:T(8,128)(2,1)} custom-call(bf16[16,64,128]{2,1,0:T(8,128)(2,1)} %get-tuple-element.7.refs_0_, bf16[16,64,128]{2,1,0:T(8,128)(2,1)} %copy-done.7, bf16[16,64,128]{2,1,0:T(8,128)(2,1)} %copy-done.8, bf16[16,64,128]{2,1,0:T(8,128)(2,1)} %copy-done.10, bf16[16,64,128]{2,1,0:T(8,128)(2,1)} %copy-done.9, ...), custom_call_target="tpu_custom_call" | custom-call | tf_op jit(solution)/shard_map/pallas_call | solution.py:221
  174.6 3.6 %shard_map.104.refs_0_ = bf16[512,128]{1,0:T(8,128)(2,1)} custom-call(bf16[16,64,128]{2,1,0:T(8,128)(2,1)} %get-tuple-element.6.refs_0_, bf16[16,64,128]{2,1,0:T(8,128)(2,1)} %collective-permute-done.6.refs_1_, bf16[16,64,128]{2,1,0:T(8,128)(2,1)} %collective-permute-done.7.refs_2_, bf16[16,64,128]{2,1,0:T(8,128)(2,1)} %collective-permute-done.8.refs_3_, ...), custom_call_target="tpu_custom_call" | custom-call | tf_op jit(solution)/shard_map/pallas_call | solution.py:221
  178.2 2.7 %collective-permute-start.14 = (bf16[512,128]{1,0:T(8,128)(2,1)}, bf16[512,128]{1,0:T(8,128)(2,1)S(1)}, u32[]{:S(2)}, u32[]{:S(2)}) collective-permute-start(bf16[512,128]{1,0:T(8,128)(2,1)} %shard_map.104.refs_0_), channel_id=1, source_target_pairs={{0,6},{2,0},{4,2},{6,4},{1,7},{3,1},{5,3},{7,5},{8,14},{10,8},{12,... | collective-permute-start | bytes 393224 | tf_op jit(solution)/shard_map/ppermute | solution.py:23
  184.8 2.8 %collective-permute-done.13.refs_1_ = bf16[512,128]{1,0:T(8,128)(2,1)S(1)} collective-permute-done((bf16[512,128]{1,0:T(8,128)(2,1)}, bf16[512,128]{1,0:T(8,128)(2,1)S(1)}, u32[]{:S(2)}, u32[]{:S(2)}) %collective-permute-start.13) | collective-permute-done | bytes 131104 | tf_op jit(solution)/shard_map/ppermute | solution.py:23
  187.6 3.1 %collective-permute-start.15 = (bf16[512,128]{1,0:T(8,128)(2,1)S(1)}, bf16[512,128]{1,0:T(8,128)(2,1)}, u32[]{:S(2)}, u32[]{:S(2)}) collective-permute-start(bf16[512,128]{1,0:T(8,128)(2,1)S(1)} %collective-permute-done.14.refs_2_), channel_id=1, source_target_pairs={{0,6},{2,0},{4,2},{6,4},{1,7},{3,1},{5,3},{7,5},{8,14},{10,8},{12,... | collective-permute-start | bytes 393224 | tf_op jit(solution)/shard_map/ppermute | solution.py:23
  193.9 3.3 %shard_map.106.refs_9_ = bf16[16,2,32,256]{3,2,1,0:T(8,128)(2,1)} custom-call(bf16[512,128]{1,0:T(8,128)(2,1)} %shard_map.105.refs_0_, bf16[512,128]{1,0:T(8,128)(2,1)} %copy-done.14, bf16[512,128]{1,0:T(8,128)(2,1)} %copy-done.15, bf16[512,128]{1,0:T(8,128)(2,1)} %copy-done.19, bf16[512,128]{1,0:T(8,128)(2,1)} %copy-done.17, bf16[512,128]{1,0:T(8,128)(2,1)} %copy-done.20, ...), custom_call_target="tpu_custom_call" | custom-call | tf_op jit(solution)/shard_map/pallas_call | solution.py:261
  197.3 3.3 %shard_map.107 = bf16[16,2,32,256]{3,2,1,0:T(8,128)(2,1)} custom-call(bf16[512,128]{1,0:T(8,128)(2,1)} %shard_map.104.refs_0_, bf16[512,128]{1,0:T(8,128)(2,1)} %copy-done.18, bf16[512,128]{1,0:T(8,128)(2,1)} %copy-done.16, bf16[512,128]{1,0:T(8,128)(2,1)} %collective-permute-done.15.refs_3_, ...), custom_call_target="tpu_custom_call", output_to_operand_aliasing={{}: (9, {})} | custom-call | tf_op jit(solution)/shard_map/pallas_call | solution.py:261
  200.6 12.2 %all-to-all-start.3 = ((bf16[16,2,32,256]{3,2,1,0:T(8,128)(2,1)}), bf16[16,2,32,256]{3,2,1,0:T(8,128)(2,1)}, u32[]{:S(2)}, u32[]{:S(2)}) async-start(bf16[16,2,32,256]{3,2,1,0:T(8,128)(2,1)} %shard_map.107), calls=%async_computation.3 | async-start | bytes 1048576 | tf_op jit(solution)/shard_map/all_to_all | solution.py:347
  221.1 20.9 %all-to-all-done.3 = bf16[16,2,32,256]{3,2,1,0:T(8,128)(2,1)} async-done(((bf16[16,2,32,256]{3,2,1,0:T(8,128)(2,1)}), bf16[16,2,32,256]{3,2,1,0:T(8,128)(2,1)}, u32[]{:S(2)}, u32[]{:S(2)}) %all-to-all-start.3) | async-done | bytes 524320 | tf_op jit(solution)/shard_map/all_to_all | solution.py:347
  242.0 2.5 %shard_map.108 = bf16[256,256]{1,0:T(8,128)(2,1)} custom-call(bf16[1024,256]{1,0:T(8,128)(2,1)} %bitcast.20.ret_ref, s32[2,256]{1,0:T(2,128)} %bitcast.36, f32[2,256]{1,0:T(2,128)} %bitcast.37), custom_call_target="tpu_custom_call" | custom-call | tf_op jit(solution)/shard_map/pallas_call | solution.py:289
  (123 shorter events, 41.2 us)
Async XLA Ops:
  3.0 52.9 %all-to-all-start.1 = ((bf16[16,128,128]{2,1,0:T(8,128)(2,1)}), bf16[16,128,128]{2,1,0:T(8,128)(2,1)S(1)}, u32[]{:S(2)}, u32[]{:S(2)}) async-start(bf16[16,128,128]{2,1,0:T(8,128)(2,1)} %multiply_convert_fusion), calls=%async_computation.1 | async-start | bytes 1048576 | tf_op jit(solution)/shard_map/all_to_all | solution.py:347
  55.9 41.4 %all-to-all-start = ((bf16[16,168,128]{2,1,0:T(8,128)(2,1)}), bf16[16,168,128]{2,1,0:T(8,128)(2,1)S(1)}, u32[]{:S(2)}, u32[]{:S(2)}) async-start(bf16[16,168,128]{2,1,0:T(8,128)(2,1)} %shard_map.102), calls=%async_computation | async-start | bytes 1376256 | tf_op jit(solution)/shard_map/all_to_all | solution.py:347
  97.3 73.1 %all-to-all-start.2 = ((bf16[16,64,256]{2,1,0:T(8,128)(2,1)}), bf16[16,64,256]{2,1,0:T(8,128)(2,1)}, u32[]{:S(2)}, u32[]{:S(2)}) async-start(bf16[16,64,256]{2,1,0:T(8,128)(2,1)} %dynamic-slice_convert_fusion), calls=%async_computation.2 | async-start | bytes 1048576 | tf_op jit(solution)/shard_map/all_to_all | solution.py:347
  105.0 41.8 %collective-permute-start.1 = (bf16[16,128,128]{2,1,0:T(8,128)(2,1)S(1)}, bf16[16,128,128]{2,1,0:T(8,128)(2,1)}, u32[]{:S(2)}, u32[]{:S(2)}) collective-permute-start(bf16[16,128,128]{2,1,0:T(8,128)(2,1)S(1)} %all-to-all-done.1), channel_id=1, source_target_pairs={{0,128},{128,0},{1,129},{129,1},{2,130},{130,2},{3,131},{131,3},{4... | collective-permute-start | bytes 1572872 | tf_op jit(solution)/shard_map/ppermute | solution.py:23
  107.3 28.1 %collective-permute-start.3 = (bf16[16,32,128]{2,1,0:T(8,128)(2,1)S(1)}, bf16[16,32,128]{2,1,0:T(8,128)(2,1)S(1)}, u32[]{:S(2)}, u32[]{:S(2)}) collective-permute-start(bf16[16,32,128]{2,1,0:T(8,128)(2,1)S(1)} %split.13.refs_0_), channel_id=1, source_target_pairs={{0,8},{8,16},{16,24},{24,0},{32,40},{40,48},{48,56},{56,32},{64,72... | collective-permute-start | bytes 393224 | tf_op jit(solution)/shard_map/ppermute | solution.py:351
  109.0 31.1 %collective-permute-start.4 = (bf16[16,32,128]{2,1,0:T(8,128)(2,1)S(1)}, bf16[16,32,128]{2,1,0:T(8,128)(2,1)S(1)}, u32[]{:S(2)}, u32[]{:S(2)}) collective-permute-start(bf16[16,32,128]{2,1,0:T(8,128)(2,1)S(1)} %split.13.refs_0_), channel_id=1, source_target_pairs={{0,16},{8,24},{16,0},{24,8},{32,48},{40,56},{48,32},{56,40},{64,80... | collective-permute-start | bytes 393224 | tf_op jit(solution)/shard_map/ppermute | solution.py:351
  111.3 29.4 %collective-permute-start.5 = (bf16[16,32,128]{2,1,0:T(8,128)(2,1)S(1)}, bf16[16,32,128]{2,1,0:T(8,128)(2,1)}, u32[]{:S(2)}, u32[]{:S(2)}) collective-permute-start(bf16[16,32,128]{2,1,0:T(8,128)(2,1)S(1)} %split.13.refs_0_), channel_id=1, source_target_pairs={{0,24},{8,0},{16,8},{24,16},{32,56},{40,32},{48,40},{56,48},{64,88... | collective-permute-start | bytes 393224 | tf_op jit(solution)/shard_map/ppermute | solution.py:351
  144.7 9.3 %collective-permute-start.21 = (bf16[16,64,128]{2,1,0:T(8,128)(2,1)}, bf16[16,64,128]{2,1,0:T(8,128)(2,1)S(1)}, u32[]{:S(2)}, u32[]{:S(2)}) collective-permute-start(bf16[16,64,128]{2,1,0:T(8,128)(2,1)} %get-tuple-element.7.refs_0_), channel_id=1, source_target_pairs={{0,6},{2,0},{4,2},{6,4},{1,7},{3,1},{5,3},{7,5},{8,14},{10,8},{12,... | collective-permute-start | bytes 786440 | tf_op jit(solution)/shard_map/ppermute | solution.py:23
  145.1 8.9 %collective-permute-start.23 = (bf16[16,64,128]{2,1,0:T(8,128)(2,1)}, bf16[16,64,128]{2,1,0:T(8,128)(2,1)S(1)}, u32[]{:S(2)}, u32[]{:S(2)}) collective-permute-start(bf16[16,64,128]{2,1,0:T(8,128)(2,1)} %get-tuple-element.7.refs_0_), channel_id=1, source_target_pairs={{0,1},{1,0},{2,3},{3,2},{4,5},{5,4},{6,7},{7,6},{8,9},{9,8},{10,11... | collective-permute-start | bytes 786440 | tf_op jit(solution)/shard_map/ppermute | solution.py:23
  145.1 11.8 %collective-permute-start.7 = (bf16[16,64,128]{2,1,0:T(8,128)(2,1)}, bf16[16,64,128]{2,1,0:T(8,128)(2,1)}, u32[]{:S(2)}, u32[]{:S(2)}) collective-permute-start(bf16[16,64,128]{2,1,0:T(8,128)(2,1)} %get-tuple-element.6.refs_0_), channel_id=1, source_target_pairs={{0,6},{2,0},{4,2},{6,4},{1,7},{3,1},{5,3},{7,5},{8,14},{10,8},{12,... | collective-permute-start | bytes 786440 | tf_op jit(solution)/shard_map/ppermute | solution.py:23
  146.8 10.2 %collective-permute-start.6 = (bf16[16,64,128]{2,1,0:T(8,128)(2,1)}, bf16[16,64,128]{2,1,0:T(8,128)(2,1)}, u32[]{:S(2)}, u32[]{:S(2)}) collective-permute-start(bf16[16,64,128]{2,1,0:T(8,128)(2,1)} %get-tuple-element.6.refs_0_), channel_id=1, source_target_pairs={{0,2},{2,4},{4,6},{6,0},{1,3},{3,5},{5,7},{7,1},{8,10},{10,12},{12... | collective-permute-start | bytes 786440 | tf_op jit(solution)/shard_map/ppermute | solution.py:23
  150.0 11.2 %collective-permute-start.22 = (bf16[16,64,128]{2,1,0:T(8,128)(2,1)S(1)}, bf16[16,64,128]{2,1,0:T(8,128)(2,1)S(1)}, u32[]{:S(2)}, u32[]{:S(2)}) collective-permute-start(bf16[16,64,128]{2,1,0:T(8,128)(2,1)S(1)} %collective-permute-done.20.refs_1_), channel_id=1, source_target_pairs={{0,2},{2,4},{4,6},{6,0},{1,3},{3,5},{5,7},{7,1},{8,10},{10,12},{12... | collective-permute-start | bytes 786440 | tf_op jit(solution)/shard_map/ppermute | solution.py:23
  154.1 18.5 %collective-permute-start = (bf16[16,128,128]{2,1,0:T(8,128)(2,1)S(1)}, bf16[16,128,128]{2,1,0:T(8,128)(2,1)}, u32[]{:S(2)}, u32[]{:S(2)}) collective-permute-start(bf16[16,128,128]{2,1,0:T(8,128)(2,1)S(1)} %split.12), channel_id=1, source_target_pairs={{0,128},{128,0},{1,129},{129,1},{2,130},{130,2},{3,131},{131,3},{4... | collective-permute-start | bytes 1572872 | tf_op jit(solution)/shard_map/ppermute | solution.py:23
  157.0 9.0 %collective-permute-start.8 = (bf16[16,64,128]{2,1,0:T(8,128)(2,1)}, bf16[16,64,128]{2,1,0:T(8,128)(2,1)}, u32[]{:S(2)}, u32[]{:S(2)}) collective-permute-start(bf16[16,64,128]{2,1,0:T(8,128)(2,1)} %collective-permute-done.7.refs_2_), channel_id=1, source_target_pairs={{0,6},{2,0},{4,2},{6,4},{1,7},{3,1},{5,3},{7,5},{8,14},{10,8},{12,... | collective-permute-start | bytes 786440 | tf_op jit(solution)/shard_map/ppermute | solution.py:23
  161.3 9.1 %collective-permute-start.9 = (bf16[16,64,128]{2,1,0:T(8,128)(2,1)}, bf16[16,64,128]{2,1,0:T(8,128)(2,1)}, u32[]{:S(2)}, u32[]{:S(2)}) collective-permute-start(bf16[16,64,128]{2,1,0:T(8,128)(2,1)} %get-tuple-element.6.refs_0_), channel_id=1, source_target_pairs={{0,1},{1,0},{2,3},{3,2},{4,5},{5,4},{6,7},{7,6},{8,9},{9,8},{10,11... | collective-permute-start | bytes 786440 | tf_op jit(solution)/shard_map/ppermute | solution.py:23
  161.9 12.1 %collective-permute-start.11 = (bf16[16,64,128]{2,1,0:T(8,128)(2,1)}, bf16[16,64,128]{2,1,0:T(8,128)(2,1)}, u32[]{:S(2)}, u32[]{:S(2)}) collective-permute-start(bf16[16,64,128]{2,1,0:T(8,128)(2,1)} %collective-permute-done.7.refs_2_), channel_id=1, source_target_pairs={{0,1},{1,0},{2,3},{3,2},{4,5},{5,4},{6,7},{7,6},{8,9},{9,8},{10,11... | collective-permute-start | bytes 786440 | tf_op jit(solution)/shard_map/ppermute | solution.py:23
  166.0 8.6 %collective-permute-start.10 = (bf16[16,64,128]{2,1,0:T(8,128)(2,1)}, bf16[16,64,128]{2,1,0:T(8,128)(2,1)}, u32[]{:S(2)}, u32[]{:S(2)}) collective-permute-start(bf16[16,64,128]{2,1,0:T(8,128)(2,1)} %collective-permute-done.6.refs_1_), channel_id=1, source_target_pairs={{0,1},{1,0},{2,3},{3,2},{4,5},{5,4},{6,7},{7,6},{8,9},{9,8},{10,11... | collective-permute-start | bytes 786440 | tf_op jit(solution)/shard_map/ppermute | solution.py:23
  166.0 8.6 %collective-permute-start.12 = (bf16[16,64,128]{2,1,0:T(8,128)(2,1)}, bf16[16,64,128]{2,1,0:T(8,128)(2,1)}, u32[]{:S(2)}, u32[]{:S(2)}) collective-permute-start(bf16[16,64,128]{2,1,0:T(8,128)(2,1)} %collective-permute-done.8.refs_3_), channel_id=1, source_target_pairs={{0,1},{1,0},{2,3},{3,2},{4,5},{5,4},{6,7},{7,6},{8,9},{9,8},{10,11... | collective-permute-start | bytes 786440 | tf_op jit(solution)/shard_map/ppermute | solution.py:23
  170.4 26.8 %collective-permute-start.2 = (bf16[16,64,256]{2,1,0:T(8,128)(2,1)}, bf16[16,64,256]{2,1,0:T(8,128)(2,1)}, u32[]{:S(2)}, u32[]{:S(2)}) collective-permute-start(bf16[16,64,256]{2,1,0:T(8,128)(2,1)} %all-to-all-done.2), channel_id=1, source_target_pairs={{0,128},{128,0},{1,129},{129,1},{2,130},{130,2},{3,131},{131,3},{4... | collective-permute-start | bytes 1572872 | tf_op jit(solution)/shard_map/ppermute | solution.py:23
  172.6 8.4 %collective-permute-start.27 = (bf16[512,128]{1,0:T(8,128)(2,1)}, bf16[512,128]{1,0:T(8,128)(2,1)S(1)}, u32[]{:S(2)}, u32[]{:S(2)}) collective-permute-start(bf16[512,128]{1,0:T(8,128)(2,1)} %shard_map.105.refs_0_), channel_id=1, source_target_pairs={{0,2},{2,4},{4,6},{6,0},{1,3},{3,5},{5,7},{7,1},{8,10},{10,12},{12... | collective-permute-start | bytes 393224 | tf_op jit(solution)/shard_map/ppermute | solution.py:23
  174.6 7.8 %collective-permute-start.30 = (bf16[512,128]{1,0:T(8,128)(2,1)}, bf16[512,128]{1,0:T(8,128)(2,1)S(1)}, u32[]{:S(2)}, u32[]{:S(2)}) collective-permute-start(bf16[512,128]{1,0:T(8,128)(2,1)} %shard_map.105.refs_0_), channel_id=1, source_target_pairs={{0,1},{1,0},{2,3},{3,2},{4,5},{5,4},{6,7},{7,6},{8,9},{9,8},{10,11... | collective-permute-start | bytes 393224 | tf_op jit(solution)/shard_map/ppermute | solution.py:23
  181.0 9.7 %collective-permute-start.29 = (bf16[512,128]{1,0:T(8,128)(2,1)S(1)}, bf16[512,128]{1,0:T(8,128)(2,1)S(1)}, u32[]{:S(2)}, u32[]{:S(2)}) collective-permute-start(bf16[512,128]{1,0:T(8,128)(2,1)S(1)} %collective-permute-done.27.refs_1_), channel_id=1, source_target_pairs={{0,2},{2,4},{4,6},{6,0},{1,3},{3,5},{5,7},{7,1},{8,10},{10,12},{12... | collective-permute-start | bytes 393224 | tf_op jit(solution)/shard_map/ppermute | solution.py:23
  182.5 8.2 %collective-permute-start.31 = (bf16[512,128]{1,0:T(8,128)(2,1)S(1)}, bf16[512,128]{1,0:T(8,128)(2,1)S(1)}, u32[]{:S(2)}, u32[]{:S(2)}) collective-permute-start(bf16[512,128]{1,0:T(8,128)(2,1)S(1)} %collective-permute-done.27.refs_1_), channel_id=1, source_target_pairs={{0,1},{1,0},{2,3},{3,2},{4,5},{5,4},{6,7},{7,6},{8,9},{9,8},{10,11... | collective-permute-start | bytes 393224 | tf_op jit(solution)/shard_map/ppermute | solution.py:23
  200.6 41.4 %all-to-all-start.3 = ((bf16[16,2,32,256]{3,2,1,0:T(8,128)(2,1)}), bf16[16,2,32,256]{3,2,1,0:T(8,128)(2,1)}, u32[]{:S(2)}, u32[]{:S(2)}) async-start(bf16[16,2,32,256]{3,2,1,0:T(8,128)(2,1)} %shard_map.107), calls=%async_computation.3 | async-start | bytes 1048576 | tf_op jit(solution)/shard_map/all_to_all | solution.py:347
  (39 other events, 398.7 us)

commit v3 on v2

--- a/solution.py
+++ b/solution.py
@@ -188,35 +188,28 @@
 def first_matmuls(blocks, gate, up, capacity):
     n, tall, _ = blocks[0].shape
     pieces = tall // capacity
+    width = pieces * LANES
     depth, cols = gate.shape
     rows = n * capacity
     count = len(blocks)
 
     def body(*refs):
-        ins, (gate_ref, up_ref, out_ref, in_buf, gate_buf, up_buf, acc_ref, sems) = (
-            refs[:count],
-            refs[count:],
-        )
-        waits = fetch(
-            [(gate_ref, gate_buf), (up_ref, up_buf)] + [(r, in_buf.at[i]) for i, r in enumerate(ins)], sems
-        )
-        waits[0]()
-        waits[1]()
+        ins, (gate_ref, up_ref, out_ref, in_buf, w_buf, sems) = (refs[:count], refs[count:])
+        pairs = []
         for i, tp in enumerate(places_of()):
-            d = pl.ds(pl.multiple_of(tp * (pieces * LANES), pieces * LANES), pieces * LANES)
-            w = jnp.concatenate([gate_buf[d, :], up_buf[d, :]], axis=1)
-            waits[2 + i]()
-            x = [
-                in_buf[i, :, p * capacity : (p + 1) * capacity, :].reshape(rows, LANES)
-                for p in range(pieces)
-            ]
-            more = dot(jnp.concatenate(x, axis=1), w)
-            if i == 0:
-                acc_ref[...] = more
-            else:
-                acc_ref[...] += more
-        g = acc_ref[:, :cols]
-        out_ref[...] = (g / (1.0 + jnp.exp(-g)) * acc_ref[:, cols:]).astype(BF)
+            d = pl.ds(pl.multiple_of(tp * width, width), width)
+            to = slice(i * width, (i + 1) * width)
+            pairs += [(gate_ref.at[d, :], w_buf.at[to, :cols]), (up_ref.at[d, :], w_buf.at[to, cols:])]
+            for p in range(pieces):
+                lanes = slice(i * width + p * LANES, i * width + (p + 1) * LANES)
+                pairs.append(
+                    (ins[i].at[:, p * capacity : (p + 1) * capacity, :], in_buf.at[:, :, lanes])
+                )
+        for wait in fetch(pairs, sems):
+            wait()
+        both = dot(in_buf[...].reshape(rows, depth), w_buf[...])
+        g = both[:, :cols]
+        out_ref[...] = (g / (1.0 + jnp.exp(-g)) * both[:, cols:]).astype(BF)
 
     return pl.pallas_call(
         body,
@@ -224,71 +217,66 @@
         in_specs=[ANY] * (count + 2),
         out_specs=VM,
         scratch_shapes=[
-            pltpu.VMEM((count, n, tall, LANES), BF),
-            pltpu.VMEM((depth, cols), BF),
-            pltpu.VMEM((depth, cols), BF),
-            pltpu.VMEM((rows, 2 * cols), F32),
-            pltpu.SemaphoreType.DMA((count + 2,)),
+            pltpu.VMEM((n, capacity, depth), BF),
+            pltpu.VMEM((depth, 2 * cols), BF),
+            pltpu.SemaphoreType.DMA((count * (2 + pieces),)),
         ],
     )(*blocks, gate, up)
 
 
-def second_matmul(blocks, down, n, k, per_device, before):
+def second_matmul(blocks, down, n):
     rows, width = blocks[0].shape
     depth, cols = down.shape
     capacity = rows // n
     count = len(blocks)
-    given = 0 if before is None else 1
 
     def body(*refs):
-        ins, rest = (refs[:count], refs[count : count + 1] + refs[count + 1 + given :])
-        down_ref, out_ref, in_buf, down_buf, acc_ref, row_ref, sems, sem = rest
-        waits = fetch([(down_ref, down_buf)] + [(r, in_buf.at[i]) for i, r in enumerate(ins)], sems)
-        waits[0]()
+        ins, (down_ref, out_ref, in_buf, down_buf, sems) = (refs[:count], refs[count:])
+        pairs = []
         for i, tp in enumerate(places_of()):
-            w = down_buf[pl.ds(pl.multiple_of(tp * width, width), width), :]
-            waits[1 + i]()
-            more = dot(in_buf[i], w)
-            if i == 0:
-                acc_ref[...] = more
-            else:
-                acc_ref[...] += more
-        row_ref[...] = acc_ref[...].reshape(n, capacity, cols).astype(BF)
-        copy = pltpu.make_async_copy(row_ref, out_ref.at[:, expert_at(k, per_device)], sem)
-        copy.start()
-        copy.wait()
-
-    return pl.pallas_call(
-        body,
-        out_shape=shape((n, per_device, capacity, cols)),
-        in_specs=[ANY] * (count + 1 + given),
-        out_specs=ANY,
-        input_output_aliases={count + 1: 0} if given else {},
+            d = pl.ds(pl.multiple_of(tp * width, width), width)
+            to = slice(i * width, (i + 1) * width)
+            pairs += [(down_ref.at[d, :], down_buf.at[to, :]), (ins[i], in_buf.at[:, to])]
+        for wait in fetch(pairs, sems):
+            wait()
+        out_ref[...] = dot(in_buf[...], down_buf[...]).reshape(n, capacity, cols).astype(BF)
+
+    return pl.pallas_call(
+        body,
+        out_shape=shape((n, capacity, cols)),
+        in_specs=[ANY] * (count + 1),
+        out_specs=VM,
         scratch_shapes=[
-            pltpu.VMEM((count, rows, width), BF),
+            pltpu.VMEM((rows, depth), BF),
             pltpu.VMEM((depth, cols), BF),
-            pltpu.VMEM((rows, cols), F32),
-            pltpu.VMEM((n, capacity, cols), BF),
-            pltpu.SemaphoreType.DMA((count + 1,)),
-            pltpu.SemaphoreType.DMA,
+            pltpu.SemaphoreType.DMA((2 * count,)),
         ],
-    )(*blocks, down, *([] if before is None else [before]))
-
-
-def combine(returned, route_ids, route_weights, capacity):
+    )(*blocks, down)
+
+
+def combine(returned, route_ids, route_weights, capacity, k, per_device, so_far):
     rows, cols = (route_ids.shape[0], returned.shape[1])
     slots = returned.shape[0]
-
-    def body(ret_ref, ids_ref, w_ref, out_ref):
-        total = jnp.zeros((rows, cols), F32)
+    last = k == per_device - 1
+
+    def body(ret_ref, ids_ref, w_ref, *refs):
+        out_ref = refs[-1]
+        total = jnp.zeros((rows, cols), F32) if so_far is None else refs[0][...]
         for r, slot in enumerate(slot_of(ids_ref, capacity)):
-            pick = (iota((rows, slots), 1) == slot).astype(BF)
+            expert, at = (slot // capacity, slot % capacity)
+            mine = expert % per_device == expert_at(k, per_device)
+            to = jnp.where(mine, expert // per_device * capacity + at, -1)
+            pick = jnp.where(iota((rows, slots), 1) == to, 1.0, 0.0).astype(BF)
             total = total + dot(pick, ret_ref[...]) * as_column(w_ref[r : r + 1, :])
-        out_ref[...] = total.astype(BF)
-
-    return pl.pallas_call(
-        body, out_shape=shape((rows, cols)), in_specs=[VM] * 3, out_specs=VM
-    )(returned, route_ids.T, route_weights.T)
+        out_ref[...] = total.astype(out_ref.dtype)
+
+    given = [] if so_far is None else [so_far]
+    return pl.pallas_call(
+        body,
+        out_shape=shape((rows, cols), BF if last else F32),
+        in_specs=[VM] * (3 + len(given)),
+        out_specs=VM,
+    )(returned, route_ids.T, route_weights.T, *given)
 
 
 def by_target(master, n):
@@ -372,14 +360,14 @@
     gates = one_by_one(gate, gate_serve, index, count, per_device)
     ups = one_by_one(up, up_serve, index, count, per_device)
     downs = one_by_one(down, down_serve, index, count, per_device)
-    out = None
+    mixed = None
     for k in range(per_device):
         blocks = gather_tp(chosen[k], k % 2)
         hidden = first_matmuls(blocks, gates[k], ups[k], capacity)
         hidden = gather_tp(hidden, k % 2)
-        out = second_matmul(hidden, downs[k], n, k, per_device, out)
-    out = swap(out)
-    mixed = combine(out.reshape(-1, out.shape[-1]), route_ids, route_weights, capacity)
+        out = second_matmul(hidden, downs[k], n)
+        out = swap(out).reshape(-1, out.shape[-1])
+        mixed = combine(out, route_ids, route_weights, capacity, k, per_device, mixed)
     return (gate_serve, up_serve, down_serve, mixed)
 
 
@@ -401,6 +389,4 @@
         P(("grp", "fs"), None, TP),
         P(("grp", "fs"), TP),
     )
-    return jax.shard_map(
-        on_device, mesh=split, in_specs=in_specs, out_specs=out_specs, check_vma=False
-    )
+    return jax.shard_map(on_device, mesh=split, in_specs=in_specs, out_specs=out_specs, check_vma=False)

time: 247 us -> 262 us (1.061)
  starting transfers between devices: 83.6 us -> 92.5 us
  local copies, waits for them, and re-layouts: 10.5 us -> 17 us
    all_to_all x4 -> x5, waiting for transfers between devices: 80.3 us -> 66.6 us  [swap(): return lax.all_to_all(x, 'fs', split_axis=0, concat_axis=0, tiled=True)]
    all_to_all x4 -> x5, starting transfers between devices: 50.5 us -> 62.6 us  [swap(): return lax.all_to_all(x, 'fs', split_axis=0, concat_axis=0, tiled=True)]
    ppermute x31, waiting for transfers between devices: 17.9 us -> 28.4 us  [shift(): return lax.ppermute(x, axis, [(i, (i + k) % n) for i in range(n)])]
    unnamed x50 -> x60, local copies, waits for them, and re-layouts: 0.88 us -> 5.4 us
    ppermute x31, starting transfers between devices: 27.6 us -> 24.3 us  [shift(): return lax.ppermute(x, axis, [(i, (i + k) % n) for i in range(n)])]
    pallas_call x3 -> x4, Pallas kernels: 9.03 us -> 10.9 us  [the longest x2 5.45 us: second_matmul(): pl.pallas_call(body, out_shape=shape((n, capacity, cols)), in_specs=[ANY]...]
  transfers between devices with their start and end apart: 38 -> 39, of which waited for: 13 -> 17; matrix products, arithmetic and copies ran while one was open for 4% -> 4% of each run, Pallas kernels for 7% -> 8%
where the time goes in v3:
time: 262 us; the launch traced here: 261 us
  waiting for transfers between devices  124 us (47%)
  starting transfers between devices  92.5 us (35%)
  Pallas kernels  23.8 us (9%)
  local copies, waits for them, and re-layouts  17 us (6%)
    all_to_all x5, waiting for transfers between devices, swap(): return lax.all_to_all(x, 'fs', split_axis=0, concat_axis=0, tiled=True)  66.6 us
    all_to_all x5, starting transfers between devices, swap(): return lax.all_to_all(x, 'fs', split_axis=0, concat_axis=0, tiled=True)  62.6 us
    ppermute x3, waiting for transfers between devices, neighbour(): return lax.ppermute(x, 'fs', pairs)  28.8 us
    ppermute x31, waiting for transfers between devices, shift(): return lax.ppermute(x, axis, [(i, (i + k) % n) for i in range(n)])  28.4 us
    ppermute x31, starting transfers between devices, shift(): return lax.ppermute(x, axis, [(i, (i + k) % n) for i in range(n)])  24.3 us
    dynamic_update_slice x6, local copies, waits for them, and re-layouts, assemble(): buffer = lax.dynamic_update_slice(buffer, piece[None], (at, 0, 0, 0))  7.66 us
    pallas_call x2, Pallas kernels, first_matmuls(): pl.pallas_call(body, out_shape=shape((rows, cols)), in_specs=[ANY] * (cou...  7.19 us
    ppermute x3, starting transfers between devices, neighbour(): return lax.ppermute(x, 'fs', pairs)  5.65 us
  transfers between devices with their start and end apart: 39, of which 17 were waited for; matrix products, arithmetic and copies ran while one was open for 4% of the time, Pallas kernels for 8%

profile of v3, /device:TPU:34, one launch (start us, length us, event | category | flops | bytes accessed | tf_op | source)
XLA Modules:
  0.0 260.5 jit_solution(8174884852035545801)
XLA Ops:
  3.0 24.0 %all-to-all-start.1 = ((bf16[16,128,128]{2,1,0:T(8,128)(2,1)}), bf16[16,128,128]{2,1,0:T(8,128)(2,1)S(1)}, u32[]{:S(2)}, u32[]{:S(2)}) async-start(bf16[16,128,128]{2,1,0:T(8,128)(2,1)} %multiply_convert_fusion), calls=%async_computation.1 | async-start | bytes 1048576 | tf_op jit(solution)/shard_map/all_to_all | solution.py:335
  27.0 3.4 %shard_map.102 = bf16[16,168,128]{2,1,0:T(8,128)(2,1)} custom-call(bf16[256,2048]{1,0:T(8,128)(2,1)} %tok_ref.1, s32[2,256]{1,0:T(2,128)} %bitcast.37, f32[1,128]{1,0:T(1,128)} %bitcast.42, f32[16,256,128]{2,1,0:T(8,128)} %bitcast.31), custom_call_target="tpu_custom_call" | custom-call | tf_op jit(solution)/shard_map/pallas_call | solution.py:114
  30.4 25.5 %all-to-all-done.1 = bf16[16,128,128]{2,1,0:T(8,128)(2,1)S(1)} async-done(((bf16[16,128,128]{2,1,0:T(8,128)(2,1)}), bf16[16,128,128]{2,1,0:T(8,128)(2,1)S(1)}, u32[]{:S(2)}, u32[]{:S(2)}) %all-to-all-start.1) | async-done | bytes 524320 | tf_op jit(solution)/shard_map/all_to_all | solution.py:335
  55.9 6.6 %all-to-all-start = ((bf16[16,168,128]{2,1,0:T(8,128)(2,1)}), bf16[16,168,128]{2,1,0:T(8,128)(2,1)S(1)}, u32[]{:S(2)}, u32[]{:S(2)}) async-start(bf16[16,168,128]{2,1,0:T(8,128)(2,1)} %shard_map.102), calls=%async_computation | async-start | bytes 1376256 | tf_op jit(solution)/shard_map/all_to_all | solution.py:335
  63.4 33.9 %all-to-all-done = bf16[16,168,128]{2,1,0:T(8,128)(2,1)S(1)} async-done(((bf16[16,168,128]{2,1,0:T(8,128)(2,1)}), bf16[16,168,128]{2,1,0:T(8,128)(2,1)S(1)}, u32[]{:S(2)}, u32[]{:S(2)}) %all-to-all-start) | async-done | bytes 688160 | tf_op jit(solution)/shard_map/all_to_all | solution.py:335
  97.3 7.7 %all-to-all-start.2 = ((bf16[16,64,256]{2,1,0:T(8,128)(2,1)}), bf16[16,64,256]{2,1,0:T(8,128)(2,1)}, u32[]{:S(2)}, u32[]{:S(2)}) async-start(bf16[16,64,256]{2,1,0:T(8,128)(2,1)} %dynamic-slice_convert_fusion), calls=%async_computation.2 | async-start | bytes 1048576 | tf_op jit(solution)/shard_map/all_to_all | solution.py:335
  111.3 24.0 %collective-permute-done.3.refs_1_ = bf16[16,32,128]{2,1,0:T(8,128)(2,1)S(1)} collective-permute-done((bf16[16,32,128]{2,1,0:T(8,128)(2,1)S(1)}, bf16[16,32,128]{2,1,0:T(8,128)(2,1)S(1)}, u32[]{:S(2)}, u32[]{:S(2)}) %collective-permute-start.3) | collective-permute-done | bytes 131104 | tf_op jit(solution)/shard_map/ppermute | solution.py:339
  135.3 4.8 %collective-permute-done.4.refs_2_ = bf16[16,32,128]{2,1,0:T(8,128)(2,1)S(1)} collective-permute-done((bf16[16,32,128]{2,1,0:T(8,128)(2,1)S(1)}, bf16[16,32,128]{2,1,0:T(8,128)(2,1)S(1)}, u32[]{:S(2)}, u32[]{:S(2)}) %collective-permute-start.4) | collective-permute-done | bytes 131104 | tf_op jit(solution)/shard_map/ppermute | solution.py:339
  145.1 5.1 %collective-permute-done.20.refs_1_ = bf16[16,64,128]{2,1,0:T(8,128)(2,1)S(1)} collective-permute-done((bf16[16,64,128]{2,1,0:T(8,128)(2,1)}, bf16[16,64,128]{2,1,0:T(8,128)(2,1)S(1)}, u32[]{:S(2)}, u32[]{:S(2)}) %collective-permute-start.20) | collective-permute-done | bytes 262176 | tf_op jit(solution)/shard_map/ppermute | solution.py:23
  152.6 4.0 %collective-permute-done.22.refs_3_ = bf16[16,64,128]{2,1,0:T(8,128)(2,1)S(1)} collective-permute-done((bf16[16,64,128]{2,1,0:T(8,128)(2,1)S(1)}, bf16[16,64,128]{2,1,0:T(8,128)(2,1)S(1)}, u32[]{:S(2)}, u32[]{:S(2)}) %collective-permute-start.22) | collective-permute-done | bytes 262176 | tf_op jit(solution)/shard_map/ppermute | solution.py:23
  163.1 3.6 %shard_map.106.refs_0_ = bf16[512,128]{1,0:T(8,128)(2,1)} custom-call(bf16[16,64,128]{2,1,0:T(8,128)(2,1)} %get-tuple-element.7.refs_0_, bf16[16,64,128]{2,1,0:T(8,128)(2,1)} %copy-done.8, bf16[16,64,128]{2,1,0:T(8,128)(2,1)} %copy-done.9, bf16[16,64,128]{2,1,0:T(8,128)(2,1)} %copy-done.10, bf16[16,64,128]{2,1,0:T(8,128)(2,1)} %copy-done.11, ...), custom_call_target="tpu_custom_call" | custom-call | tf_op jit(solution)/shard_map/pallas_call | solution.py:214
  168.8 3.5 %collective-permute-done.27.refs_1_ = bf16[512,128]{1,0:T(8,128)(2,1)S(1)} collective-permute-done((bf16[512,128]{1,0:T(8,128)(2,1)}, bf16[512,128]{1,0:T(8,128)(2,1)S(1)}, u32[]{:S(2)}, u32[]{:S(2)}) %collective-permute-start.27) | collective-permute-done | bytes 131104 | tf_op jit(solution)/shard_map/ppermute | solution.py:23
  173.7 4.3 %collective-permute-done.29.refs_3_ = bf16[512,128]{1,0:T(8,128)(2,1)} collective-permute-done((bf16[512,128]{1,0:T(8,128)(2,1)S(1)}, bf16[512,128]{1,0:T(8,128)(2,1)}, u32[]{:S(2)}, u32[]{:S(2)}) %collective-permute-start.29) | collective-permute-done | bytes 131104 | tf_op jit(solution)/shard_map/ppermute | solution.py:23
  178.0 3.3 %collective-permute-start.8 = (bf16[16,64,128]{2,1,0:T(8,128)(2,1)}, bf16[16,64,128]{2,1,0:T(8,128)(2,1)}, u32[]{:S(2)}, u32[]{:S(2)}) collective-permute-start(bf16[16,64,128]{2,1,0:T(8,128)(2,1)} %collective-permute-done.7.refs_2_), channel_id=1, source_target_pairs={{0,6},{2,0},{4,2},{6,4},{1,7},{3,1},{5,3},{7,5},{8,14},{10,8},{12,... | collective-permute-start | bytes 786440 | tf_op jit(solution)/shard_map/ppermute | solution.py:23
  183.7 2.7 %shard_map.107 = bf16[16,32,256]{2,1,0:T(8,128)(2,1)} custom-call(bf16[512,128]{1,0:T(8,128)(2,1)} %shard_map.106.refs_0_, bf16[512,128]{1,0:T(8,128)(2,1)} %copy-done.17, bf16[512,128]{1,0:T(8,128)(2,1)} %copy-done.18, bf16[512,128]{1,0:T(8,128)(2,1)} %collective-permute-done.29.refs_3_, bf16[512,128]{1,0:T(8,128)(2,1)} %copy-done.19, ...), custom_call_target="tpu_custom_call" | custom-call | tf_op jit(solution)/shard_map/pallas_call | solution.py:244
  186.5 12.4 %all-to-all-start.4 = ((bf16[16,32,256]{2,1,0:T(8,128)(2,1)}), bf16[16,32,256]{2,1,0:T(8,128)(2,1)}, u32[]{:S(2)}, u32[]{:S(2)}) async-start(bf16[16,32,256]{2,1,0:T(8,128)(2,1)} %shard_map.107), calls=%async_computation.4 | async-start | bytes 524288 | tf_op jit(solution)/shard_map/all_to_all | solution.py:335
  202.2 3.6 %shard_map.104.refs_0_ = bf16[512,128]{1,0:T(8,128)(2,1)} custom-call(bf16[16,64,128]{2,1,0:T(8,128)(2,1)} %get-tuple-element.6.refs_0_, bf16[16,64,128]{2,1,0:T(8,128)(2,1)} %collective-permute-done.6.refs_1_, bf16[16,64,128]{2,1,0:T(8,128)(2,1)} %collective-permute-done.7.refs_2_, bf16[16,64,128]{2,1,0:T(8,128)(2,1)} %collective-permute-done.8.refs_3_, ...), custom_call_target="tpu_custom_call" | custom-call | tf_op jit(solution)/shard_map/pallas_call | solution.py:214
  205.8 3.6 %collective-permute-start.14 = (bf16[512,128]{1,0:T(8,128)(2,1)}, bf16[512,128]{1,0:T(8,128)(2,1)}, u32[]{:S(2)}, u32[]{:S(2)}) collective-permute-start(bf16[512,128]{1,0:T(8,128)(2,1)} %shard_map.104.refs_0_), channel_id=1, source_target_pairs={{0,6},{2,0},{4,2},{6,4},{1,7},{3,1},{5,3},{7,5},{8,14},{10,8},{12,... | collective-permute-start | bytes 393224 | tf_op jit(solution)/shard_map/ppermute | solution.py:23
  209.9 2.9 %collective-permute-done.14.refs_2_ = bf16[512,128]{1,0:T(8,128)(2,1)} collective-permute-done((bf16[512,128]{1,0:T(8,128)(2,1)}, bf16[512,128]{1,0:T(8,128)(2,1)}, u32[]{:S(2)}, u32[]{:S(2)}) %collective-permute-start.14) | collective-permute-done | bytes 131104 | tf_op jit(solution)/shard_map/ppermute | solution.py:23
  219.3 4.0 %collective-permute-done.2 = bf16[16,64,256]{2,1,0:T(8,128)(2,1)} collective-permute-done((bf16[16,64,256]{2,1,0:T(8,128)(2,1)}, bf16[16,64,256]{2,1,0:T(8,128)(2,1)}, u32[]{:S(2)}, u32[]{:S(2)}) %collective-permute-start.2) | collective-permute-done | bytes 524320 | tf_op jit(solution)/shard_map/ppermute | solution.py:23
  224.7 2.7 %shard_map.105 = bf16[16,32,256]{2,1,0:T(8,128)(2,1)} custom-call(bf16[512,128]{1,0:T(8,128)(2,1)} %shard_map.104.refs_0_, bf16[512,128]{1,0:T(8,128)(2,1)} %copy-done.20, bf16[512,128]{1,0:T(8,128)(2,1)} %collective-permute-done.14.refs_2_, bf16[512,128]{1,0:T(8,128)(2,1)} %copy-done.22, bf16[512,128]{1,0:T(8,128)(2,1)} %copy-done.24, ...), custom_call_target="tpu_custom_call" | custom-call | tf_op jit(solution)/shard_map/pallas_call | solution.py:244
  227.5 11.9 %all-to-all-start.3 = ((bf16[16,32,256]{2,1,0:T(8,128)(2,1)}), bf16[16,32,256]{2,1,0:T(8,128)(2,1)S(1)}, u32[]{:S(2)}, u32[]{:S(2)}) async-start(bf16[16,32,256]{2,1,0:T(8,128)(2,1)} %shard_map.105), calls=%async_computation.3 | async-start | bytes 524288 | tf_op jit(solution)/shard_map/all_to_all | solution.py:335
  249.8 7.2 %all-to-all-done.3 = bf16[16,32,256]{2,1,0:T(8,128)(2,1)S(1)} async-done(((bf16[16,32,256]{2,1,0:T(8,128)(2,1)}), bf16[16,32,256]{2,1,0:T(8,128)(2,1)S(1)}, u32[]{:S(2)}, u32[]{:S(2)}) %all-to-all-start.3) | async-done | bytes 262176 | tf_op jit(solution)/shard_map/all_to_all | solution.py:335
  257.8 2.7 %shard_map.109 = bf16[256,256]{1,0:T(8,128)(2,1)} custom-call(bf16[512,256]{1,0:T(8,128)(2,1)} %bitcast.35, s32[2,256]{1,0:T(2,128)} %bitcast.39, f32[2,256]{1,0:T(2,128)} %bitcast.41, f32[256,256]{1,0:T(8,128)} %shard_map.108.refs_0_), custom_call_target="tpu_custom_call" | custom-call | tf_op jit(solution)/shard_map/pallas_call | solution.py:274
  (136 shorter events, 51.9 us)
Async XLA Ops:
  3.0 52.9 %all-to-all-start.1 = ((bf16[16,128,128]{2,1,0:T(8,128)(2,1)}), bf16[16,128,128]{2,1,0:T(8,128)(2,1)S(1)}, u32[]{:S(2)}, u32[]{:S(2)}) async-start(bf16[16,128,128]{2,1,0:T(8,128)(2,1)} %multiply_convert_fusion), calls=%async_computation.1 | async-start | bytes 1048576 | tf_op jit(solution)/shard_map/all_to_all | solution.py:335
  55.9 41.4 %all-to-all-start = ((bf16[16,168,128]{2,1,0:T(8,128)(2,1)}), bf16[16,168,128]{2,1,0:T(8,128)(2,1)S(1)}, u32[]{:S(2)}, u32[]{:S(2)}) async-start(bf16[16,168,128]{2,1,0:T(8,128)(2,1)} %shard_map.102), calls=%async_computation | async-start | bytes 1376256 | tf_op jit(solution)/shard_map/all_to_all | solution.py:335
  97.3 84.8 %all-to-all-start.2 = ((bf16[16,64,256]{2,1,0:T(8,128)(2,1)}), bf16[16,64,256]{2,1,0:T(8,128)(2,1)}, u32[]{:S(2)}, u32[]{:S(2)}) async-start(bf16[16,64,256]{2,1,0:T(8,128)(2,1)} %dynamic-slice_convert_fusion), calls=%async_computation.2 | async-start | bytes 1048576 | tf_op jit(solution)/shard_map/all_to_all | solution.py:335
  105.0 30.3 %collective-permute-start.3 = (bf16[16,32,128]{2,1,0:T(8,128)(2,1)S(1)}, bf16[16,32,128]{2,1,0:T(8,128)(2,1)S(1)}, u32[]{:S(2)}, u32[]{:S(2)}) collective-permute-start(bf16[16,32,128]{2,1,0:T(8,128)(2,1)S(1)} %split.13.refs_0_), channel_id=1, source_target_pairs={{0,8},{8,16},{16,24},{24,0},{32,40},{40,48},{48,56},{56,32},{64,72... | collective-permute-start | bytes 393224 | tf_op jit(solution)/shard_map/ppermute | solution.py:339
  106.9 33.3 %collective-permute-start.4 = (bf16[16,32,128]{2,1,0:T(8,128)(2,1)S(1)}, bf16[16,32,128]{2,1,0:T(8,128)(2,1)S(1)}, u32[]{:S(2)}, u32[]{:S(2)}) collective-permute-start(bf16[16,32,128]{2,1,0:T(8,128)(2,1)S(1)} %split.13.refs_0_), channel_id=1, source_target_pairs={{0,16},{8,24},{16,0},{24,8},{32,48},{40,56},{48,32},{56,40},{64,80... | collective-permute-start | bytes 393224 | tf_op jit(solution)/shard_map/ppermute | solution.py:339
  109.2 31.5 %collective-permute-start.5 = (bf16[16,32,128]{2,1,0:T(8,128)(2,1)S(1)}, bf16[16,32,128]{2,1,0:T(8,128)(2,1)}, u32[]{:S(2)}, u32[]{:S(2)}) collective-permute-start(bf16[16,32,128]{2,1,0:T(8,128)(2,1)S(1)} %split.13.refs_0_), channel_id=1, source_target_pairs={{0,24},{8,0},{16,8},{24,16},{32,56},{40,32},{48,40},{56,48},{64,88... | collective-permute-start | bytes 393224 | tf_op jit(solution)/shard_map/ppermute | solution.py:339
  143.1 7.2 %collective-permute-start.20 = (bf16[16,64,128]{2,1,0:T(8,128)(2,1)}, bf16[16,64,128]{2,1,0:T(8,128)(2,1)S(1)}, u32[]{:S(2)}, u32[]{:S(2)}) collective-permute-start(bf16[16,64,128]{2,1,0:T(8,128)(2,1)} %get-tuple-element.7.refs_0_), channel_id=1, source_target_pairs={{0,2},{2,4},{4,6},{6,0},{1,3},{3,5},{5,7},{7,1},{8,10},{10,12},{12... | collective-permute-start | bytes 786440 | tf_op jit(solution)/shard_map/ppermute | solution.py:23
  144.7 7.8 %collective-permute-start.21 = (bf16[16,64,128]{2,1,0:T(8,128)(2,1)}, bf16[16,64,128]{2,1,0:T(8,128)(2,1)S(1)}, u32[]{:S(2)}, u32[]{:S(2)}) collective-permute-start(bf16[16,64,128]{2,1,0:T(8,128)(2,1)} %get-tuple-element.7.refs_0_), channel_id=1, source_target_pairs={{0,6},{2,0},{4,2},{6,4},{1,7},{3,1},{5,3},{7,5},{8,14},{10,8},{12,... | collective-permute-start | bytes 786440 | tf_op jit(solution)/shard_map/ppermute | solution.py:23
  152.0 7.8 %collective-permute-start.23 = (bf16[16,64,128]{2,1,0:T(8,128)(2,1)}, bf16[16,64,128]{2,1,0:T(8,128)(2,1)S(1)}, u32[]{:S(2)}, u32[]{:S(2)}) collective-permute-start(bf16[16,64,128]{2,1,0:T(8,128)(2,1)} %get-tuple-element.7.refs_0_), channel_id=1, source_target_pairs={{0,1},{1,0},{2,3},{3,2},{4,5},{5,4},{6,7},{7,6},{8,9},{9,8},{10,11... | collective-permute-start | bytes 786440 | tf_op jit(solution)/shard_map/ppermute | solution.py:23
  152.0 10.2 %collective-permute-start.24 = (bf16[16,64,128]{2,1,0:T(8,128)(2,1)S(1)}, bf16[16,64,128]{2,1,0:T(8,128)(2,1)S(1)}, u32[]{:S(2)}, u32[]{:S(2)}) collective-permute-start(bf16[16,64,128]{2,1,0:T(8,128)(2,1)S(1)} %collective-permute-done.20.refs_1_), channel_id=1, source_target_pairs={{0,1},{1,0},{2,3},{3,2},{4,5},{5,4},{6,7},{7,6},{8,9},{9,8},{10,11... | collective-permute-start | bytes 786440 | tf_op jit(solution)/shard_map/ppermute | solution.py:23
  152.5 9.7 %collective-permute-start.25 = (bf16[16,64,128]{2,1,0:T(8,128)(2,1)S(1)}, bf16[16,64,128]{2,1,0:T(8,128)(2,1)S(1)}, u32[]{:S(2)}, u32[]{:S(2)}) collective-permute-start(bf16[16,64,128]{2,1,0:T(8,128)(2,1)S(1)} %collective-permute-done.21.refs_2_), channel_id=1, source_target_pairs={{0,1},{1,0},{2,3},{3,2},{4,5},{5,4},{6,7},{7,6},{8,9},{9,8},{10,11... | collective-permute-start | bytes 786440 | tf_op jit(solution)/shard_map/ppermute | solution.py:23
  156.6 16.0 %collective-permute-start.7 = (bf16[16,64,128]{2,1,0:T(8,128)(2,1)}, bf16[16,64,128]{2,1,0:T(8,128)(2,1)}, u32[]{:S(2)}, u32[]{:S(2)}) collective-permute-start(bf16[16,64,128]{2,1,0:T(8,128)(2,1)} %get-tuple-element.6.refs_0_), channel_id=1, source_target_pairs={{0,6},{2,0},{4,2},{6,4},{1,7},{3,1},{5,3},{7,5},{8,14},{10,8},{12,... | collective-permute-start | bytes 786440 | tf_op jit(solution)/shard_map/ppermute | solution.py:23
  159.7 39.3 %collective-permute-start.1 = (bf16[16,128,128]{2,1,0:T(8,128)(2,1)S(1)}, bf16[16,128,128]{2,1,0:T(8,128)(2,1)}, u32[]{:S(2)}, u32[]{:S(2)}) collective-permute-start(bf16[16,128,128]{2,1,0:T(8,128)(2,1)S(1)} %all-to-all-done.1), channel_id=1, source_target_pairs={{0,128},{128,0},{1,129},{129,1},{2,130},{130,2},{3,131},{131,3},{4... | collective-permute-start | bytes 1572872 | tf_op jit(solution)/shard_map/ppermute | solution.py:23
  172.7 8.7 %collective-permute-start.32 = (bf16[512,128]{1,0:T(8,128)(2,1)S(1)}, bf16[512,128]{1,0:T(8,128)(2,1)S(1)}, u32[]{:S(2)}, u32[]{:S(2)}) collective-permute-start(bf16[512,128]{1,0:T(8,128)(2,1)S(1)} %collective-permute-done.28.refs_2_), channel_id=1, source_target_pairs={{0,1},{1,0},{2,3},{3,2},{4,5},{5,4},{6,7},{7,6},{8,9},{9,8},{10,11... | collective-permute-start | bytes 393224 | tf_op jit(solution)/shard_map/ppermute | solution.py:23
  173.2 27.7 %collective-permute-start = (bf16[16,128,128]{2,1,0:T(8,128)(2,1)}, bf16[16,128,128]{2,1,0:T(8,128)(2,1)}, u32[]{:S(2)}, u32[]{:S(2)}) collective-permute-start(bf16[16,128,128]{2,1,0:T(8,128)(2,1)} %split.12), channel_id=1, source_target_pairs={{0,128},{128,0},{1,129},{129,1},{2,130},{130,2},{3,131},{131,3},{4... | collective-permute-start | bytes 1572872 | tf_op jit(solution)/shard_map/ppermute | solution.py:23
  178.0 21.5 %collective-permute-start.6 = (bf16[16,64,128]{2,1,0:T(8,128)(2,1)}, bf16[16,64,128]{2,1,0:T(8,128)(2,1)}, u32[]{:S(2)}, u32[]{:S(2)}) collective-permute-start(bf16[16,64,128]{2,1,0:T(8,128)(2,1)} %get-tuple-element.6.refs_0_), channel_id=1, source_target_pairs={{0,2},{2,4},{4,6},{6,0},{1,3},{3,5},{5,7},{7,1},{8,10},{10,12},{12... | collective-permute-start | bytes 786440 | tf_op jit(solution)/shard_map/ppermute | solution.py:23
  178.0 21.6 %collective-permute-start.8 = (bf16[16,64,128]{2,1,0:T(8,128)(2,1)}, bf16[16,64,128]{2,1,0:T(8,128)(2,1)}, u32[]{:S(2)}, u32[]{:S(2)}) collective-permute-start(bf16[16,64,128]{2,1,0:T(8,128)(2,1)} %collective-permute-done.7.refs_2_), channel_id=1, source_target_pairs={{0,6},{2,0},{4,2},{6,4},{1,7},{3,1},{5,3},{7,5},{8,14},{10,8},{12,... | collective-permute-start | bytes 786440 | tf_op jit(solution)/shard_map/ppermute | solution.py:23
  186.5 41.0 %all-to-all-start.4 = ((bf16[16,32,256]{2,1,0:T(8,128)(2,1)}), bf16[16,32,256]{2,1,0:T(8,128)(2,1)}, u32[]{:S(2)}, u32[]{:S(2)}) async-start(bf16[16,32,256]{2,1,0:T(8,128)(2,1)} %shard_map.107), calls=%async_computation.4 | async-start | bytes 524288 | tf_op jit(solution)/shard_map/all_to_all | solution.py:335
  205.8 6.9 %collective-permute-start.14 = (bf16[512,128]{1,0:T(8,128)(2,1)}, bf16[512,128]{1,0:T(8,128)(2,1)}, u32[]{:S(2)}, u32[]{:S(2)}) collective-permute-start(bf16[512,128]{1,0:T(8,128)(2,1)} %shard_map.104.refs_0_), channel_id=1, source_target_pairs={{0,6},{2,0},{4,2},{6,4},{1,7},{3,1},{5,3},{7,5},{8,14},{10,8},{12,... | collective-permute-start | bytes 393224 | tf_op jit(solution)/shard_map/ppermute | solution.py:23
  209.3 14.0 %collective-permute-start.2 = (bf16[16,64,256]{2,1,0:T(8,128)(2,1)}, bf16[16,64,256]{2,1,0:T(8,128)(2,1)}, u32[]{:S(2)}, u32[]{:S(2)}) collective-permute-start(bf16[16,64,256]{2,1,0:T(8,128)(2,1)} %all-to-all-done.2), channel_id=1, source_target_pairs={{0,128},{128,0},{1,129},{129,1},{2,130},{130,2},{3,131},{131,3},{4... | collective-permute-start | bytes 1572872 | tf_op jit(solution)/shard_map/ppermute | solution.py:23
  209.9 7.2 %collective-permute-start.13 = (bf16[512,128]{1,0:T(8,128)(2,1)}, bf16[512,128]{1,0:T(8,128)(2,1)S(1)}, u32[]{:S(2)}, u32[]{:S(2)}) collective-permute-start(bf16[512,128]{1,0:T(8,128)(2,1)} %shard_map.104.refs_0_), channel_id=1, source_target_pairs={{0,2},{2,4},{4,6},{6,0},{1,3},{3,5},{5,7},{7,1},{8,10},{10,12},{12... | collective-permute-start | bytes 393224 | tf_op jit(solution)/shard_map/ppermute | solution.py:23
  216.4 6.9 %collective-permute-start.16 = (bf16[512,128]{1,0:T(8,128)(2,1)S(1)}, bf16[512,128]{1,0:T(8,128)(2,1)S(1)}, u32[]{:S(2)}, u32[]{:S(2)}) collective-permute-start(bf16[512,128]{1,0:T(8,128)(2,1)S(1)} %copy-done.6), channel_id=1, source_target_pairs={{0,1},{1,0},{2,3},{3,2},{4,5},{5,4},{6,7},{7,6},{8,9},{9,8},{10,11... | collective-permute-start | bytes 393224 | tf_op jit(solution)/shard_map/ppermute | solution.py:23
  216.6 6.8 %collective-permute-start.18 = (bf16[512,128]{1,0:T(8,128)(2,1)}, bf16[512,128]{1,0:T(8,128)(2,1)S(1)}, u32[]{:S(2)}, u32[]{:S(2)}) collective-permute-start(bf16[512,128]{1,0:T(8,128)(2,1)} %collective-permute-done.14.refs_2_), channel_id=1, source_target_pairs={{0,1},{1,0},{2,3},{3,2},{4,5},{5,4},{6,7},{7,6},{8,9},{9,8},{10,11... | collective-permute-start | bytes 393224 | tf_op jit(solution)/shard_map/ppermute | solution.py:23
  227.5 29.6 %all-to-all-start.3 = ((bf16[16,32,256]{2,1,0:T(8,128)(2,1)}), bf16[16,32,256]{2,1,0:T(8,128)(2,1)S(1)}, u32[]{:S(2)}, u32[]{:S(2)}) async-start(bf16[16,32,256]{2,1,0:T(8,128)(2,1)} %shard_map.105), calls=%async_computation.3 | async-start | bytes 524288 | tf_op jit(solution)/shard_map/all_to_all | solution.py:335
  (45 other events, 376.0 us)

commit v4 on v3

--- a/solution.py
+++ b/solution.py
@@ -13,6 +13,7 @@
 F32 = jnp.float32
 LANES = 128
 META = 8
+LIMIT = pltpu.CompilerParams(vmem_limit_bytes=14 * 2**20)
 
 VM = pl.BlockSpec(memory_space=pltpu.VMEM)
 ANY = pl.BlockSpec(memory_space=pl.ANY)
@@ -25,6 +26,14 @@
 
 def shape(dims, dtype=BF):
     return jax.ShapeDtypeStruct(dims, dtype)
+
+
+def held(dims, dtype=BF):
+    return pltpu.VMEM(dims, dtype)
+
+
+def near_core(arrays):
+    return [pltpu.with_memory_space_constraint(a, pltpu.VMEM) for a in arrays]
 
 
 def iota(dims, dim):
@@ -52,13 +61,6 @@
         (i * capacity + jnp.sum(jnp.where(h, count, 0.0), axis=1, keepdims=True)).astype(jnp.int32)
         for i, h in zip(ids, hits)
     ]
-
-
-def fetch(pairs, sems):
-    copies = [pltpu.make_async_copy(src, dst, sems.at[i]) for i, (src, dst) in enumerate(pairs)]
-    for c in copies:
-        c.start()
-    return [c.wait for c in copies]
 
 
 def pack_first(tokens, route_ids, gain, gate, n, count, groups):
@@ -160,11 +162,12 @@
 
     return pl.pallas_call(
         body,
-        out_shape=tuple(shape((n, pieces * capacity, LANES)) for _ in range(per_device)),
+        out_shape=tuple(held((n, pieces * capacity, LANES)) for _ in range(per_device)),
         in_specs=[VM] * (members + 1),
         out_specs=tuple(VM for _ in range(per_device)),
+        compiler_params=LIMIT,
         scratch_shapes=[pltpu.VMEM((n, part, pieces * LANES), BF)],
-    )(*blocks, named)
+    )(*near_core([*blocks, named]))
 
 
 def expert_at(k, per_device):
@@ -194,89 +197,75 @@
     count = len(blocks)
 
     def body(*refs):
-        ins, (gate_ref, up_ref, out_ref, in_buf, w_buf, sems) = (refs[:count], refs[count:])
-        pairs = []
+        ins, (gate_ref, up_ref, out_ref, in_buf, w_buf) = (refs[:count], refs[count:])
         for i, tp in enumerate(places_of()):
             d = pl.ds(pl.multiple_of(tp * width, width), width)
             to = slice(i * width, (i + 1) * width)
-            pairs += [(gate_ref.at[d, :], w_buf.at[to, :cols]), (up_ref.at[d, :], w_buf.at[to, cols:])]
+            w_buf[to, :cols] = gate_ref[d, :]
+            w_buf[to, cols:] = up_ref[d, :]
             for p in range(pieces):
                 lanes = slice(i * width + p * LANES, i * width + (p + 1) * LANES)
-                pairs.append(
-                    (ins[i].at[:, p * capacity : (p + 1) * capacity, :], in_buf.at[:, :, lanes])
-                )
-        for wait in fetch(pairs, sems):
-            wait()
-        both = dot(in_buf[...].reshape(rows, depth), w_buf[...])
+                in_buf[:, lanes] = ins[i][:, p * capacity : (p + 1) * capacity, :].reshape(rows, LANES)
+        both = dot(in_buf[...], w_buf[...])
         g = both[:, :cols]
         out_ref[...] = (g / (1.0 + jnp.exp(-g)) * both[:, cols:]).astype(BF)
 
     return pl.pallas_call(
         body,
-        out_shape=shape((rows, cols)),
-        in_specs=[ANY] * (count + 2),
+        out_shape=held((rows, cols)),
+        in_specs=[VM] * (count + 2),
         out_specs=VM,
-        scratch_shapes=[
-            pltpu.VMEM((n, capacity, depth), BF),
-            pltpu.VMEM((depth, 2 * cols), BF),
-            pltpu.SemaphoreType.DMA((count * (2 + pieces),)),
-        ],
-    )(*blocks, gate, up)
-
-
-def second_matmul(blocks, down, n):
+        compiler_params=LIMIT,
+        scratch_shapes=[pltpu.VMEM((rows, depth), BF), pltpu.VMEM((depth, 2 * cols), BF)],
+    )(*near_core([*blocks, gate, up]))
+
+
+def second_matmul(blocks, down, n, k, per_device, done):
     rows, width = blocks[0].shape
     depth, cols = down.shape
     capacity = rows // n
     count = len(blocks)
+    last = k == per_device - 1
 
     def body(*refs):
-        ins, (down_ref, out_ref, in_buf, down_buf, sems) = (refs[:count], refs[count:])
-        pairs = []
+        ins, (down_ref, *dones) = (refs[:count], refs[count : count + 1 + len(done)])
+        out_ref, in_buf, down_buf = refs[count + 1 + len(done) :]
         for i, tp in enumerate(places_of()):
-            d = pl.ds(pl.multiple_of(tp * width, width), width)
             to = slice(i * width, (i + 1) * width)
-            pairs += [(down_ref.at[d, :], down_buf.at[to, :]), (ins[i], in_buf.at[:, to])]
-        for wait in fetch(pairs, sems):
-            wait()
-        out_ref[...] = dot(in_buf[...], down_buf[...]).reshape(n, capacity, cols).astype(BF)
+            down_buf[to, :] = down_ref[pl.ds(pl.multiple_of(tp * width, width), width), :]
+            in_buf[:, to] = ins[i][...]
+        out = dot(in_buf[...], down_buf[...]).reshape(n, capacity, cols).astype(BF)
+        if last:
+            out_ref[:, expert_at(k, per_device)] = out
+            for i, ref in enumerate(dones):
+                out_ref[:, expert_at(i, per_device)] = ref[...]
+        else:
+            out_ref[...] = out
 
     return pl.pallas_call(
         body,
-        out_shape=shape((n, capacity, cols)),
-        in_specs=[ANY] * (count + 1),
+        out_shape=shape((n, per_device, capacity, cols)) if last else held((n, capacity, cols)),
+        in_specs=[VM] * (count + 1 + len(done)),
         out_specs=VM,
-        scratch_shapes=[
-            pltpu.VMEM((rows, depth), BF),
-            pltpu.VMEM((depth, cols), BF),
-            pltpu.SemaphoreType.DMA((2 * count,)),
-        ],
-    )(*blocks, down)
-
-
-def combine(returned, route_ids, route_weights, capacity, k, per_device, so_far):
+        compiler_params=LIMIT,
+        scratch_shapes=[pltpu.VMEM((rows, depth), BF), pltpu.VMEM((depth, cols), BF)],
+    )(*near_core([*blocks, down, *done]))
+
+
+def combine(returned, route_ids, route_weights, capacity):
     rows, cols = (route_ids.shape[0], returned.shape[1])
     slots = returned.shape[0]
-    last = k == per_device - 1
-
-    def body(ret_ref, ids_ref, w_ref, *refs):
-        out_ref = refs[-1]
-        total = jnp.zeros((rows, cols), F32) if so_far is None else refs[0][...]
+
+    def body(ret_ref, ids_ref, w_ref, out_ref):
+        total = jnp.zeros((rows, cols), F32)
         for r, slot in enumerate(slot_of(ids_ref, capacity)):
-            expert, at = (slot // capacity, slot % capacity)
-            mine = expert % per_device == expert_at(k, per_device)
-            to = jnp.where(mine, expert // per_device * capacity + at, -1)
-            pick = jnp.where(iota((rows, slots), 1) == to, 1.0, 0.0).astype(BF)
+            pick = (iota((rows, slots), 1) == slot).astype(BF)
             total = total + dot(pick, ret_ref[...]) * as_column(w_ref[r : r + 1, :])
-        out_ref[...] = total.astype(out_ref.dtype)
-
-    given = [] if so_far is None else [so_far]
-    return pl.pallas_call(
-        body,
-        out_shape=shape((rows, cols), BF if last else F32),
-        in_specs=[VM] * (3 + len(given)),
-        out_specs=VM,
-    )(returned, route_ids.T, route_weights.T, *given)
+        out_ref[...] = total.astype(BF)
+
+    return pl.pallas_call(
+        body, out_shape=shape((rows, cols)), in_specs=[VM] * 3, out_specs=VM, compiler_params=LIMIT
+    )(*near_core([returned, route_ids.T, route_weights.T]))
 
 
 def by_target(master, n):
@@ -360,14 +349,15 @@
     gates = one_by_one(gate, gate_serve, index, count, per_device)
     ups = one_by_one(up, up_serve, index, count, per_device)
     downs = one_by_one(down, down_serve, index, count, per_device)
-    mixed = None
+    outs = []
     for k in range(per_device):
         blocks = gather_tp(chosen[k], k % 2)
         hidden = first_matmuls(blocks, gates[k], ups[k], capacity)
         hidden = gather_tp(hidden, k % 2)
-        out = second_matmul(hidden, downs[k], n)
-        out = swap(out).reshape(-1, out.shape[-1])
-        mixed = combine(out, route_ids, route_weights, capacity, k, per_device, mixed)
+        last = k == per_device - 1
+        outs.append(second_matmul(hidden, downs[k], n, k, per_device, outs if last else []))
+    out = swap(outs[-1])
+    mixed = combine(out.reshape(-1, out.shape[-1]), route_ids, route_weights, capacity)
     return (gate_serve, up_serve, down_serve, mixed)
 
 

time: 262 us -> 239 us (0.912)
  Pallas kernels: 23.8 us -> 11.7 us
  starting transfers between devices: 92.5 us -> 84 us
    all_to_all x5 -> x4, waiting for transfers between devices: 66.6 us -> 81.4 us  [swap(): return lax.all_to_all(x, 'fs', split_axis=0, concat_axis=0, tiled=True)]
    ppermute x31, waiting for transfers between devices: 28.4 us -> 15.5 us  [shift(): return lax.ppermute(x, axis, [(i, (i + k) % n) for i in range(n)])]
    pallas_call x7 -> x6, Pallas kernels: 20.4 us -> 8.35 us  [the longest x2 4.5 us: first_matmuls(): pl.pallas_call(body, out_shape=held((rows, cols)), in_specs=[VM] * (count...]
    all_to_all x5 -> x4, starting transfers between devices: 62.6 us -> 50.9 us  [swap(): return lax.all_to_all(x, 'fs', split_axis=0, concat_axis=0, tiled=True)]
    dynamic_update_slice x6, local copies, waits for them, and re-layouts: 7.66 us -> 4.03 us  [assemble(): buffer = lax.dynamic_update_slice(buffer, piece[None], (at, 0, 0, 0))]
    ppermute x31, starting transfers between devices: 24.3 us -> 27.5 us  [shift(): return lax.ppermute(x, axis, [(i, (i + k) % n) for i in range(n)])]
    ppermute x3, waiting for transfers between devices: 28.8 us -> 25.7 us  [neighbour(): return lax.ppermute(x, 'fs', pairs)]
    unnamed x60 -> x22, local copies, waits for them, and re-layouts: 5.4 us -> 4.98 us
  transfers between devices with their start and end apart: 39 -> 38, of which waited for: 17 -> 16; matrix products, arithmetic and copies ran while one was open for 4% -> 4% of each run, Pallas kernels for 8% -> 4%
where the time goes in v4:
time: 239 us; the launch traced here: 237 us
  waiting for transfers between devices  122 us (51%)
  starting transfers between devices  84 us (35%)
  local copies, waits for them, and re-layouts  15.1 us (6%)
  Pallas kernels  11.7 us (5%)
    all_to_all x4, waiting for transfers between devices, swap(): return lax.all_to_all(x, 'fs', split_axis=0, concat_axis=0, tiled=True)  81.4 us
    all_to_all x4, starting transfers between devices, swap(): return lax.all_to_all(x, 'fs', split_axis=0, concat_axis=0, tiled=True)  50.9 us
    ppermute x31, starting transfers between devices, shift(): return lax.ppermute(x, axis, [(i, (i + k) % n) for i in range(n)])  27.5 us
    ppermute x3, waiting for transfers between devices, neighbour(): return lax.ppermute(x, 'fs', pairs)  25.7 us
    ppermute x31, waiting for transfers between devices, shift(): return lax.ppermute(x, axis, [(i, (i + k) % n) for i in range(n)])  15.5 us
    ppermute x3, starting transfers between devices, neighbour(): return lax.ppermute(x, 'fs', pairs)  5.54 us
    unnamed x22, local copies, waits for them, and re-layouts  4.98 us
  transfers between devices with their start and end apart: 38, of which 16 were waited for; matrix products, arithmetic and copies ran while one was open for 4% of the time, Pallas kernels for 4%

profile of v4, /device:TPU:34, one launch (start us, length us, event | category | flops | bytes accessed | tf_op | source)
XLA Modules:
  0.0 236.6 jit_solution(3026271875110439856)
XLA Ops:
  0.7 2.4 %multiply_convert_fusion = bf16[16,128,128]{2,1,0:T(8,128)(2,1)} fusion(f32[16,256,128]{2,1,0:T(8,128)} %bitcast.39, s32[]{:T(128)S(6)} %select_n.39, f32[128]{0:T(128)} %param.10), kind=kLoop, calls=%fused_computation.1 | loop fusion | flops 524288 | bytes 1573380 | tf_op jit(solution)/shard_map/convert_element_type | solution.py:340
  3.0 24.0 %all-to-all-start.1 = ((bf16[16,128,128]{2,1,0:T(8,128)(2,1)}), bf16[16,128,128]{2,1,0:T(8,128)(2,1)S(1)}, u32[]{:S(2)}, u32[]{:S(2)}) async-start(bf16[16,128,128]{2,1,0:T(8,128)(2,1)} %multiply_convert_fusion), calls=%async_computation.1 | async-start | bytes 1048576 | tf_op jit(solution)/shard_map/all_to_all | solution.py:324
  27.0 3.4 %shard_map.102 = bf16[16,168,128]{2,1,0:T(8,128)(2,1)} custom-call(bf16[256,2048]{1,0:T(8,128)(2,1)} %tok_ref.1, s32[2,256]{1,0:T(2,128)} %bitcast.33, f32[1,128]{1,0:T(1,128)} %bitcast.40, f32[16,256,128]{2,1,0:T(8,128)} %bitcast.36), custom_call_target="tpu_custom_call" | custom-call | tf_op jit(solution)/shard_map/pallas_call | solution.py:116
  30.4 25.5 %all-to-all-done.1 = bf16[16,128,128]{2,1,0:T(8,128)(2,1)S(1)} async-done(((bf16[16,128,128]{2,1,0:T(8,128)(2,1)}), bf16[16,128,128]{2,1,0:T(8,128)(2,1)S(1)}, u32[]{:S(2)}, u32[]{:S(2)}) %all-to-all-start.1) | async-done | bytes 524320 | tf_op jit(solution)/shard_map/all_to_all | solution.py:324
  55.9 6.6 %all-to-all-start = ((bf16[16,168,128]{2,1,0:T(8,128)(2,1)}), bf16[16,168,128]{2,1,0:T(8,128)(2,1)}, u32[]{:S(2)}, u32[]{:S(2)}) async-start(bf16[16,168,128]{2,1,0:T(8,128)(2,1)} %shard_map.102), calls=%async_computation | async-start | bytes 1376256 | tf_op jit(solution)/shard_map/all_to_all | solution.py:324
  63.4 34.0 %all-to-all-done = bf16[16,168,128]{2,1,0:T(8,128)(2,1)} async-done(((bf16[16,168,128]{2,1,0:T(8,128)(2,1)}), bf16[16,168,128]{2,1,0:T(8,128)(2,1)}, u32[]{:S(2)}, u32[]{:S(2)}) %all-to-all-start) | async-done | bytes 688160 | tf_op jit(solution)/shard_map/all_to_all | solution.py:324
  97.4 7.7 %all-to-all-start.2 = ((bf16[16,64,256]{2,1,0:T(8,128)(2,1)}), bf16[16,64,256]{2,1,0:T(8,128)(2,1)S(1)}, u32[]{:S(2)}, u32[]{:S(2)}) async-start(bf16[16,64,256]{2,1,0:T(8,128)(2,1)} %dynamic-slice_convert_fusion), calls=%async_computation.2 | async-start | bytes 1048576 | tf_op jit(solution)/shard_map/all_to_all | solution.py:324
  105.1 2.2 collective-permute-start.1
  110.0 2.4 collective-permute-start.4
  114.6 20.9 %collective-permute-done.3.refs_1_ = bf16[16,32,128]{2,1,0:T(8,128)(2,1)S(1)} collective-permute-done((bf16[16,32,128]{2,1,0:T(8,128)(2,1)S(1)}, bf16[16,32,128]{2,1,0:T(8,128)(2,1)S(1)}, u32[]{:S(2)}, u32[]{:S(2)}) %collective-permute-start.3) | collective-permute-done | bytes 131104 | tf_op jit(solution)/shard_map/ppermute | solution.py:328
  135.4 4.8 %collective-permute-done.4.refs_2_ = bf16[16,32,128]{2,1,0:T(8,128)(2,1)S(1)} collective-permute-done((bf16[16,32,128]{2,1,0:T(8,128)(2,1)S(1)}, bf16[16,32,128]{2,1,0:T(8,128)(2,1)S(1)}, u32[]{:S(2)}, u32[]{:S(2)}) %collective-permute-start.4) | collective-permute-done | bytes 131104 | tf_op jit(solution)/shard_map/ppermute | solution.py:328
  151.5 2.1 collective-permute-start
  154.6 3.1 %collective-permute-start.8 = (bf16[16,64,128]{2,1,0:T(8,128)(2,1)}, bf16[16,64,128]{2,1,0:T(8,128)(2,1)}, u32[]{:S(2)}, u32[]{:S(2)}) collective-permute-start(bf16[16,64,128]{2,1,0:T(8,128)(2,1)} %collective-permute-done.7.refs_2_), channel_id=1, source_target_pairs={{0,6},{2,0},{4,2},{6,4},{1,7},{3,1},{5,3},{7,5},{8,14},{10,8},{12,... | collective-permute-start | bytes 786440 | tf_op jit(solution)/shard_map/ppermute | solution.py:24
  160.1 3.4 %collective-permute-done.8.refs_3_ = bf16[16,64,128]{2,1,0:T(8,128)(2,1)} collective-permute-done((bf16[16,64,128]{2,1,0:T(8,128)(2,1)}, bf16[16,64,128]{2,1,0:T(8,128)(2,1)}, u32[]{:S(2)}, u32[]{:S(2)}) %collective-permute-start.8) | collective-permute-done | bytes 262176 | tf_op jit(solution)/shard_map/ppermute | solution.py:24
  164.0 2.0 shard_map.105.refs_0_
  166.0 2.2 collective-permute-start.2
  171.3 2.5 %shard_map.104.refs_0_ = bf16[512,128]{1,0:T(8,128)(2,1)S(1)} custom-call(bf16[16,64,128]{2,1,0:T(8,128)(2,1)S(1)} %get-tuple-element.6.refs_0_, bf16[16,64,128]{2,1,0:T(8,128)(2,1)} %collective-permute-done.6.refs_1_, bf16[16,64,128]{2,1,0:T(8,128)(2,1)} %collective-permute-done.7.refs_2_, bf16[16,64,128]{2,1,0:T(8,128)(2,1)} %collective-permute-done.8.refs_3_, ...), custom_call_target="tpu_custom_call" | custom-call | tf_op jit(solution)/shard_map/pallas_call | solution.py:213
  173.9 2.8 %collective-permute-start.14 = (bf16[512,128]{1,0:T(8,128)(2,1)S(1)}, bf16[512,128]{1,0:T(8,128)(2,1)S(1)}, u32[]{:S(2)}, u32[]{:S(2)}) collective-permute-start(bf16[512,128]{1,0:T(8,128)(2,1)S(1)} %shard_map.104.refs_0_), channel_id=1, source_target_pairs={{0,6},{2,0},{4,2},{6,4},{1,7},{3,1},{5,3},{7,5},{8,14},{10,8},{12,... | collective-permute-start | bytes 393224 | tf_op jit(solution)/shard_map/ppermute | solution.py:24
  178.1 2.1 collective-permute-done.14.refs_2_
  180.2 2.8 %collective-permute-done.13.refs_1_ = bf16[512,128]{1,0:T(8,128)(2,1)S(1)} collective-permute-done((bf16[512,128]{1,0:T(8,128)(2,1)S(1)}, bf16[512,128]{1,0:T(8,128)(2,1)S(1)}, u32[]{:S(2)}, u32[]{:S(2)}) %collective-permute-start.13) | collective-permute-done | bytes 131104 | tf_op jit(solution)/shard_map/ppermute | solution.py:24
  183.0 3.1 %collective-permute-start.15 = (bf16[512,128]{1,0:T(8,128)(2,1)S(1)}, bf16[512,128]{1,0:T(8,128)(2,1)S(1)}, u32[]{:S(2)}, u32[]{:S(2)}) collective-permute-start(bf16[512,128]{1,0:T(8,128)(2,1)S(1)} %collective-permute-done.14.refs_2_), channel_id=1, source_target_pairs={{0,6},{2,0},{4,2},{6,4},{1,7},{3,1},{5,3},{7,5},{8,14},{10,8},{12,... | collective-permute-start | bytes 393224 | tf_op jit(solution)/shard_map/ppermute | solution.py:24
  192.3 12.6 %all-to-all-start.3 = ((bf16[16,2,32,256]{3,2,1,0:T(8,128)(2,1)}), bf16[16,2,32,256]{3,2,1,0:T(8,128)(2,1)}, u32[]{:S(2)}, u32[]{:S(2)}) async-start(bf16[16,2,32,256]{3,2,1,0:T(8,128)(2,1)} %copy-done.4), calls=%async_computation.3 | async-start | bytes 1048576 | tf_op jit(solution)/shard_map/all_to_all | solution.py:324
  212.2 21.9 %all-to-all-done.3 = bf16[16,2,32,256]{3,2,1,0:T(8,128)(2,1)} async-done(((bf16[16,2,32,256]{3,2,1,0:T(8,128)(2,1)}), bf16[16,2,32,256]{3,2,1,0:T(8,128)(2,1)}, u32[]{:S(2)}, u32[]{:S(2)}) %all-to-all-start.3) | async-done | bytes 524320 | tf_op jit(solution)/shard_map/all_to_all | solution.py:324
  234.1 2.5 %shard_map.108 = bf16[256,256]{1,0:T(8,128)(2,1)} custom-call(bf16[1024,256]{1,0:T(8,128)(2,1)} %bitcast.20.ret_ref, s32[2,256]{1,0:T(2,128)S(1)} %bitcast.34, f32[2,256]{1,0:T(2,128)S(1)} %bitcast.35), custom_call_target="tpu_custom_call" | custom-call | tf_op jit(solution)/shard_map/pallas_call | solution.py:266
  (95 shorter events, 38.8 us)
Async XLA Ops:
  3.0 52.9 %all-to-all-start.1 = ((bf16[16,128,128]{2,1,0:T(8,128)(2,1)}), bf16[16,128,128]{2,1,0:T(8,128)(2,1)S(1)}, u32[]{:S(2)}, u32[]{:S(2)}) async-start(bf16[16,128,128]{2,1,0:T(8,128)(2,1)} %multiply_convert_fusion), calls=%async_computation.1 | async-start | bytes 1048576 | tf_op jit(solution)/shard_map/all_to_all | solution.py:324
  55.9 41.5 %all-to-all-start = ((bf16[16,168,128]{2,1,0:T(8,128)(2,1)}), bf16[16,168,128]{2,1,0:T(8,128)(2,1)}, u32[]{:S(2)}, u32[]{:S(2)}) async-start(bf16[16,168,128]{2,1,0:T(8,128)(2,1)} %shard_map.102), calls=%async_computation | async-start | bytes 1376256 | tf_op jit(solution)/shard_map/all_to_all | solution.py:324
  97.4 68.6 %all-to-all-start.2 = ((bf16[16,64,256]{2,1,0:T(8,128)(2,1)}), bf16[16,64,256]{2,1,0:T(8,128)(2,1)S(1)}, u32[]{:S(2)}, u32[]{:S(2)}) async-start(bf16[16,64,256]{2,1,0:T(8,128)(2,1)} %dynamic-slice_convert_fusion), calls=%async_computation.2 | async-start | bytes 1048576 | tf_op jit(solution)/shard_map/all_to_all | solution.py:324
  105.1 39.4 %collective-permute-start.1 = (bf16[16,128,128]{2,1,0:T(8,128)(2,1)S(1)}, bf16[16,128,128]{2,1,0:T(8,128)(2,1)S(1)}, u32[]{:S(2)}, u32[]{:S(2)}) collective-permute-start(bf16[16,128,128]{2,1,0:T(8,128)(2,1)S(1)} %all-to-all-done.1), channel_id=1, source_target_pairs={{0,128},{128,0},{1,129},{129,1},{2,130},{130,2},{3,131},{131,3},{4... | collective-permute-start | bytes 1572872 | tf_op jit(solution)/shard_map/ppermute | solution.py:24
  108.3 27.2 %collective-permute-start.3 = (bf16[16,32,128]{2,1,0:T(8,128)(2,1)S(1)}, bf16[16,32,128]{2,1,0:T(8,128)(2,1)S(1)}, u32[]{:S(2)}, u32[]{:S(2)}) collective-permute-start(bf16[16,32,128]{2,1,0:T(8,128)(2,1)S(1)} %split.13.refs_0_), channel_id=1, source_target_pairs={{0,8},{8,16},{16,24},{24,0},{32,40},{40,48},{48,56},{56,32},{64,72... | collective-permute-start | bytes 393224 | tf_op jit(solution)/shard_map/ppermute | solution.py:328
  110.0 30.2 %collective-permute-start.4 = (bf16[16,32,128]{2,1,0:T(8,128)(2,1)S(1)}, bf16[16,32,128]{2,1,0:T(8,128)(2,1)S(1)}, u32[]{:S(2)}, u32[]{:S(2)}) collective-permute-start(bf16[16,32,128]{2,1,0:T(8,128)(2,1)S(1)} %split.13.refs_0_), channel_id=1, source_target_pairs={{0,16},{8,24},{16,0},{24,8},{32,48},{40,56},{48,32},{56,40},{64,80... | collective-permute-start | bytes 393224 | tf_op jit(solution)/shard_map/ppermute | solution.py:328
  112.3 27.9 %collective-permute-start.5 = (bf16[16,32,128]{2,1,0:T(8,128)(2,1)S(1)}, bf16[16,32,128]{2,1,0:T(8,128)(2,1)S(1)}, u32[]{:S(2)}, u32[]{:S(2)}) collective-permute-start(bf16[16,32,128]{2,1,0:T(8,128)(2,1)S(1)} %split.13.refs_0_), channel_id=1, source_target_pairs={{0,24},{8,0},{16,8},{24,16},{32,56},{40,32},{48,40},{56,48},{64,88... | collective-permute-start | bytes 393224 | tf_op jit(solution)/shard_map/ppermute | solution.py:328
  142.4 9.1 %collective-permute-start.21 = (bf16[16,64,128]{2,1,0:T(8,128)(2,1)S(1)}, bf16[16,64,128]{2,1,0:T(8,128)(2,1)S(1)}, u32[]{:S(2)}, u32[]{:S(2)}) collective-permute-start(bf16[16,64,128]{2,1,0:T(8,128)(2,1)S(1)} %get-tuple-element.7.refs_0_), channel_id=1, source_target_pairs={{0,6},{2,0},{4,2},{6,4},{1,7},{3,1},{5,3},{7,5},{8,14},{10,8},{12,... | collective-permute-start | bytes 786440 | tf_op jit(solution)/shard_map/ppermute | solution.py:24
  142.8 8.7 %collective-permute-start.23 = (bf16[16,64,128]{2,1,0:T(8,128)(2,1)S(1)}, bf16[16,64,128]{2,1,0:T(8,128)(2,1)S(1)}, u32[]{:S(2)}, u32[]{:S(2)}) collective-permute-start(bf16[16,64,128]{2,1,0:T(8,128)(2,1)S(1)} %get-tuple-element.7.refs_0_), channel_id=1, source_target_pairs={{0,1},{1,0},{2,3},{3,2},{4,5},{5,4},{6,7},{7,6},{8,9},{9,8},{10,11... | collective-permute-start | bytes 786440 | tf_op jit(solution)/shard_map/ppermute | solution.py:24
  142.8 11.6 %collective-permute-start.7 = (bf16[16,64,128]{2,1,0:T(8,128)(2,1)S(1)}, bf16[16,64,128]{2,1,0:T(8,128)(2,1)}, u32[]{:S(2)}, u32[]{:S(2)}) collective-permute-start(bf16[16,64,128]{2,1,0:T(8,128)(2,1)S(1)} %get-tuple-element.6.refs_0_), channel_id=1, source_target_pairs={{0,6},{2,0},{4,2},{6,4},{1,7},{3,1},{5,3},{7,5},{8,14},{10,8},{12,... | collective-permute-start | bytes 786440 | tf_op jit(solution)/shard_map/ppermute | solution.py:24
  145.3 9.3 %collective-permute-start.6 = (bf16[16,64,128]{2,1,0:T(8,128)(2,1)S(1)}, bf16[16,64,128]{2,1,0:T(8,128)(2,1)}, u32[]{:S(2)}, u32[]{:S(2)}) collective-permute-start(bf16[16,64,128]{2,1,0:T(8,128)(2,1)S(1)} %get-tuple-element.6.refs_0_), channel_id=1, source_target_pairs={{0,2},{2,4},{4,6},{6,0},{1,3},{3,5},{5,7},{7,1},{8,10},{10,12},{12... | collective-permute-start | bytes 786440 | tf_op jit(solution)/shard_map/ppermute | solution.py:24
  147.2 12.3 %collective-permute-start.22 = (bf16[16,64,128]{2,1,0:T(8,128)(2,1)S(1)}, bf16[16,64,128]{2,1,0:T(8,128)(2,1)S(1)}, u32[]{:S(2)}, u32[]{:S(2)}) collective-permute-start(bf16[16,64,128]{2,1,0:T(8,128)(2,1)S(1)} %collective-permute-done.20.refs_1_), channel_id=1, source_target_pairs={{0,2},{2,4},{4,6},{6,0},{1,3},{3,5},{5,7},{7,1},{8,10},{10,12},{12... | collective-permute-start | bytes 786440 | tf_op jit(solution)/shard_map/ppermute | solution.py:24
  151.5 8.0 %collective-permute-start.24 = (bf16[16,64,128]{2,1,0:T(8,128)(2,1)S(1)}, bf16[16,64,128]{2,1,0:T(8,128)(2,1)S(1)}, u32[]{:S(2)}, u32[]{:S(2)}) collective-permute-start(bf16[16,64,128]{2,1,0:T(8,128)(2,1)S(1)} %collective-permute-done.20.refs_1_), channel_id=1, source_target_pairs={{0,1},{1,0},{2,3},{3,2},{4,5},{5,4},{6,7},{7,6},{8,9},{9,8},{10,11... | collective-permute-start | bytes 786440 | tf_op jit(solution)/shard_map/ppermute | solution.py:24
  151.5 16.7 %collective-permute-start = (bf16[16,128,128]{2,1,0:T(8,128)(2,1)}, bf16[16,128,128]{2,1,0:T(8,128)(2,1)}, u32[]{:S(2)}, u32[]{:S(2)}) collective-permute-start(bf16[16,128,128]{2,1,0:T(8,128)(2,1)} %split.12), channel_id=1, source_target_pairs={{0,128},{128,0},{1,129},{129,1},{2,130},{130,2},{3,131},{131,3},{4... | collective-permute-start | bytes 1572872 | tf_op jit(solution)/shard_map/ppermute | solution.py:24
  154.6 8.9 %collective-permute-start.8 = (bf16[16,64,128]{2,1,0:T(8,128)(2,1)}, bf16[16,64,128]{2,1,0:T(8,128)(2,1)}, u32[]{:S(2)}, u32[]{:S(2)}) collective-permute-start(bf16[16,64,128]{2,1,0:T(8,128)(2,1)} %collective-permute-done.7.refs_2_), channel_id=1, source_target_pairs={{0,6},{2,0},{4,2},{6,4},{1,7},{3,1},{5,3},{7,5},{8,14},{10,8},{12,... | collective-permute-start | bytes 786440 | tf_op jit(solution)/shard_map/ppermute | solution.py:24
  160.0 9.6 %collective-permute-start.11 = (bf16[16,64,128]{2,1,0:T(8,128)(2,1)}, bf16[16,64,128]{2,1,0:T(8,128)(2,1)}, u32[]{:S(2)}, u32[]{:S(2)}) collective-permute-start(bf16[16,64,128]{2,1,0:T(8,128)(2,1)} %collective-permute-done.7.refs_2_), channel_id=1, source_target_pairs={{0,1},{1,0},{2,3},{3,2},{4,5},{5,4},{6,7},{7,6},{8,9},{9,8},{10,11... | collective-permute-start | bytes 786440 | tf_op jit(solution)/shard_map/ppermute | solution.py:24
  163.5 6.8 %collective-permute-start.10 = (bf16[16,64,128]{2,1,0:T(8,128)(2,1)}, bf16[16,64,128]{2,1,0:T(8,128)(2,1)}, u32[]{:S(2)}, u32[]{:S(2)}) collective-permute-start(bf16[16,64,128]{2,1,0:T(8,128)(2,1)} %collective-permute-done.6.refs_1_), channel_id=1, source_target_pairs={{0,1},{1,0},{2,3},{3,2},{4,5},{5,4},{6,7},{7,6},{8,9},{9,8},{10,11... | collective-permute-start | bytes 786440 | tf_op jit(solution)/shard_map/ppermute | solution.py:24
  166.0 23.6 %collective-permute-start.2 = (bf16[16,64,256]{2,1,0:T(8,128)(2,1)S(1)}, bf16[16,64,256]{2,1,0:T(8,128)(2,1)S(1)}, u32[]{:S(2)}, u32[]{:S(2)}) collective-permute-start(bf16[16,64,256]{2,1,0:T(8,128)(2,1)S(1)} %all-to-all-done.2), channel_id=1, source_target_pairs={{0,128},{128,0},{1,129},{129,1},{2,130},{130,2},{3,131},{131,3},{4... | collective-permute-start | bytes 1572872 | tf_op jit(solution)/shard_map/ppermute | solution.py:24
  168.2 8.4 %collective-permute-start.27 = (bf16[512,128]{1,0:T(8,128)(2,1)S(1)}, bf16[512,128]{1,0:T(8,128)(2,1)S(1)}, u32[]{:S(2)}, u32[]{:S(2)}) collective-permute-start(bf16[512,128]{1,0:T(8,128)(2,1)S(1)} %shard_map.105.refs_0_), channel_id=1, source_target_pairs={{0,2},{2,4},{4,6},{6,0},{1,3},{3,5},{5,7},{7,1},{8,10},{10,12},{12... | collective-permute-start | bytes 393224 | tf_op jit(solution)/shard_map/ppermute | solution.py:24
  169.6 7.0 %collective-permute-start.28 = (bf16[512,128]{1,0:T(8,128)(2,1)S(1)}, bf16[512,128]{1,0:T(8,128)(2,1)S(1)}, u32[]{:S(2)}, u32[]{:S(2)}) collective-permute-start(bf16[512,128]{1,0:T(8,128)(2,1)S(1)} %shard_map.105.refs_0_), channel_id=1, source_target_pairs={{0,6},{2,0},{4,2},{6,4},{1,7},{3,1},{5,3},{7,5},{8,14},{10,8},{12,... | collective-permute-start | bytes 393224 | tf_op jit(solution)/shard_map/ppermute | solution.py:24
  170.3 7.8 %collective-permute-start.30 = (bf16[512,128]{1,0:T(8,128)(2,1)S(1)}, bf16[512,128]{1,0:T(8,128)(2,1)S(1)}, u32[]{:S(2)}, u32[]{:S(2)}) collective-permute-start(bf16[512,128]{1,0:T(8,128)(2,1)S(1)} %shard_map.105.refs_0_), channel_id=1, source_target_pairs={{0,1},{1,0},{2,3},{3,2},{4,5},{5,4},{6,7},{7,6},{8,9},{9,8},{10,11... | collective-permute-start | bytes 393224 | tf_op jit(solution)/shard_map/ppermute | solution.py:24
  176.6 9.5 %collective-permute-start.29 = (bf16[512,128]{1,0:T(8,128)(2,1)S(1)}, bf16[512,128]{1,0:T(8,128)(2,1)S(1)}, u32[]{:S(2)}, u32[]{:S(2)}) collective-permute-start(bf16[512,128]{1,0:T(8,128)(2,1)S(1)} %collective-permute-done.27.refs_1_), channel_id=1, source_target_pairs={{0,2},{2,4},{4,6},{6,0},{1,3},{3,5},{5,7},{7,1},{8,10},{10,12},{12... | collective-permute-start | bytes 393224 | tf_op jit(solution)/shard_map/ppermute | solution.py:24
  178.1 8.0 %collective-permute-start.31 = (bf16[512,128]{1,0:T(8,128)(2,1)S(1)}, bf16[512,128]{1,0:T(8,128)(2,1)S(1)}, u32[]{:S(2)}, u32[]{:S(2)}) collective-permute-start(bf16[512,128]{1,0:T(8,128)(2,1)S(1)} %collective-permute-done.27.refs_1_), channel_id=1, source_target_pairs={{0,1},{1,0},{2,3},{3,2},{4,5},{5,4},{6,7},{7,6},{8,9},{9,8},{10,11... | collective-permute-start | bytes 393224 | tf_op jit(solution)/shard_map/ppermute | solution.py:24
  192.3 41.9 %all-to-all-start.3 = ((bf16[16,2,32,256]{3,2,1,0:T(8,128)(2,1)}), bf16[16,2,32,256]{3,2,1,0:T(8,128)(2,1)}, u32[]{:S(2)}, u32[]{:S(2)}) async-start(bf16[16,2,32,256]{3,2,1,0:T(8,128)(2,1)} %copy-done.4), calls=%async_computation.3 | async-start | bytes 1048576 | tf_op jit(solution)/shard_map/all_to_all | solution.py:324
  (25 other events, 192.0 us)

commit v5 on v4

--- a/solution.py
+++ b/solution.py
@@ -13,6 +13,7 @@
 F32 = jnp.float32
 LANES = 128
 META = 8
+PAIR = 2
 LIMIT = pltpu.CompilerParams(vmem_limit_bytes=14 * 2**20)
 
 VM = pl.BlockSpec(memory_space=pltpu.VMEM)
@@ -63,21 +64,25 @@
     ]
 
 
-def pack_first(tokens, route_ids, gain, gate, n, count, groups):
+def pack_first(tokens, route_ids, gain, gate, up, n, count, groups):
     tokens_n, model = tokens.shape
     _, whole, cols = gate.shape
     size = whole // count
     width = model // lax.axis_size(TP)
     part = tokens_n // groups
     members = n // groups
-    each = part // members
+    each = part // PAIR
     pieces = width // LANES
     gain_rows = gain.shape[1]
 
-    def body(tok_ref, ids_ref, gain_ref, gate_ref, out_ref, buf_ref, sem):
-        start = pl.multiple_of(lax.axis_index("grp") * size, size)
-        copy = pltpu.make_async_copy(gate_ref.at[:, pl.ds(start, size), :], buf_ref, sem)
-        copy.start()
+    def body(tok_ref, ids_ref, gain_ref, gate_ref, up_ref, out_ref, buf_ref, sems):
+        share_of = pl.ds(pl.multiple_of(lax.axis_index("grp") * size, size), size)
+        copies = [
+            pltpu.make_async_copy(ref.at[:, share_of, :], buf_ref.at[i], sems.at[i])
+            for i, ref in enumerate((gate_ref, up_ref))
+        ]
+        for c in copies:
+            c.start()
         tok = tok_ref[...].astype(F32)
         scale = lax.rsqrt(jnp.mean(tok * tok, axis=1, keepdims=True) + 1e-06)
         at = pl.multiple_of(lax.axis_index(TP) * width, width)
@@ -94,14 +99,14 @@
         named = [jnp.sum(jnp.where(place, i, 0.0), axis=0, keepdims=True) for i in local]
         named = jnp.concatenate(named + [jnp.zeros((META - 2, tokens_n), F32)], axis=0)
         for j in range(n):
-            first = j * each
+            a = j // members
+            first = a * part + j % PAIR * each
             for p in range(pieces):
-                to = size + p * each
+                to = 2 * size + p * each
                 out_ref[j, to : to + each, :] = ordered[first : first + each, p * LANES : (p + 1) * LANES]
-            a = j // members
             piece = named[:, a * part : (a + 1) * part]
             piece = jnp.concatenate([piece, jnp.zeros((META, LANES - part), F32)], axis=1)
-            out_ref[j, size + pieces * each :, :] = piece.astype(BF)
+            out_ref[j, 2 * size + pieces * each :, :] = piece.astype(BF)
         column = as_column(gain_ref[...])
         if size >= gain_rows:
             column = jnp.concatenate([column] * (size // gain_rows), axis=0)
@@ -109,34 +114,31 @@
             skip = lax.axis_index("grp") * size % gain_rows
             row = iota((size, gain_rows), 1) == iota((size, gain_rows), 0) + skip
             column = jnp.sum(jnp.where(row, gain_ref[...], 0.0), axis=1, keepdims=True)
-        copy.wait()
-        for j in range(n):
-            out_ref[j, :size, :] = (buf_ref[j] * column).astype(BF)
-
-    return pl.pallas_call(
-        body,
-        out_shape=shape((n, size + pieces * each + META, cols)),
-        in_specs=[VM, VM, VM, ANY],
+        for i, c in enumerate(copies):
+            c.wait()
+            for j in range(n):
+                out_ref[j, i * size : (i + 1) * size, :] = (buf_ref[i, j] * column).astype(BF)
+
+    return pl.pallas_call(
+        body,
+        out_shape=shape((n, 2 * size + pieces * each + META, cols)),
+        in_specs=[VM, VM, VM, ANY, ANY],
         out_specs=VM,
-        scratch_shapes=[pltpu.VMEM((n, size, cols), F32), pltpu.SemaphoreType.DMA],
-    )(tokens, route_ids.T, gain, gate)
-
-
-def select_rows(blocks, named, per_device, capacity):
-    members = len(blocks)
+        scratch_shapes=[pltpu.VMEM((2, n, size, cols), F32), pltpu.SemaphoreType.DMA((2,))],
+    )(tokens, route_ids.T, gain, gate, up)
+
+
+def select_rows(blocks, named, members, pieces, per_device, capacity):
     n, tall, _ = blocks[0].shape
-    pieces = 2 * LANES // LANES
     each = tall // pieces
-    part = members * each
+    part = PAIR * each
 
     def body(*refs):
-        ins, (named_ref, *outs) = (refs[:members], refs[members : members + 1 + per_device])
+        ins, (named_ref, *outs) = (refs[:PAIR], refs[PAIR : PAIR + 1 + per_device])
         row_ref = refs[-1]
         here = lax.axis_index("fs") % members
-        for k in range(members):
-            back = here - k
-            back = jnp.where(back < 0, back + members, back)
-            to = pl.ds(pl.multiple_of(back * each, each), each)
+        for k in range(PAIR):
+            to = pl.ds(pl.multiple_of((here + k) % PAIR * each, each), each)
             for p in range(pieces):
                 row_ref[:, to, p * LANES : (p + 1) * LANES] = ins[k][:, p * each : (p + 1) * each, :]
         named_rows = named_ref[...].astype(F32)
@@ -163,7 +165,7 @@
     return pl.pallas_call(
         body,
         out_shape=tuple(held((n, pieces * capacity, LANES)) for _ in range(per_device)),
-        in_specs=[VM] * (members + 1),
+        in_specs=[VM] * (PAIR + 1),
         out_specs=tuple(VM for _ in range(per_device)),
         compiler_params=LIMIT,
         scratch_shapes=[pltpu.VMEM((n, part, pieces * LANES), BF)],
@@ -188,21 +190,24 @@
     ]
 
 
-def first_matmuls(blocks, gate, up, capacity):
+def first_matmuls(blocks, weights, capacity):
     n, tall, _ = blocks[0].shape
     pieces = tall // capacity
     width = pieces * LANES
-    depth, cols = gate.shape
+    _, both_rows, cols = weights.shape
+    each = both_rows // 2
+    depth = n * each
     rows = n * capacity
     count = len(blocks)
 
     def body(*refs):
-        ins, (gate_ref, up_ref, out_ref, in_buf, w_buf) = (refs[:count], refs[count:])
+        ins, (weight_ref, out_ref, in_buf, w_buf) = (refs[:count], refs[count:])
         for i, tp in enumerate(places_of()):
-            d = pl.ds(pl.multiple_of(tp * width, width), width)
-            to = slice(i * width, (i + 1) * width)
-            w_buf[to, :cols] = gate_ref[d, :]
-            w_buf[to, cols:] = up_ref[d, :]
+            for q in range(width // each):
+                to = slice(i * width + q * each, i * width + (q + 1) * each)
+                from_fs = tp * (width // each) + q
+                w_buf[to, :cols] = weight_ref[from_fs, :each, :]
+                w_buf[to, cols:] = weight_ref[from_fs, each:, :]
             for p in range(pieces):
                 lanes = slice(i * width + p * LANES, i * width + (p + 1) * LANES)
                 in_buf[:, lanes] = ins[i][:, p * capacity : (p + 1) * capacity, :].reshape(rows, LANES)
@@ -213,11 +218,11 @@
     return pl.pallas_call(
         body,
         out_shape=held((rows, cols)),
-        in_specs=[VM] * (count + 2),
+        in_specs=[VM] * (count + 1),
         out_specs=VM,
         compiler_params=LIMIT,
         scratch_shapes=[pltpu.VMEM((rows, depth), BF), pltpu.VMEM((depth, 2 * cols), BF)],
-    )(*near_core([*blocks, gate, up]))
+    )(*near_core([*blocks, weights]))
 
 
 def second_matmul(blocks, down, n, k, per_device, done):
@@ -252,20 +257,38 @@
     )(*near_core([*blocks, down, *done]))
 
 
-def combine(returned, route_ids, route_weights, capacity):
-    rows, cols = (route_ids.shape[0], returned.shape[1])
-    slots = returned.shape[0]
-
-    def body(ret_ref, ids_ref, w_ref, out_ref):
-        total = jnp.zeros((rows, cols), F32)
+def weigh(route_ids, route_weights, slots, capacity):
+    rows = route_ids.shape[0]
+
+    def body(ids_ref, w_ref, out_ref):
+        lane = iota((rows, slots), 1)
+        total = jnp.zeros((rows, slots), F32)
         for r, slot in enumerate(slot_of(ids_ref, capacity)):
-            pick = (iota((rows, slots), 1) == slot).astype(BF)
-            total = total + dot(pick, ret_ref[...]) * as_column(w_ref[r : r + 1, :])
-        out_ref[...] = total.astype(BF)
-
-    return pl.pallas_call(
-        body, out_shape=shape((rows, cols)), in_specs=[VM] * 3, out_specs=VM, compiler_params=LIMIT
-    )(*near_core([returned, route_ids.T, route_weights.T]))
+            total = jnp.where(lane == slot, as_column(w_ref[r : r + 1, :]), total)
+        high = total.astype(BF)
+        out_ref[0] = high
+        out_ref[1] = (total - high.astype(F32)).astype(BF)
+
+    return pl.pallas_call(
+        body,
+        out_shape=held((2, rows, slots)),
+        in_specs=[VM] * 2,
+        out_specs=VM,
+        compiler_params=LIMIT,
+    )(route_ids.T, route_weights.T)
+
+
+def combine(returned, picks):
+    def body(ret_ref, pick_ref, out_ref):
+        out_ref[...] = (dot(pick_ref[0], ret_ref[...]) + dot(pick_ref[1], ret_ref[...])).astype(BF)
+
+    return pl.pallas_call(
+        body,
+        out_shape=shape((picks.shape[1], returned.shape[1])),
+        in_specs=[VM] * 2,
+        out_specs=VM,
+        compiler_params=LIMIT,
+    )(*near_core([returned, picks]))
 
 
 def by_target(master, n):
@@ -301,13 +324,15 @@
     return buffer.reshape(per_device, -1, cols)
 
 
-def one_by_one(pieces, served, index, count, per_device):
+def one_by_one(pieces, served, index, count, n, per_device):
     if count == per_device:
-        return [p.reshape(-1, p.shape[-1]) for _, p in sorted(pieces, key=lambda q: q[0])]
-    return [
-        lax.dynamic_index_in_dim(served, (index + per_device - k) % per_device, 0, False)
-        for k in range(per_device)
-    ]
+        return [p for _, p in sorted(pieces, key=lambda q: q[0])]
+    out = []
+    for k in range(per_device):
+        e = (index + per_device - k) % per_device
+        own = [lax.dynamic_index_in_dim(m, e, 0, False) for m in served]
+        out.append(jnp.concatenate([m.reshape(n, -1, m.shape[-1]) for m in own], axis=1))
+    return out
 
 
 def on_device(tokens, route_ids, route_weights, ffn_gain, gate_master, up_master, down_master):
@@ -318,46 +343,45 @@
     groups = experts // GROUP_SIZE
     members = n // groups
     capacity = tokens.shape[0] // (2 * groups)
+    pieces = tokens.shape[1] // lax.axis_size(TP) // LANES
     size = per_device * rows // count
 
     def swap(x):
         return lax.all_to_all(x, "fs", split_axis=0, concat_axis=0, tiled=True)
 
-    def neighbour(x, k):
-        pairs = [(i, i - i % members + (i + k) % members) for i in range(n)]
-        return lax.ppermute(x, "fs", pairs)
-
     packed = pack_first(
-        tokens, route_ids, ffn_gain[None, :], by_target(gate_master, n), n, count, groups
+        tokens,
+        route_ids,
+        ffn_gain[None, :],
+        by_target(gate_master, n),
+        by_target(up_master, n),
+        n,
+        count,
+        groups,
     )
     packed = swap(packed)
-    gate, near, named = jnp.split(packed, [size, packed.shape[1] - META], axis=1)
-    near = [near] + [neighbour(near, k) for k in range(1, members)]
-    if size < rows:
-        gain = lax.dynamic_slice_in_dim(ffn_gain, index * size % rows, size)
-    else:
-        gain = jnp.concatenate([ffn_gain] * (size // rows))
-    up = swap((share(up_master, index, count, n) * gain[None, :, None]).astype(BF))
-    chosen = select_rows(near, named, per_device, capacity)
+    both, own, named = jnp.split(packed, [2 * size, packed.shape[1] - META], axis=1)
+    other = lax.ppermute(own, "fs", [(i, i - i % PAIR + (i + 1) % PAIR) for i in range(n)])
+    chosen = select_rows([own, other], named, members, pieces, per_device, capacity)
     down = swap(share(down_master, index, count, n).astype(BF))
-    gate = ring(gate, "grp")
-    up = ring(up, "grp")
+    both = ring(both, "grp")
     down = ring(down, "grp")
-    gate_serve = assemble(gate, index, count, per_device)
-    up_serve = assemble(up, index, count, per_device)
+    gate_serve = assemble([(k, p[:, :size]) for k, p in both], index, count, per_device)
+    up_serve = assemble([(k, p[:, size:]) for k, p in both], index, count, per_device)
     down_serve = assemble(down, index, count, per_device)
-    gates = one_by_one(gate, gate_serve, index, count, per_device)
-    ups = one_by_one(up, up_serve, index, count, per_device)
-    downs = one_by_one(down, down_serve, index, count, per_device)
+    firsts = one_by_one(both, [gate_serve, up_serve], index, count, n, per_device)
+    seconds = one_by_one(down, [down_serve], index, count, n, per_device)
     outs = []
     for k in range(per_device):
         blocks = gather_tp(chosen[k], k % 2)
-        hidden = first_matmuls(blocks, gates[k], ups[k], capacity)
+        hidden = first_matmuls(blocks, firsts[k], capacity)
         hidden = gather_tp(hidden, k % 2)
         last = k == per_device - 1
-        outs.append(second_matmul(hidden, downs[k], n, k, per_device, outs if last else []))
+        weights = seconds[k].reshape(-1, seconds[k].shape[-1])
+        outs.append(second_matmul(hidden, weights, n, k, per_device, outs if last else []))
+    picks = weigh(route_ids, route_weights, experts * capacity, capacity)
     out = swap(outs[-1])
-    mixed = combine(out.reshape(-1, out.shape[-1]), route_ids, route_weights, capacity)
+    mixed = combine(out.reshape(-1, out.shape[-1]), picks)
     return (gate_serve, up_serve, down_serve, mixed)
 
 

time: 239 us -> 229 us (0.958)
  starting transfers between devices: 84 us -> 69 us
  waiting for transfers between devices: 122 us -> 128 us
    all_to_all x4 -> x3, starting transfers between devices: 50.9 us -> 42.1 us  [swap(): return lax.all_to_all(x, 'fs', split_axis=0, concat_axis=0, tiled=True)]
    unnamed x22 -> x12, local copies, waits for them, and re-layouts: 4.98 us -> 1 us
    ppermute x3 -> x1, starting transfers between devices: 5.54 us -> 1.84 us  [on_device(): lax.ppermute(own, 'fs', [(i, i - i % PAIR + (i + 1) % PAIR) for i in rang...]
    ppermute x31 -> x30, waiting for transfers between devices: 15.5 us -> 19.1 us  [shift(): return lax.ppermute(x, axis, [(i, (i + k) % n) for i in range(n)])]
    ppermute x31 -> x30, starting transfers between devices: 27.5 us -> 25.1 us  [shift(): return lax.ppermute(x, axis, [(i, (i + k) % n) for i in range(n)])]
    dynamic_update_slice x6 -> x5, local copies, waits for them, and re-layouts: 4.03 us -> 6.15 us  [assemble(): buffer = lax.dynamic_update_slice(buffer, piece[None], (at, 0, 0, 0))]
    ppermute x3 -> x1, waiting for transfers between devices: 25.7 us -> 26.8 us  [on_device(): lax.ppermute(own, 'fs', [(i, i - i % PAIR + (i + 1) % PAIR) for i in rang...]
    pallas_call x2 -> x3, Pallas kernels: 5.86 us -> 6.95 us  [the longest x1 4.1 us: pack_first(): pl.pallas_call(body, out_shape=shape((n, 2 * size + pieces * each + META,...]
  transfers between devices with their start and end apart: 38 -> 34, of which waited for: 16 -> 13; matrix products, arithmetic and copies ran while one was open for 4% -> 6% of each run, Pallas kernels for 4% -> 3%
where the time goes in v5:
time: 229 us; the launch traced here: 227 us
  waiting for transfers between devices  128 us (56%)
  starting transfers between devices  69 us (30%)
  local copies, waits for them, and re-layouts  14.7 us (6%)
  Pallas kernels  14 us (6%)
    all_to_all x3, waiting for transfers between devices, swap(): return lax.all_to_all(x, 'fs', split_axis=0, concat_axis=0, tiled=True)  82.1 us
    all_to_all x3, starting transfers between devices, swap(): return lax.all_to_all(x, 'fs', split_axis=0, concat_axis=0, tiled=True)  42.1 us
    ppermute x1, waiting for transfers between devices, on_device(): lax.ppermute(own, 'fs', [(i, i - i % PAIR + (i + 1) % PAIR) for i in rang...  26.8 us
    ppermute x30, starting transfers between devices, shift(): return lax.ppermute(x, axis, [(i, (i + k) % n) for i in range(n)])  25.1 us
    ppermute x30, waiting for transfers between devices, shift(): return lax.ppermute(x, axis, [(i, (i + k) % n) for i in range(n)])  19.1 us
    dynamic_update_slice x5, local copies, waits for them, and re-layouts, assemble(): buffer = lax.dynamic_update_slice(buffer, piece[None], (at, 0, 0, 0))  6.15 us
    pallas_call x2, Pallas kernels, first_matmuls(): pl.pallas_call(body, out_shape=held((rows, cols)), in_specs=[VM] * (count...  4.85 us
  transfers between devices with their start and end apart: 34, of which 13 were waited for; matrix products, arithmetic and copies ran while one was open for 6% of the time, Pallas kernels for 3%

profile of v5, /device:TPU:34, one launch (start us, length us, event | category | flops | bytes accessed | tf_op | source)
XLA Modules:
  0.0 226.6 jit_solution(5854552828546139274)
XLA Ops:
  0.6 4.1 %shard_map.102 = bf16[16,328,128]{2,1,0:T(8,128)(2,1)} custom-call(bf16[256,2048]{1,0:T(8,128)(2,1)} %tok_ref.1, s32[2,256]{1,0:T(2,128)} %bitcast.35, f32[1,128]{1,0:T(1,128)} %bitcast.41, f32[16,256,128]{2,1,0:T(8,128)} %bitcast.38, f32[16,256,128]{2,1,0:T(8,128)} %bitcast.39), custom_call_target="tpu_custom_call" | custom-call | tf_op jit(solution)/shard_map/pallas_call | solution.py:122
  4.8 24.0 %all-to-all-start = ((bf16[16,328,128]{2,1,0:T(8,128)(2,1)}), bf16[16,328,128]{2,1,0:T(8,128)(2,1)}, u32[]{:S(2)}, u32[]{:S(2)}) async-start(bf16[16,328,128]{2,1,0:T(8,128)(2,1)} %shard_map.102), calls=%async_computation | async-start | bytes 2686976 | tf_op jit(solution)/shard_map/all_to_all | solution.py:350
  29.6 63.5 %all-to-all-done = bf16[16,328,128]{2,1,0:T(8,128)(2,1)} async-done(((bf16[16,328,128]{2,1,0:T(8,128)(2,1)}), bf16[16,328,128]{2,1,0:T(8,128)(2,1)}, u32[]{:S(2)}, u32[]{:S(2)}) %all-to-all-start) | async-done | bytes 1343520 | tf_op jit(solution)/shard_map/all_to_all | solution.py:350
  93.1 6.3 %all-to-all-start.1 = ((bf16[16,64,256]{2,1,0:T(8,128)(2,1)}), bf16[16,64,256]{2,1,0:T(8,128)(2,1)S(1)}, u32[]{:S(2)}, u32[]{:S(2)}) async-start(bf16[16,64,256]{2,1,0:T(8,128)(2,1)} %dynamic-slice_convert_fusion), calls=%async_computation.1 | async-start | bytes 1048576 | tf_op jit(solution)/shard_map/all_to_all | solution.py:350
  103.0 26.8 %collective-permute-done.2.refs_1_ = bf16[16,64,128]{2,1,0:T(8,128)(2,1)S(1)} collective-permute-done((bf16[16,64,128]{2,1,0:T(8,128)(2,1)S(1)}, bf16[16,64,128]{2,1,0:T(8,128)(2,1)S(1)}, u32[]{:S(2)}, u32[]{:S(2)}) %collective-permute-start.2) | collective-permute-done | bytes 262176 | tf_op jit(solution)/shard_map/ppermute | solution.py:364
  132.0 2.3 %split.12.refs_8_ = bf16[16,256,128]{2,1,0:T(8,128)(2,1)} slice(bf16[16,328,128]{2,1,0:T(8,128)(2,1)} %all-to-all-done), slice={[0:16], [0:256], [0:128]} | slice | bytes 2097152 | tf_op jit(solution)/shard_map/split | solution.py:363
  134.7 2.1 collective-permute-start
  139.3 3.4 %collective-permute-done.18.refs_2_ = bf16[16,64,128]{2,1,0:T(8,128)(2,1)S(1)} collective-permute-done((bf16[16,64,128]{2,1,0:T(8,128)(2,1)S(1)}, bf16[16,64,128]{2,1,0:T(8,128)(2,1)S(1)}, u32[]{:S(2)}, u32[]{:S(2)}) %collective-permute-start.18) | collective-permute-done | bytes 262176 | tf_op jit(solution)/shard_map/ppermute | solution.py:25
  143.8 3.3 %collective-permute-done.4.refs_2_ = bf16[16,64,128]{2,1,0:T(8,128)(2,1)} collective-permute-done((bf16[16,64,128]{2,1,0:T(8,128)(2,1)S(1)}, bf16[16,64,128]{2,1,0:T(8,128)(2,1)}, u32[]{:S(2)}, u32[]{:S(2)}) %collective-permute-start.4) | collective-permute-done | bytes 262176 | tf_op jit(solution)/shard_map/ppermute | solution.py:25
  147.7 3.2 %collective-permute-start.5 = (bf16[16,64,128]{2,1,0:T(8,128)(2,1)}, bf16[16,64,128]{2,1,0:T(8,128)(2,1)}, u32[]{:S(2)}, u32[]{:S(2)}) collective-permute-start(bf16[16,64,128]{2,1,0:T(8,128)(2,1)} %collective-permute-done.4.refs_2_), channel_id=1, source_target_pairs={{0,6},{2,0},{4,2},{6,4},{1,7},{3,1},{5,3},{7,5},{8,14},{10,8},{12,... | collective-permute-start | bytes 786440 | tf_op jit(solution)/shard_map/ppermute | solution.py:25
  153.4 2.8 %collective-permute-done.5.refs_3_ = bf16[16,64,128]{2,1,0:T(8,128)(2,1)} collective-permute-done((bf16[16,64,128]{2,1,0:T(8,128)(2,1)}, bf16[16,64,128]{2,1,0:T(8,128)(2,1)}, u32[]{:S(2)}, u32[]{:S(2)}) %collective-permute-start.5) | collective-permute-done | bytes 262176 | tf_op jit(solution)/shard_map/ppermute | solution.py:25
  156.6 2.1 shard_map.105.refs_0_
  158.8 2.2 collective-permute-start.1
  163.1 2.7 %shard_map.104.refs_0_ = bf16[512,128]{1,0:T(8,128)(2,1)S(1)} custom-call(bf16[16,64,128]{2,1,0:T(8,128)(2,1)S(1)} %get-tuple-element.6.refs_0_, bf16[16,64,128]{2,1,0:T(8,128)(2,1)} %collective-permute-done.3.refs_1_, bf16[16,64,128]{2,1,0:T(8,128)(2,1)} %collective-permute-done.4.refs_2_, bf16[16,64,128]{2,1,0:T(8,128)(2,1)} %collective-permute-done.5.refs_3_, ...), custom_call_target="tpu_custom_call" | custom-call | tf_op jit(solution)/shard_map/pallas_call | solution.py:218
  165.8 2.9 %collective-permute-start.11 = (bf16[512,128]{1,0:T(8,128)(2,1)S(1)}, bf16[512,128]{1,0:T(8,128)(2,1)S(1)}, u32[]{:S(2)}, u32[]{:S(2)}) collective-permute-start(bf16[512,128]{1,0:T(8,128)(2,1)S(1)} %shard_map.104.refs_0_), channel_id=1, source_target_pairs={{0,6},{2,0},{4,2},{6,4},{1,7},{3,1},{5,3},{7,5},{8,14},{10,8},{12,... | collective-permute-start | bytes 393224 | tf_op jit(solution)/shard_map/ppermute | solution.py:25
  170.2 2.0 collective-permute-done.11.refs_2_
  172.2 2.8 %collective-permute-done.10.refs_1_ = bf16[512,128]{1,0:T(8,128)(2,1)S(1)} collective-permute-done((bf16[512,128]{1,0:T(8,128)(2,1)S(1)}, bf16[512,128]{1,0:T(8,128)(2,1)S(1)}, u32[]{:S(2)}, u32[]{:S(2)}) %collective-permute-start.10) | collective-permute-done | bytes 131104 | tf_op jit(solution)/shard_map/ppermute | solution.py:25
  175.0 3.1 %collective-permute-start.12 = (bf16[512,128]{1,0:T(8,128)(2,1)S(1)}, bf16[512,128]{1,0:T(8,128)(2,1)S(1)}, u32[]{:S(2)}, u32[]{:S(2)}) collective-permute-start(bf16[512,128]{1,0:T(8,128)(2,1)S(1)} %collective-permute-done.11.refs_2_), channel_id=1, source_target_pairs={{0,6},{2,0},{4,2},{6,4},{1,7},{3,1},{5,3},{7,5},{8,14},{10,8},{12,... | collective-permute-start | bytes 393224 | tf_op jit(solution)/shard_map/ppermute | solution.py:25
  183.5 11.7 %all-to-all-start.2 = ((bf16[16,2,32,256]{3,2,1,0:T(8,128)(2,1)}), bf16[16,2,32,256]{3,2,1,0:T(8,128)(2,1)}, u32[]{:S(2)}, u32[]{:S(2)}) async-start(bf16[16,2,32,256]{3,2,1,0:T(8,128)(2,1)} %shard_map.107), calls=%async_computation.2 | async-start | bytes 1048576 | tf_op jit(solution)/shard_map/all_to_all | solution.py:350
  198.6 1.9 fusion.3
  201.7 1.9 fusion.1
  203.6 2.3 %fusion = (bf16[2,16,128,128]{3,2,1,0:T(8,128)(2,1)}, bf16[2,16,128,128]{3,2,1,0:T(8,128)(2,1)}) fusion(bf16[2,16,128,128]{3,2,1,0:T(8,128)(2,1)} %fusion.1, s32[]{:T(128)S(6)} %select_n.35, bf16[16,256,128]{2,1,0:T(8,128)(2,1)} %collective-permute-done.refs_8_, bf16[2,16,128,128]{3,2,1,0:T(8,128)(2,1)} %fusion.3), kind=kLoop, calls=%fused_computation.2 | loop fusion | bytes 2097156 | tf_op jit(solution)/shard_map/dynamic_update_slice | solution.py:321
  205.9 18.6 %all-to-all-done.2 = bf16[16,2,32,256]{3,2,1,0:T(8,128)(2,1)} async-done(((bf16[16,2,32,256]{3,2,1,0:T(8,128)(2,1)}), bf16[16,2,32,256]{3,2,1,0:T(8,128)(2,1)}, u32[]{:S(2)}, u32[]{:S(2)}) %all-to-all-start.2) | async-done | bytes 524320 | tf_op jit(solution)/shard_map/all_to_all | solution.py:350
  224.5 2.1 shard_map.109
  (76 shorter events, 27.6 us)
Async XLA Ops:
  4.8 88.3 %all-to-all-start = ((bf16[16,328,128]{2,1,0:T(8,128)(2,1)}), bf16[16,328,128]{2,1,0:T(8,128)(2,1)}, u32[]{:S(2)}, u32[]{:S(2)}) async-start(bf16[16,328,128]{2,1,0:T(8,128)(2,1)} %shard_map.102), calls=%async_computation | async-start | bytes 2686976 | tf_op jit(solution)/shard_map/all_to_all | solution.py:350
  93.1 65.7 %all-to-all-start.1 = ((bf16[16,64,256]{2,1,0:T(8,128)(2,1)}), bf16[16,64,256]{2,1,0:T(8,128)(2,1)S(1)}, u32[]{:S(2)}, u32[]{:S(2)}) async-start(bf16[16,64,256]{2,1,0:T(8,128)(2,1)} %dynamic-slice_convert_fusion), calls=%async_computation.1 | async-start | bytes 1048576 | tf_op jit(solution)/shard_map/all_to_all | solution.py:350
  100.4 29.4 %collective-permute-start.2 = (bf16[16,64,128]{2,1,0:T(8,128)(2,1)S(1)}, bf16[16,64,128]{2,1,0:T(8,128)(2,1)S(1)}, u32[]{:S(2)}, u32[]{:S(2)}) collective-permute-start(bf16[16,64,128]{2,1,0:T(8,128)(2,1)S(1)} %split.13.refs_0_), channel_id=1, source_target_pairs={{0,8},{8,0},{16,24},{24,16},{32,40},{40,32},{48,56},{56,48},{64,72... | collective-permute-start | bytes 786440 | tf_op jit(solution)/shard_map/ppermute | solution.py:364
  130.3 8.2 %collective-permute-start.17 = (bf16[16,64,128]{2,1,0:T(8,128)(2,1)S(1)}, bf16[16,64,128]{2,1,0:T(8,128)(2,1)S(1)}, u32[]{:S(2)}, u32[]{:S(2)}) collective-permute-start(bf16[16,64,128]{2,1,0:T(8,128)(2,1)S(1)} %get-tuple-element.7.refs_0_), channel_id=1, source_target_pairs={{0,2},{2,4},{4,6},{6,0},{1,3},{3,5},{5,7},{7,1},{8,10},{10,12},{12... | collective-permute-start | bytes 786440 | tf_op jit(solution)/shard_map/ppermute | solution.py:25
  134.3 8.5 %collective-permute-start.18 = (bf16[16,64,128]{2,1,0:T(8,128)(2,1)S(1)}, bf16[16,64,128]{2,1,0:T(8,128)(2,1)S(1)}, u32[]{:S(2)}, u32[]{:S(2)}) collective-permute-start(bf16[16,64,128]{2,1,0:T(8,128)(2,1)S(1)} %get-tuple-element.7.refs_0_), channel_id=1, source_target_pairs={{0,6},{2,0},{4,2},{6,4},{1,7},{3,1},{5,3},{7,5},{8,14},{10,8},{12,... | collective-permute-start | bytes 786440 | tf_op jit(solution)/shard_map/ppermute | solution.py:25
  134.7 28.4 %collective-permute-start = (bf16[16,256,128]{2,1,0:T(8,128)(2,1)}, bf16[16,256,128]{2,1,0:T(8,128)(2,1)}, u32[]{:S(2)}, u32[]{:S(2)}) collective-permute-start(bf16[16,256,128]{2,1,0:T(8,128)(2,1)} %split.12.refs_8_), channel_id=1, source_target_pairs={{0,128},{128,0},{1,129},{129,1},{2,130},{130,2},{3,131},{131,3},{4... | collective-permute-start | bytes 3145736 | tf_op jit(solution)/shard_map/ppermute | solution.py:25
  136.8 7.0 %collective-permute-start.20 = (bf16[16,64,128]{2,1,0:T(8,128)(2,1)S(1)}, bf16[16,64,128]{2,1,0:T(8,128)(2,1)S(1)}, u32[]{:S(2)}, u32[]{:S(2)}) collective-permute-start(bf16[16,64,128]{2,1,0:T(8,128)(2,1)S(1)} %get-tuple-element.7.refs_0_), channel_id=1, source_target_pairs={{0,1},{1,0},{2,3},{3,2},{4,5},{5,4},{6,7},{7,6},{8,9},{9,8},{10,11... | collective-permute-start | bytes 786440 | tf_op jit(solution)/shard_map/ppermute | solution.py:25
  136.8 10.2 %collective-permute-start.4 = (bf16[16,64,128]{2,1,0:T(8,128)(2,1)S(1)}, bf16[16,64,128]{2,1,0:T(8,128)(2,1)}, u32[]{:S(2)}, u32[]{:S(2)}) collective-permute-start(bf16[16,64,128]{2,1,0:T(8,128)(2,1)S(1)} %get-tuple-element.6.refs_0_), channel_id=1, source_target_pairs={{0,6},{2,0},{4,2},{6,4},{1,7},{3,1},{5,3},{7,5},{8,14},{10,8},{12,... | collective-permute-start | bytes 786440 | tf_op jit(solution)/shard_map/ppermute | solution.py:25
  138.4 9.3 %collective-permute-start.3 = (bf16[16,64,128]{2,1,0:T(8,128)(2,1)S(1)}, bf16[16,64,128]{2,1,0:T(8,128)(2,1)}, u32[]{:S(2)}, u32[]{:S(2)}) collective-permute-start(bf16[16,64,128]{2,1,0:T(8,128)(2,1)S(1)} %get-tuple-element.6.refs_0_), channel_id=1, source_target_pairs={{0,2},{2,4},{4,6},{6,0},{1,3},{3,5},{5,7},{7,1},{8,10},{10,12},{12... | collective-permute-start | bytes 786440 | tf_op jit(solution)/shard_map/ppermute | solution.py:25
  142.8 9.9 %collective-permute-start.19 = (bf16[16,64,128]{2,1,0:T(8,128)(2,1)S(1)}, bf16[16,64,128]{2,1,0:T(8,128)(2,1)S(1)}, u32[]{:S(2)}, u32[]{:S(2)}) collective-permute-start(bf16[16,64,128]{2,1,0:T(8,128)(2,1)S(1)} %collective-permute-done.17.refs_1_), channel_id=1, source_target_pairs={{0,2},{2,4},{4,6},{6,0},{1,3},{3,5},{5,7},{7,1},{8,10},{10,12},{12... | collective-permute-start | bytes 786440 | tf_op jit(solution)/shard_map/ppermute | solution.py:25
  143.8 8.9 %collective-permute-start.21 = (bf16[16,64,128]{2,1,0:T(8,128)(2,1)S(1)}, bf16[16,64,128]{2,1,0:T(8,128)(2,1)S(1)}, u32[]{:S(2)}, u32[]{:S(2)}) collective-permute-start(bf16[16,64,128]{2,1,0:T(8,128)(2,1)S(1)} %collective-permute-done.17.refs_1_), channel_id=1, source_target_pairs={{0,1},{1,0},{2,3},{3,2},{4,5},{5,4},{6,7},{7,6},{8,9},{9,8},{10,11... | collective-permute-start | bytes 786440 | tf_op jit(solution)/shard_map/ppermute | solution.py:25
  147.7 8.4 %collective-permute-start.5 = (bf16[16,64,128]{2,1,0:T(8,128)(2,1)}, bf16[16,64,128]{2,1,0:T(8,128)(2,1)}, u32[]{:S(2)}, u32[]{:S(2)}) collective-permute-start(bf16[16,64,128]{2,1,0:T(8,128)(2,1)} %collective-permute-done.4.refs_2_), channel_id=1, source_target_pairs={{0,6},{2,0},{4,2},{6,4},{1,7},{3,1},{5,3},{7,5},{8,14},{10,8},{12,... | collective-permute-start | bytes 786440 | tf_op jit(solution)/shard_map/ppermute | solution.py:25
  153.2 7.8 %collective-permute-start.8 = (bf16[16,64,128]{2,1,0:T(8,128)(2,1)}, bf16[16,64,128]{2,1,0:T(8,128)(2,1)}, u32[]{:S(2)}, u32[]{:S(2)}) collective-permute-start(bf16[16,64,128]{2,1,0:T(8,128)(2,1)} %collective-permute-done.4.refs_2_), channel_id=1, source_target_pairs={{0,1},{1,0},{2,3},{3,2},{4,5},{5,4},{6,7},{7,6},{8,9},{9,8},{10,11... | collective-permute-start | bytes 786440 | tf_op jit(solution)/shard_map/ppermute | solution.py:25
  156.1 7.0 %collective-permute-start.9 = (bf16[16,64,128]{2,1,0:T(8,128)(2,1)}, bf16[16,64,128]{2,1,0:T(8,128)(2,1)}, u32[]{:S(2)}, u32[]{:S(2)}) collective-permute-start(bf16[16,64,128]{2,1,0:T(8,128)(2,1)} %collective-permute-done.5.refs_3_), channel_id=1, source_target_pairs={{0,1},{1,0},{2,3},{3,2},{4,5},{5,4},{6,7},{7,6},{8,9},{9,8},{10,11... | collective-permute-start | bytes 786440 | tf_op jit(solution)/shard_map/ppermute | solution.py:25
  158.8 22.9 %collective-permute-start.1 = (bf16[16,64,256]{2,1,0:T(8,128)(2,1)S(1)}, bf16[16,64,256]{2,1,0:T(8,128)(2,1)S(1)}, u32[]{:S(2)}, u32[]{:S(2)}) collective-permute-start(bf16[16,64,256]{2,1,0:T(8,128)(2,1)S(1)} %all-to-all-done.1), channel_id=1, source_target_pairs={{0,128},{128,0},{1,129},{129,1},{2,130},{130,2},{3,131},{131,3},{4... | collective-permute-start | bytes 1572872 | tf_op jit(solution)/shard_map/ppermute | solution.py:25
  161.0 7.6 %collective-permute-start.24 = (bf16[512,128]{1,0:T(8,128)(2,1)S(1)}, bf16[512,128]{1,0:T(8,128)(2,1)S(1)}, u32[]{:S(2)}, u32[]{:S(2)}) collective-permute-start(bf16[512,128]{1,0:T(8,128)(2,1)S(1)} %shard_map.105.refs_0_), channel_id=1, source_target_pairs={{0,2},{2,4},{4,6},{6,0},{1,3},{3,5},{5,7},{7,1},{8,10},{10,12},{12... | collective-permute-start | bytes 393224 | tf_op jit(solution)/shard_map/ppermute | solution.py:25
  162.4 6.3 %collective-permute-start.25 = (bf16[512,128]{1,0:T(8,128)(2,1)S(1)}, bf16[512,128]{1,0:T(8,128)(2,1)S(1)}, u32[]{:S(2)}, u32[]{:S(2)}) collective-permute-start(bf16[512,128]{1,0:T(8,128)(2,1)S(1)} %shard_map.105.refs_0_), channel_id=1, source_target_pairs={{0,6},{2,0},{4,2},{6,4},{1,7},{3,1},{5,3},{7,5},{8,14},{10,8},{12,... | collective-permute-start | bytes 393224 | tf_op jit(solution)/shard_map/ppermute | solution.py:25
  163.1 7.2 %collective-permute-start.27 = (bf16[512,128]{1,0:T(8,128)(2,1)S(1)}, bf16[512,128]{1,0:T(8,128)(2,1)S(1)}, u32[]{:S(2)}, u32[]{:S(2)}) collective-permute-start(bf16[512,128]{1,0:T(8,128)(2,1)S(1)} %shard_map.105.refs_0_), channel_id=1, source_target_pairs={{0,1},{1,0},{2,3},{3,2},{4,5},{5,4},{6,7},{7,6},{8,9},{9,8},{10,11... | collective-permute-start | bytes 393224 | tf_op jit(solution)/shard_map/ppermute | solution.py:25
  165.8 6.4 %collective-permute-start.11 = (bf16[512,128]{1,0:T(8,128)(2,1)S(1)}, bf16[512,128]{1,0:T(8,128)(2,1)S(1)}, u32[]{:S(2)}, u32[]{:S(2)}) collective-permute-start(bf16[512,128]{1,0:T(8,128)(2,1)S(1)} %shard_map.104.refs_0_), channel_id=1, source_target_pairs={{0,6},{2,0},{4,2},{6,4},{1,7},{3,1},{5,3},{7,5},{8,14},{10,8},{12,... | collective-permute-start | bytes 393224 | tf_op jit(solution)/shard_map/ppermute | solution.py:25
  168.7 6.4 %collective-permute-start.10 = (bf16[512,128]{1,0:T(8,128)(2,1)S(1)}, bf16[512,128]{1,0:T(8,128)(2,1)S(1)}, u32[]{:S(2)}, u32[]{:S(2)}) collective-permute-start(bf16[512,128]{1,0:T(8,128)(2,1)S(1)} %shard_map.104.refs_0_), channel_id=1, source_target_pairs={{0,2},{2,4},{4,6},{6,0},{1,3},{3,5},{5,7},{7,1},{8,10},{10,12},{12... | collective-permute-start | bytes 393224 | tf_op jit(solution)/shard_map/ppermute | solution.py:25
  168.7 9.5 %collective-permute-start.26 = (bf16[512,128]{1,0:T(8,128)(2,1)S(1)}, bf16[512,128]{1,0:T(8,128)(2,1)S(1)}, u32[]{:S(2)}, u32[]{:S(2)}) collective-permute-start(bf16[512,128]{1,0:T(8,128)(2,1)S(1)} %collective-permute-done.24.refs_1_), channel_id=1, source_target_pairs={{0,2},{2,4},{4,6},{6,0},{1,3},{3,5},{5,7},{7,1},{8,10},{10,12},{12... | collective-permute-start | bytes 393224 | tf_op jit(solution)/shard_map/ppermute | solution.py:25
  170.2 7.9 %collective-permute-start.28 = (bf16[512,128]{1,0:T(8,128)(2,1)S(1)}, bf16[512,128]{1,0:T(8,128)(2,1)S(1)}, u32[]{:S(2)}, u32[]{:S(2)}) collective-permute-start(bf16[512,128]{1,0:T(8,128)(2,1)S(1)} %collective-permute-done.24.refs_1_), channel_id=1, source_target_pairs={{0,1},{1,0},{2,3},{3,2},{4,5},{5,4},{6,7},{7,6},{8,9},{9,8},{10,11... | collective-permute-start | bytes 393224 | tf_op jit(solution)/shard_map/ppermute | solution.py:25
  172.2 6.4 %collective-permute-start.29 = (bf16[512,128]{1,0:T(8,128)(2,1)S(1)}, bf16[512,128]{1,0:T(8,128)(2,1)S(1)}, u32[]{:S(2)}, u32[]{:S(2)}) collective-permute-start(bf16[512,128]{1,0:T(8,128)(2,1)S(1)} %collective-permute-done.25.refs_2_), channel_id=1, source_target_pairs={{0,1},{1,0},{2,3},{3,2},{4,5},{5,4},{6,7},{7,6},{8,9},{9,8},{10,11... | collective-permute-start | bytes 393224 | tf_op jit(solution)/shard_map/ppermute | solution.py:25
  183.5 41.0 %all-to-all-start.2 = ((bf16[16,2,32,256]{3,2,1,0:T(8,128)(2,1)}), bf16[16,2,32,256]{3,2,1,0:T(8,128)(2,1)}, u32[]{:S(2)}, u32[]{:S(2)}) async-start(bf16[16,2,32,256]{3,2,1,0:T(8,128)(2,1)} %shard_map.107), calls=%async_computation.2 | async-start | bytes 1048576 | tf_op jit(solution)/shard_map/all_to_all | solution.py:350
  (16 other events, 121.6 us)

commit v6 on v5

--- a/solution.py
+++ b/solution.py
@@ -128,6 +128,32 @@
     )(tokens, route_ids.T, gain, gate, up)
 
 
+def unpack(packed, cuts):
+    n, tall, cols = packed.shape
+    ends = [0, *cuts, tall]
+    parts = list(zip(ends[:-1], ends[1:]))
+
+    def body(packed_ref, *refs):
+        sems = refs[-1]
+        copies = [
+            pltpu.make_async_copy(packed_ref.at[:, a:b, :], refs[i], sems.at[i])
+            for i, (a, b) in enumerate(parts)
+        ]
+        for c in copies:
+            c.start()
+        for c in copies:
+            c.wait()
+
+    return pl.pallas_call(
+        body,
+        out_shape=tuple(shape((n, b - a, cols)) for a, b in parts),
+        in_specs=[ANY],
+        out_specs=tuple(VM for _ in parts),
+        compiler_params=LIMIT,
+        scratch_shapes=[pltpu.SemaphoreType.DMA((len(parts),))],
+    )(packed)
+
+
 def select_rows(blocks, named, members, pieces, per_device, capacity):
     n, tall, _ = blocks[0].shape
     each = tall // pieces
@@ -179,8 +205,9 @@
 def gather_tp(x, back):
     left, right = (shift(x, "tp_0", 1), shift(x, "tp_0", -1))
     across = shift(right, "tp_0", -1) if back else shift(left, "tp_0", 1)
-    mine = (x, left, right, across)
-    return mine + tuple(shift(b, "tp_1", 1) for b in mine)
+    mine = (x, left, right)
+    theirs = tuple(shift(b, "tp_1", 1) for b in mine)
+    return mine + (across,) + theirs + (shift(across, "tp_1", 1),)
 
 
 def places_of():
@@ -360,7 +387,7 @@
         groups,
     )
     packed = swap(packed)
-    both, own, named = jnp.split(packed, [2 * size, packed.shape[1] - META], axis=1)
+    both, own, named = unpack(packed, [2 * size, packed.shape[1] - META])
     other = lax.ppermute(own, "fs", [(i, i - i % PAIR + (i + 1) % PAIR) for i in range(n)])
     chosen = select_rows([own, other], named, members, pieces, per_device, capacity)
     down = swap(share(down_master, index, count, n).astype(BF))

time: 229 us -> 228 us (level)
    split x3 -> x0, local copies, waits for them, and re-layouts: 4.03 us -> none  [on_device(): jnp.split(packed, [2 * size, packed.shape[1] - META], axis=1)]
    unnamed x12 -> x18, local copies, waits for them, and re-layouts: 1 us -> 4.81 us
  transfers between devices with their start and end apart: 34 -> 34, of which waited for: 13 -> 13; matrix products, arithmetic and copies ran while one was open for 6% -> 4% of each run, Pallas kernels for 3% -> 4%
where the time goes in v6:
time: 228 us; the launch traced here: 227 us
  waiting for transfers between devices  129 us (57%)
  starting transfers between devices  68.1 us (30%)
  Pallas kernels  15 us (7%)
  local copies, waits for them, and re-layouts  14.2 us (6%)
    all_to_all x3, waiting for transfers between devices, swap(): return lax.all_to_all(x, 'fs', split_axis=0, concat_axis=0, tiled=True)  81.4 us
    all_to_all x3, starting transfers between devices, swap(): return lax.all_to_all(x, 'fs', split_axis=0, concat_axis=0, tiled=True)  41.7 us
    ppermute x1, waiting for transfers between devices, on_device(): lax.ppermute(own, 'fs', [(i, i - i % PAIR + (i + 1) % PAIR) for i in rang...  27.4 us
    ppermute x30, starting transfers between devices, shift(): return lax.ppermute(x, axis, [(i, (i + k) % n) for i in range(n)])  24.6 us
    ppermute x30, waiting for transfers between devices, shift(): return lax.ppermute(x, axis, [(i, (i + k) % n) for i in range(n)])  19.9 us
    dynamic_update_slice x5, local copies, waits for them, and re-layouts, assemble(): buffer = lax.dynamic_update_slice(buffer, piece[None], (at, 0, 0, 0))  5.98 us
    unnamed x18, local copies, waits for them, and re-layouts  4.81 us
  transfers between devices with their start and end apart: 34, of which 13 were waited for; matrix products, arithmetic and copies ran while one was open for 4% of the time, Pallas kernels for 4%

profile of v6, /device:TPU:34, one launch (start us, length us, event | category | flops | bytes accessed | tf_op | source)
XLA Modules:
  0.0 227.0 jit_solution(14794627241400785610)
XLA Ops:
  0.6 4.1 %shard_map.102 = bf16[16,328,128]{2,1,0:T(8,128)(2,1)} custom-call(bf16[256,2048]{1,0:T(8,128)(2,1)} %tok_ref.1, s32[2,256]{1,0:T(2,128)} %bitcast.30, f32[1,128]{1,0:T(1,128)} %bitcast.36, f32[16,256,128]{2,1,0:T(8,128)} %bitcast.33, f32[16,256,128]{2,1,0:T(8,128)} %bitcast.34), custom_call_target="tpu_custom_call" | custom-call | tf_op jit(solution)/shard_map/pallas_call | solution.py:122
  4.8 24.0 %all-to-all-start = ((bf16[16,328,128]{2,1,0:T(8,128)(2,1)}), bf16[16,328,128]{2,1,0:T(8,128)(2,1)S(1)}, u32[]{:S(2)}, u32[]{:S(2)}) async-start(bf16[16,328,128]{2,1,0:T(8,128)(2,1)} %shard_map.102), calls=%async_computation | async-start | bytes 2686976 | tf_op jit(solution)/shard_map/all_to_all | solution.py:377
  29.7 63.7 %all-to-all-done.packed_ref = bf16[16,328,128]{2,1,0:T(8,128)(2,1)S(1)} async-done(((bf16[16,328,128]{2,1,0:T(8,128)(2,1)}), bf16[16,328,128]{2,1,0:T(8,128)(2,1)S(1)}, u32[]{:S(2)}, u32[]{:S(2)}) %all-to-all-start) | async-done | bytes 1343520 | tf_op jit(solution)/shard_map/all_to_all | solution.py:377
  93.3 6.0 %all-to-all-start.1 = ((bf16[16,64,256]{2,1,0:T(8,128)(2,1)}), bf16[16,64,256]{2,1,0:T(8,128)(2,1)}, u32[]{:S(2)}, u32[]{:S(2)}) async-start(bf16[16,64,256]{2,1,0:T(8,128)(2,1)} %dynamic-slice_convert_fusion), calls=%async_computation.1 | async-start | bytes 1048576 | tf_op jit(solution)/shard_map/all_to_all | solution.py:377
  100.5 1.8 collective-permute-start.2
  102.4 27.4 %collective-permute-done.2.refs_1_ = bf16[16,64,128]{2,1,0:T(8,128)(2,1)S(1)} collective-permute-done((bf16[16,64,128]{2,1,0:T(8,128)(2,1)S(1)}, bf16[16,64,128]{2,1,0:T(8,128)(2,1)S(1)}, u32[]{:S(2)}, u32[]{:S(2)}) %collective-permute-start.2) | collective-permute-done | bytes 262176 | tf_op jit(solution)/shard_map/ppermute | solution.py:391
  132.3 2.1 collective-permute-start
  141.5 3.2 %collective-permute-done.4.refs_2_ = bf16[16,64,128]{2,1,0:T(8,128)(2,1)} collective-permute-done((bf16[16,64,128]{2,1,0:T(8,128)(2,1)S(1)}, bf16[16,64,128]{2,1,0:T(8,128)(2,1)}, u32[]{:S(2)}, u32[]{:S(2)}) %collective-permute-start.4) | collective-permute-done | bytes 262176 | tf_op jit(solution)/shard_map/ppermute | solution.py:25
  144.7 2.2 collective-permute-done.3.refs_1_
  147.0 3.0 %collective-permute-start.5 = (bf16[16,64,128]{2,1,0:T(8,128)(2,1)}, bf16[16,64,128]{2,1,0:T(8,128)(2,1)}, u32[]{:S(2)}, u32[]{:S(2)}) collective-permute-start(bf16[16,64,128]{2,1,0:T(8,128)(2,1)} %collective-permute-done.4.refs_2_), channel_id=1, source_target_pairs={{0,6},{2,0},{4,2},{6,4},{1,7},{3,1},{5,3},{7,5},{8,14},{10,8},{12,... | collective-permute-start | bytes 786440 | tf_op jit(solution)/shard_map/ppermute | solution.py:25
  151.0 3.2 %collective-permute-done.5.refs_3_ = bf16[16,64,128]{2,1,0:T(8,128)(2,1)} collective-permute-done((bf16[16,64,128]{2,1,0:T(8,128)(2,1)}, bf16[16,64,128]{2,1,0:T(8,128)(2,1)}, u32[]{:S(2)}, u32[]{:S(2)}) %collective-permute-start.5) | collective-permute-done | bytes 262176 | tf_op jit(solution)/shard_map/ppermute | solution.py:25
  154.7 2.1 shard_map.106.refs_0_
  156.9 2.2 collective-permute-start.1
  161.8 2.3 %shard_map.105.refs_0_ = bf16[512,128]{1,0:T(8,128)(2,1)S(1)} custom-call(bf16[16,64,128]{2,1,0:T(8,128)(2,1)S(1)} %get-tuple-element.12.refs_0_, bf16[16,64,128]{2,1,0:T(8,128)(2,1)} %collective-permute-done.3.refs_1_, bf16[16,64,128]{2,1,0:T(8,128)(2,1)} %collective-permute-done.4.refs_2_, bf16[16,64,128]{2,1,0:T(8,128)(2,1)} %collective-permute-done.5.refs_3_, ...), custom_call_target="tpu_custom_call" | custom-call | tf_op jit(solution)/shard_map/pallas_call | solution.py:245
  164.1 3.2 %collective-permute-start.11 = (bf16[512,128]{1,0:T(8,128)(2,1)S(1)}, bf16[512,128]{1,0:T(8,128)(2,1)S(1)}, u32[]{:S(2)}, u32[]{:S(2)}) collective-permute-start(bf16[512,128]{1,0:T(8,128)(2,1)S(1)} %shard_map.105.refs_0_), channel_id=1, source_target_pairs={{0,6},{2,0},{4,2},{6,4},{1,7},{3,1},{5,3},{7,5},{8,14},{10,8},{12,... | collective-permute-start | bytes 393224 | tf_op jit(solution)/shard_map/ppermute | solution.py:25
  168.0 2.7 %collective-permute-done.11.refs_2_ = bf16[512,128]{1,0:T(8,128)(2,1)S(1)} collective-permute-done((bf16[512,128]{1,0:T(8,128)(2,1)S(1)}, bf16[512,128]{1,0:T(8,128)(2,1)S(1)}, u32[]{:S(2)}, u32[]{:S(2)}) %collective-permute-start.11) | collective-permute-done | bytes 131104 | tf_op jit(solution)/shard_map/ppermute | solution.py:25
  170.8 2.9 %collective-permute-done.10.refs_1_ = bf16[512,128]{1,0:T(8,128)(2,1)S(1)} collective-permute-done((bf16[512,128]{1,0:T(8,128)(2,1)S(1)}, bf16[512,128]{1,0:T(8,128)(2,1)S(1)}, u32[]{:S(2)}, u32[]{:S(2)}) %collective-permute-start.10) | collective-permute-done | bytes 131104 | tf_op jit(solution)/shard_map/ppermute | solution.py:25
  173.7 1.9 collective-permute-start.12
  176.4 2.3 collective-permute-done.12.refs_3_
  182.9 11.7 %all-to-all-start.2 = ((bf16[16,2,32,256]{3,2,1,0:T(8,128)(2,1)}), bf16[16,2,32,256]{3,2,1,0:T(8,128)(2,1)}, u32[]{:S(2)}, u32[]{:S(2)}) async-start(bf16[16,2,32,256]{3,2,1,0:T(8,128)(2,1)} %copy-done.3), calls=%async_computation.2 | async-start | bytes 1048576 | tf_op jit(solution)/shard_map/all_to_all | solution.py:377
  199.9 1.9 bitcast_dynamic-update-slice_fusion.3
  203.0 1.9 bitcast_dynamic-update-slice_fusion.2
  205.9 17.7 %all-to-all-done.2 = bf16[16,2,32,256]{3,2,1,0:T(8,128)(2,1)} async-done(((bf16[16,2,32,256]{3,2,1,0:T(8,128)(2,1)}), bf16[16,2,32,256]{3,2,1,0:T(8,128)(2,1)}, u32[]{:S(2)}, u32[]{:S(2)}) %all-to-all-start.2) | async-done | bytes 524320 | tf_op jit(solution)/shard_map/all_to_all | solution.py:377
  224.8 2.1 shard_map.110
  (80 shorter events, 30.0 us)
Async XLA Ops:
  4.8 88.6 %all-to-all-start = ((bf16[16,328,128]{2,1,0:T(8,128)(2,1)}), bf16[16,328,128]{2,1,0:T(8,128)(2,1)S(1)}, u32[]{:S(2)}, u32[]{:S(2)}) async-start(bf16[16,328,128]{2,1,0:T(8,128)(2,1)} %shard_map.102), calls=%async_computation | async-start | bytes 2686976 | tf_op jit(solution)/shard_map/all_to_all | solution.py:377
  93.3 63.5 %all-to-all-start.1 = ((bf16[16,64,256]{2,1,0:T(8,128)(2,1)}), bf16[16,64,256]{2,1,0:T(8,128)(2,1)}, u32[]{:S(2)}, u32[]{:S(2)}) async-start(bf16[16,64,256]{2,1,0:T(8,128)(2,1)} %dynamic-slice_convert_fusion), calls=%async_computation.1 | async-start | bytes 1048576 | tf_op jit(solution)/shard_map/all_to_all | solution.py:377
  100.5 29.2 %collective-permute-start.2 = (bf16[16,64,128]{2,1,0:T(8,128)(2,1)S(1)}, bf16[16,64,128]{2,1,0:T(8,128)(2,1)S(1)}, u32[]{:S(2)}, u32[]{:S(2)}) collective-permute-start(bf16[16,64,128]{2,1,0:T(8,128)(2,1)S(1)} %get-tuple-element.10.refs_0_), channel_id=1, source_target_pairs={{0,8},{8,0},{16,24},{24,16},{32,40},{40,32},{48,56},{56,48},{64,72... | collective-permute-start | bytes 786440 | tf_op jit(solution)/shard_map/ppermute | solution.py:391
  130.2 7.5 %collective-permute-start.17 = (bf16[16,64,128]{2,1,0:T(8,128)(2,1)S(1)}, bf16[16,64,128]{2,1,0:T(8,128)(2,1)S(1)}, u32[]{:S(2)}, u32[]{:S(2)}) collective-permute-start(bf16[16,64,128]{2,1,0:T(8,128)(2,1)S(1)} %get-tuple-element.13.refs_0_), channel_id=1, source_target_pairs={{0,2},{2,4},{4,6},{6,0},{1,3},{3,5},{5,7},{7,1},{8,10},{10,12},{12... | collective-permute-start | bytes 786440 | tf_op jit(solution)/shard_map/ppermute | solution.py:25
  131.9 8.6 %collective-permute-start.18 = (bf16[16,64,128]{2,1,0:T(8,128)(2,1)S(1)}, bf16[16,64,128]{2,1,0:T(8,128)(2,1)S(1)}, u32[]{:S(2)}, u32[]{:S(2)}) collective-permute-start(bf16[16,64,128]{2,1,0:T(8,128)(2,1)S(1)} %get-tuple-element.13.refs_0_), channel_id=1, source_target_pairs={{0,6},{2,0},{4,2},{6,4},{1,7},{3,1},{5,3},{7,5},{8,14},{10,8},{12,... | collective-permute-start | bytes 786440 | tf_op jit(solution)/shard_map/ppermute | solution.py:25
  132.3 29.4 %collective-permute-start = (bf16[16,256,128]{2,1,0:T(8,128)(2,1)}, bf16[16,256,128]{2,1,0:T(8,128)(2,1)S(1)}, u32[]{:S(2)}, u32[]{:S(2)}) collective-permute-start(bf16[16,256,128]{2,1,0:T(8,128)(2,1)} %get-tuple-element.9.refs_8_), channel_id=1, source_target_pairs={{0,128},{128,0},{1,129},{129,1},{2,130},{130,2},{3,131},{131,3},{4... | collective-permute-start | bytes 3145736 | tf_op jit(solution)/shard_map/ppermute | solution.py:25
  134.4 7.1 %collective-permute-start.20 = (bf16[16,64,128]{2,1,0:T(8,128)(2,1)S(1)}, bf16[16,64,128]{2,1,0:T(8,128)(2,1)S(1)}, u32[]{:S(2)}, u32[]{:S(2)}) collective-permute-start(bf16[16,64,128]{2,1,0:T(8,128)(2,1)S(1)} %get-tuple-element.13.refs_0_), channel_id=1, source_target_pairs={{0,1},{1,0},{2,3},{3,2},{4,5},{5,4},{6,7},{7,6},{8,9},{9,8},{10,11... | collective-permute-start | bytes 786440 | tf_op jit(solution)/shard_map/ppermute | solution.py:25
  134.4 10.3 %collective-permute-start.4 = (bf16[16,64,128]{2,1,0:T(8,128)(2,1)S(1)}, bf16[16,64,128]{2,1,0:T(8,128)(2,1)}, u32[]{:S(2)}, u32[]{:S(2)}) collective-permute-start(bf16[16,64,128]{2,1,0:T(8,128)(2,1)S(1)} %get-tuple-element.12.refs_0_), channel_id=1, source_target_pairs={{0,6},{2,0},{4,2},{6,4},{1,7},{3,1},{5,3},{7,5},{8,14},{10,8},{12,... | collective-permute-start | bytes 786440 | tf_op jit(solution)/shard_map/ppermute | solution.py:25
  137.7 9.3 %collective-permute-start.3 = (bf16[16,64,128]{2,1,0:T(8,128)(2,1)S(1)}, bf16[16,64,128]{2,1,0:T(8,128)(2,1)}, u32[]{:S(2)}, u32[]{:S(2)}) collective-permute-start(bf16[16,64,128]{2,1,0:T(8,128)(2,1)S(1)} %get-tuple-element.12.refs_0_), channel_id=1, source_target_pairs={{0,2},{2,4},{4,6},{6,0},{1,3},{3,5},{5,7},{7,1},{8,10},{10,12},{12... | collective-permute-start | bytes 786440 | tf_op jit(solution)/shard_map/ppermute | solution.py:25
  140.5 9.8 %collective-permute-start.19 = (bf16[16,64,128]{2,1,0:T(8,128)(2,1)S(1)}, bf16[16,64,128]{2,1,0:T(8,128)(2,1)S(1)}, u32[]{:S(2)}, u32[]{:S(2)}) collective-permute-start(bf16[16,64,128]{2,1,0:T(8,128)(2,1)S(1)} %collective-permute-done.17.refs_1_), channel_id=1, source_target_pairs={{0,2},{2,4},{4,6},{6,0},{1,3},{3,5},{5,7},{7,1},{8,10},{10,12},{12... | collective-permute-start | bytes 786440 | tf_op jit(solution)/shard_map/ppermute | solution.py:25
  141.5 8.8 %collective-permute-start.21 = (bf16[16,64,128]{2,1,0:T(8,128)(2,1)S(1)}, bf16[16,64,128]{2,1,0:T(8,128)(2,1)S(1)}, u32[]{:S(2)}, u32[]{:S(2)}) collective-permute-start(bf16[16,64,128]{2,1,0:T(8,128)(2,1)S(1)} %collective-permute-done.17.refs_1_), channel_id=1, source_target_pairs={{0,1},{1,0},{2,3},{3,2},{4,5},{5,4},{6,7},{7,6},{8,9},{9,8},{10,11... | collective-permute-start | bytes 786440 | tf_op jit(solution)/shard_map/ppermute | solution.py:25
  147.0 7.3 %collective-permute-start.5 = (bf16[16,64,128]{2,1,0:T(8,128)(2,1)}, bf16[16,64,128]{2,1,0:T(8,128)(2,1)}, u32[]{:S(2)}, u32[]{:S(2)}) collective-permute-start(bf16[16,64,128]{2,1,0:T(8,128)(2,1)} %collective-permute-done.4.refs_2_), channel_id=1, source_target_pairs={{0,6},{2,0},{4,2},{6,4},{1,7},{3,1},{5,3},{7,5},{8,14},{10,8},{12,... | collective-permute-start | bytes 786440 | tf_op jit(solution)/shard_map/ppermute | solution.py:25
  150.3 6.5 %collective-permute-start.6 = (bf16[16,64,128]{2,1,0:T(8,128)(2,1)S(1)}, bf16[16,64,128]{2,1,0:T(8,128)(2,1)}, u32[]{:S(2)}, u32[]{:S(2)}) collective-permute-start(bf16[16,64,128]{2,1,0:T(8,128)(2,1)S(1)} %get-tuple-element.12.refs_0_), channel_id=1, source_target_pairs={{0,1},{1,0},{2,3},{3,2},{4,5},{5,4},{6,7},{7,6},{8,9},{9,8},{10,11... | collective-permute-start | bytes 786440 | tf_op jit(solution)/shard_map/ppermute | solution.py:25
  150.8 8.3 %collective-permute-start.8 = (bf16[16,64,128]{2,1,0:T(8,128)(2,1)}, bf16[16,64,128]{2,1,0:T(8,128)(2,1)}, u32[]{:S(2)}, u32[]{:S(2)}) collective-permute-start(bf16[16,64,128]{2,1,0:T(8,128)(2,1)} %collective-permute-done.4.refs_2_), channel_id=1, source_target_pairs={{0,1},{1,0},{2,3},{3,2},{4,5},{5,4},{6,7},{7,6},{8,9},{9,8},{10,11... | collective-permute-start | bytes 786440 | tf_op jit(solution)/shard_map/ppermute | solution.py:25
  154.2 7.5 %collective-permute-start.9 = (bf16[16,64,128]{2,1,0:T(8,128)(2,1)}, bf16[16,64,128]{2,1,0:T(8,128)(2,1)}, u32[]{:S(2)}, u32[]{:S(2)}) collective-permute-start(bf16[16,64,128]{2,1,0:T(8,128)(2,1)} %collective-permute-done.5.refs_3_), channel_id=1, source_target_pairs={{0,1},{1,0},{2,3},{3,2},{4,5},{5,4},{6,7},{7,6},{8,9},{9,8},{10,11... | collective-permute-start | bytes 786440 | tf_op jit(solution)/shard_map/ppermute | solution.py:25
  156.9 23.8 %collective-permute-start.1 = (bf16[16,64,256]{2,1,0:T(8,128)(2,1)}, bf16[16,64,256]{2,1,0:T(8,128)(2,1)S(1)}, u32[]{:S(2)}, u32[]{:S(2)}) collective-permute-start(bf16[16,64,256]{2,1,0:T(8,128)(2,1)} %all-to-all-done.1), channel_id=1, source_target_pairs={{0,128},{128,0},{1,129},{129,1},{2,130},{130,2},{3,131},{131,3},{4... | collective-permute-start | bytes 1572872 | tf_op jit(solution)/shard_map/ppermute | solution.py:25
  159.1 8.2 %collective-permute-start.24 = (bf16[512,128]{1,0:T(8,128)(2,1)S(1)}, bf16[512,128]{1,0:T(8,128)(2,1)S(1)}, u32[]{:S(2)}, u32[]{:S(2)}) collective-permute-start(bf16[512,128]{1,0:T(8,128)(2,1)S(1)} %shard_map.106.refs_0_), channel_id=1, source_target_pairs={{0,2},{2,4},{4,6},{6,0},{1,3},{3,5},{5,7},{7,1},{8,10},{10,12},{12... | collective-permute-start | bytes 393224 | tf_op jit(solution)/shard_map/ppermute | solution.py:25
  160.2 7.2 %collective-permute-start.25 = (bf16[512,128]{1,0:T(8,128)(2,1)S(1)}, bf16[512,128]{1,0:T(8,128)(2,1)S(1)}, u32[]{:S(2)}, u32[]{:S(2)}) collective-permute-start(bf16[512,128]{1,0:T(8,128)(2,1)S(1)} %shard_map.106.refs_0_), channel_id=1, source_target_pairs={{0,6},{2,0},{4,2},{6,4},{1,7},{3,1},{5,3},{7,5},{8,14},{10,8},{12,... | collective-permute-start | bytes 393224 | tf_op jit(solution)/shard_map/ppermute | solution.py:25
  161.7 6.3 %collective-permute-start.27 = (bf16[512,128]{1,0:T(8,128)(2,1)S(1)}, bf16[512,128]{1,0:T(8,128)(2,1)S(1)}, u32[]{:S(2)}, u32[]{:S(2)}) collective-permute-start(bf16[512,128]{1,0:T(8,128)(2,1)S(1)} %shard_map.106.refs_0_), channel_id=1, source_target_pairs={{0,1},{1,0},{2,3},{3,2},{4,5},{5,4},{6,7},{7,6},{8,9},{9,8},{10,11... | collective-permute-start | bytes 393224 | tf_op jit(solution)/shard_map/ppermute | solution.py:25
  164.1 6.7 %collective-permute-start.11 = (bf16[512,128]{1,0:T(8,128)(2,1)S(1)}, bf16[512,128]{1,0:T(8,128)(2,1)S(1)}, u32[]{:S(2)}, u32[]{:S(2)}) collective-permute-start(bf16[512,128]{1,0:T(8,128)(2,1)S(1)} %shard_map.105.refs_0_), channel_id=1, source_target_pairs={{0,6},{2,0},{4,2},{6,4},{1,7},{3,1},{5,3},{7,5},{8,14},{10,8},{12,... | collective-permute-start | bytes 393224 | tf_op jit(solution)/shard_map/ppermute | solution.py:25
  167.3 6.4 %collective-permute-start.10 = (bf16[512,128]{1,0:T(8,128)(2,1)S(1)}, bf16[512,128]{1,0:T(8,128)(2,1)S(1)}, u32[]{:S(2)}, u32[]{:S(2)}) collective-permute-start(bf16[512,128]{1,0:T(8,128)(2,1)S(1)} %shard_map.105.refs_0_), channel_id=1, source_target_pairs={{0,2},{2,4},{4,6},{6,0},{1,3},{3,5},{5,7},{7,1},{8,10},{10,12},{12... | collective-permute-start | bytes 393224 | tf_op jit(solution)/shard_map/ppermute | solution.py:25
  167.3 8.4 %collective-permute-start.26 = (bf16[512,128]{1,0:T(8,128)(2,1)S(1)}, bf16[512,128]{1,0:T(8,128)(2,1)S(1)}, u32[]{:S(2)}, u32[]{:S(2)}) collective-permute-start(bf16[512,128]{1,0:T(8,128)(2,1)S(1)} %collective-permute-done.24.refs_1_), channel_id=1, source_target_pairs={{0,2},{2,4},{4,6},{6,0},{1,3},{3,5},{5,7},{7,1},{8,10},{10,12},{12... | collective-permute-start | bytes 393224 | tf_op jit(solution)/shard_map/ppermute | solution.py:25
  168.0 7.8 %collective-permute-start.28 = (bf16[512,128]{1,0:T(8,128)(2,1)S(1)}, bf16[512,128]{1,0:T(8,128)(2,1)S(1)}, u32[]{:S(2)}, u32[]{:S(2)}) collective-permute-start(bf16[512,128]{1,0:T(8,128)(2,1)S(1)} %collective-permute-done.24.refs_1_), channel_id=1, source_target_pairs={{0,1},{1,0},{2,3},{3,2},{4,5},{5,4},{6,7},{7,6},{8,9},{9,8},{10,11... | collective-permute-start | bytes 393224 | tf_op jit(solution)/shard_map/ppermute | solution.py:25
  182.9 40.7 %all-to-all-start.2 = ((bf16[16,2,32,256]{3,2,1,0:T(8,128)(2,1)}), bf16[16,2,32,256]{3,2,1,0:T(8,128)(2,1)}, u32[]{:S(2)}, u32[]{:S(2)}) async-start(bf16[16,2,32,256]{3,2,1,0:T(8,128)(2,1)} %copy-done.3), calls=%async_computation.2 | async-start | bytes 1048576 | tf_op jit(solution)/shard_map/all_to_all | solution.py:377
  (19 other events, 105.0 us)

commit v7 on v4

--- a/solution.py
+++ b/solution.py
@@ -229,43 +229,71 @@
 
     def body(*refs):
         ins, (down_ref, *dones) = (refs[:count], refs[count : count + 1 + len(done)])
-        out_ref, in_buf, down_buf = refs[count + 1 + len(done) :]
+        out_ref, in_buf, down_buf, *rest = refs[count + 1 + len(done) :]
         for i, tp in enumerate(places_of()):
             to = slice(i * width, (i + 1) * width)
             down_buf[to, :] = down_ref[pl.ds(pl.multiple_of(tp * width, width), width), :]
             in_buf[:, to] = ins[i][...]
         out = dot(in_buf[...], down_buf[...]).reshape(n, capacity, cols).astype(BF)
-        if last:
-            out_ref[:, expert_at(k, per_device)] = out
-            for i, ref in enumerate(dones):
-                out_ref[:, expert_at(i, per_device)] = ref[...]
-        else:
+        if not last:
             out_ref[...] = out
-
-    return pl.pallas_call(
-        body,
-        out_shape=shape((n, per_device, capacity, cols)) if last else held((n, capacity, cols)),
+            return
+        row_ref, sems = rest
+        copies = [
+            pltpu.make_async_copy(ref, out_ref.at[:, expert_at(i, per_device)], sems.at[i])
+            for i, ref in enumerate((*dones, row_ref))
+        ]
+        for c in copies[:-1]:
+            c.start()
+        row_ref[...] = out
+        copies[-1].start()
+        for c in copies:
+            c.wait()
+
+    return pl.pallas_call(
+        body,
+        out_shape=pltpu.HBM((n, per_device, capacity, cols), BF) if last else held((n, capacity, cols)),
         in_specs=[VM] * (count + 1 + len(done)),
+        out_specs=pl.BlockSpec(memory_space=pltpu.HBM) if last else VM,
+        compiler_params=LIMIT,
+        scratch_shapes=[pltpu.VMEM((rows, depth), BF), pltpu.VMEM((depth, cols), BF)]
+        + [pltpu.VMEM((n, capacity, cols), BF), pltpu.SemaphoreType.DMA((per_device,))] * last,
+    )(*near_core([*blocks, down, *done]))
+
+
+def weigh(route_ids, route_weights, slots, capacity):
+    rows = route_ids.shape[0]
+
+    def body(ids_ref, w_ref, out_ref):
+        lane = iota((rows, slots), 1)
+        total = jnp.zeros((rows, slots), F32)
+        for r, slot in enumerate(slot_of(ids_ref, capacity)):
+            total = jnp.where(lane == slot, as_column(w_ref[r : r + 1, :]), total)
+        high = total.astype(BF)
+        out_ref[0] = high
+        out_ref[1] = (total - high.astype(F32)).astype(BF)
+
+    return pl.pallas_call(
+        body,
+        out_shape=held((2, rows, slots)),
+        in_specs=[VM] * 2,
         out_specs=VM,
         compiler_params=LIMIT,
-        scratch_shapes=[pltpu.VMEM((rows, depth), BF), pltpu.VMEM((depth, cols), BF)],
-    )(*near_core([*blocks, down, *done]))
-
-
-def combine(returned, route_ids, route_weights, capacity):
-    rows, cols = (route_ids.shape[0], returned.shape[1])
-    slots = returned.shape[0]
-
-    def body(ret_ref, ids_ref, w_ref, out_ref):
-        total = jnp.zeros((rows, cols), F32)
-        for r, slot in enumerate(slot_of(ids_ref, capacity)):
-            pick = (iota((rows, slots), 1) == slot).astype(BF)
-            total = total + dot(pick, ret_ref[...]) * as_column(w_ref[r : r + 1, :])
-        out_ref[...] = total.astype(BF)
-
-    return pl.pallas_call(
-        body, out_shape=shape((rows, cols)), in_specs=[VM] * 3, out_specs=VM, compiler_params=LIMIT
-    )(*near_core([returned, route_ids.T, route_weights.T]))
+    )(route_ids.T, route_weights.T)
+
+
+def combine(returned, picks):
+    def body(ret_ref, pick_ref, out_ref):
+        rows = ret_ref[...].reshape(-1, ret_ref.shape[-1])
+        out_ref[...] = (dot(pick_ref[0], rows) + dot(pick_ref[1], rows)).astype(BF)
+
+    return pl.pallas_call(
+        body,
+        out_shape=shape((picks.shape[1], returned.shape[-1])),
+        in_specs=[VM] * 2,
+        out_specs=VM,
+        compiler_params=LIMIT,
+    )(*near_core([returned, picks]))
 
 
 def by_target(master, n):
@@ -356,8 +384,9 @@
         hidden = gather_tp(hidden, k % 2)
         last = k == per_device - 1
         outs.append(second_matmul(hidden, downs[k], n, k, per_device, outs if last else []))
+    picks = weigh(route_ids, route_weights, experts * capacity, capacity)
     out = swap(outs[-1])
-    mixed = combine(out.reshape(-1, out.shape[-1]), route_ids, route_weights, capacity)
+    mixed = combine(out, picks)
     return (gate_serve, up_serve, down_serve, mixed)
 
 

time: 239 us -> 239 us (level)
    unnamed x22 -> x24, local copies, waits for them, and re-layouts: 4.98 us -> 5.18 us
where the time goes in v7:
time: 239 us; the launch traced here: 236 us
  waiting for transfers between devices  121 us (51%)
  starting transfers between devices  84 us (35%)
  local copies, waits for them, and re-layouts  15.3 us (6%)
  Pallas kernels  12.9 us (5%)
    all_to_all x4, waiting for transfers between devices, swap(): return lax.all_to_all(x, 'fs', split_axis=0, concat_axis=0, tiled=True)  79.6 us
    all_to_all x4, starting transfers between devices, swap(): return lax.all_to_all(x, 'fs', split_axis=0, concat_axis=0, tiled=True)  50.9 us
    ppermute x31, starting transfers between devices, shift(): return lax.ppermute(x, axis, [(i, (i + k) % n) for i in range(n)])  27.5 us
    ppermute x3, waiting for transfers between devices, neighbour(): return lax.ppermute(x, 'fs', pairs)  25.7 us
    ppermute x31, waiting for transfers between devices, shift(): return lax.ppermute(x, axis, [(i, (i + k) % n) for i in range(n)])  15.4 us
    ppermute x3, starting transfers between devices, neighbour(): return lax.ppermute(x, 'fs', pairs)  5.54 us
    unnamed x24, local copies, waits for them, and re-layouts  5.18 us
  transfers between devices with their start and end apart: 38, of which 16 were waited for; matrix products, arithmetic and copies ran while one was open for 4% of the time, Pallas kernels for 4%

profile of v7, /device:TPU:34, one launch (start us, length us, event | category | flops | bytes accessed | tf_op | source)
XLA Modules:
  0.0 236.2 jit_solution(11039984497421495256)
XLA Ops:
  0.7 2.4 %multiply_convert_fusion = bf16[16,128,128]{2,1,0:T(8,128)(2,1)} fusion(f32[16,256,128]{2,1,0:T(8,128)} %bitcast.38, s32[]{:T(128)S(6)} %select_n.39, f32[128]{0:T(128)} %param.10), kind=kLoop, calls=%fused_computation.1 | loop fusion | flops 524288 | bytes 1573380 | tf_op jit(solution)/shard_map/convert_element_type | solution.py:368
  3.0 24.0 %all-to-all-start.1 = ((bf16[16,128,128]{2,1,0:T(8,128)(2,1)}), bf16[16,128,128]{2,1,0:T(8,128)(2,1)S(1)}, u32[]{:S(2)}, u32[]{:S(2)}) async-start(bf16[16,128,128]{2,1,0:T(8,128)(2,1)} %multiply_convert_fusion), calls=%async_computation.1 | async-start | bytes 1048576 | tf_op jit(solution)/shard_map/all_to_all | solution.py:352
  27.0 3.4 %shard_map.102 = bf16[16,168,128]{2,1,0:T(8,128)(2,1)} custom-call(bf16[256,2048]{1,0:T(8,128)(2,1)} %tok_ref.1, s32[2,256]{1,0:T(2,128)} %bitcast.32, f32[1,128]{1,0:T(1,128)} %bitcast.39, f32[16,256,128]{2,1,0:T(8,128)} %bitcast.35), custom_call_target="tpu_custom_call" | custom-call | tf_op jit(solution)/shard_map/pallas_call | solution.py:116
  30.4 25.5 %all-to-all-done.1 = bf16[16,128,128]{2,1,0:T(8,128)(2,1)S(1)} async-done(((bf16[16,128,128]{2,1,0:T(8,128)(2,1)}), bf16[16,128,128]{2,1,0:T(8,128)(2,1)S(1)}, u32[]{:S(2)}, u32[]{:S(2)}) %all-to-all-start.1) | async-done | bytes 524320 | tf_op jit(solution)/shard_map/all_to_all | solution.py:352
  55.9 6.6 %all-to-all-start = ((bf16[16,168,128]{2,1,0:T(8,128)(2,1)}), bf16[16,168,128]{2,1,0:T(8,128)(2,1)}, u32[]{:S(2)}, u32[]{:S(2)}) async-start(bf16[16,168,128]{2,1,0:T(8,128)(2,1)} %shard_map.102), calls=%async_computation | async-start | bytes 1376256 | tf_op jit(solution)/shard_map/all_to_all | solution.py:352
  63.4 34.0 %all-to-all-done = bf16[16,168,128]{2,1,0:T(8,128)(2,1)} async-done(((bf16[16,168,128]{2,1,0:T(8,128)(2,1)}), bf16[16,168,128]{2,1,0:T(8,128)(2,1)}, u32[]{:S(2)}, u32[]{:S(2)}) %all-to-all-start) | async-done | bytes 688160 | tf_op jit(solution)/shard_map/all_to_all | solution.py:352
  97.4 7.7 %all-to-all-start.2 = ((bf16[16,64,256]{2,1,0:T(8,128)(2,1)}), bf16[16,64,256]{2,1,0:T(8,128)(2,1)S(1)}, u32[]{:S(2)}, u32[]{:S(2)}) async-start(bf16[16,64,256]{2,1,0:T(8,128)(2,1)} %dynamic-slice_convert_fusion), calls=%async_computation.2 | async-start | bytes 1048576 | tf_op jit(solution)/shard_map/all_to_all | solution.py:352
  105.1 2.2 collective-permute-start.1
  110.0 2.4 %collective-permute-start.4 = (bf16[16,32,128]{2,1,0:T(8,128)(2,1)S(1)}, bf16[16,32,128]{2,1,0:T(8,128)(2,1)S(1)}, u32[]{:S(2)}, u32[]{:S(2)}) collective-permute-start(bf16[16,32,128]{2,1,0:T(8,128)(2,1)S(1)} %split.13.refs_0_), channel_id=1, source_target_pairs={{0,16},{8,24},{16,0},{24,8},{32,48},{40,56},{48,32},{56,40},{64,80... | collective-permute-start | bytes 393224 | tf_op jit(solution)/shard_map/ppermute | solution.py:356
  114.6 20.9 %collective-permute-done.3.refs_1_ = bf16[16,32,128]{2,1,0:T(8,128)(2,1)S(1)} collective-permute-done((bf16[16,32,128]{2,1,0:T(8,128)(2,1)S(1)}, bf16[16,32,128]{2,1,0:T(8,128)(2,1)S(1)}, u32[]{:S(2)}, u32[]{:S(2)}) %collective-permute-start.3) | collective-permute-done | bytes 131104 | tf_op jit(solution)/shard_map/ppermute | solution.py:356
  135.4 4.8 %collective-permute-done.4.refs_2_ = bf16[16,32,128]{2,1,0:T(8,128)(2,1)S(1)} collective-permute-done((bf16[16,32,128]{2,1,0:T(8,128)(2,1)S(1)}, bf16[16,32,128]{2,1,0:T(8,128)(2,1)S(1)}, u32[]{:S(2)}, u32[]{:S(2)}) %collective-permute-start.4) | collective-permute-done | bytes 131104 | tf_op jit(solution)/shard_map/ppermute | solution.py:356
  151.5 2.1 collective-permute-start
  154.6 3.1 %collective-permute-start.8 = (bf16[16,64,128]{2,1,0:T(8,128)(2,1)}, bf16[16,64,128]{2,1,0:T(8,128)(2,1)}, u32[]{:S(2)}, u32[]{:S(2)}) collective-permute-start(bf16[16,64,128]{2,1,0:T(8,128)(2,1)} %collective-permute-done.7.refs_2_), channel_id=1, source_target_pairs={{0,6},{2,0},{4,2},{6,4},{1,7},{3,1},{5,3},{7,5},{8,14},{10,8},{12,... | collective-permute-start | bytes 786440 | tf_op jit(solution)/shard_map/ppermute | solution.py:24
  160.1 3.4 %collective-permute-done.8.refs_3_ = bf16[16,64,128]{2,1,0:T(8,128)(2,1)} collective-permute-done((bf16[16,64,128]{2,1,0:T(8,128)(2,1)}, bf16[16,64,128]{2,1,0:T(8,128)(2,1)}, u32[]{:S(2)}, u32[]{:S(2)}) %collective-permute-start.8) | collective-permute-done | bytes 262176 | tf_op jit(solution)/shard_map/ppermute | solution.py:24
  164.0 2.0 shard_map.105.refs_0_
  166.0 2.2 collective-permute-start.2
  171.3 2.5 %shard_map.104.refs_0_ = bf16[512,128]{1,0:T(8,128)(2,1)S(1)} custom-call(bf16[16,64,128]{2,1,0:T(8,128)(2,1)S(1)} %get-tuple-element.6.refs_0_, bf16[16,64,128]{2,1,0:T(8,128)(2,1)} %collective-permute-done.6.refs_1_, bf16[16,64,128]{2,1,0:T(8,128)(2,1)} %collective-permute-done.7.refs_2_, bf16[16,64,128]{2,1,0:T(8,128)(2,1)} %collective-permute-done.8.refs_3_, ...), custom_call_target="tpu_custom_call" | custom-call | tf_op jit(solution)/shard_map/pallas_call | solution.py:213
  173.9 2.8 %collective-permute-start.14 = (bf16[512,128]{1,0:T(8,128)(2,1)S(1)}, bf16[512,128]{1,0:T(8,128)(2,1)S(1)}, u32[]{:S(2)}, u32[]{:S(2)}) collective-permute-start(bf16[512,128]{1,0:T(8,128)(2,1)S(1)} %shard_map.104.refs_0_), channel_id=1, source_target_pairs={{0,6},{2,0},{4,2},{6,4},{1,7},{3,1},{5,3},{7,5},{8,14},{10,8},{12,... | collective-permute-start | bytes 393224 | tf_op jit(solution)/shard_map/ppermute | solution.py:24
  178.1 2.1 collective-permute-done.14.refs_2_
  180.2 2.8 %collective-permute-done.13.refs_1_ = bf16[512,128]{1,0:T(8,128)(2,1)S(1)} collective-permute-done((bf16[512,128]{1,0:T(8,128)(2,1)S(1)}, bf16[512,128]{1,0:T(8,128)(2,1)S(1)}, u32[]{:S(2)}, u32[]{:S(2)}) %collective-permute-start.13) | collective-permute-done | bytes 131104 | tf_op jit(solution)/shard_map/ppermute | solution.py:24
  183.0 3.1 %collective-permute-start.15 = (bf16[512,128]{1,0:T(8,128)(2,1)S(1)}, bf16[512,128]{1,0:T(8,128)(2,1)S(1)}, u32[]{:S(2)}, u32[]{:S(2)}) collective-permute-start(bf16[512,128]{1,0:T(8,128)(2,1)S(1)} %collective-permute-done.14.refs_2_), channel_id=1, source_target_pairs={{0,6},{2,0},{4,2},{6,4},{1,7},{3,1},{5,3},{7,5},{8,14},{10,8},{12,... | collective-permute-start | bytes 393224 | tf_op jit(solution)/shard_map/ppermute | solution.py:24
  192.2 12.6 %all-to-all-start.3 = ((bf16[16,2,32,256]{3,2,1,0:T(8,128)(2,1)}), bf16[16,2,32,256]{3,2,1,0:T(8,128)(2,1)}, u32[]{:S(2)}, u32[]{:S(2)}) async-start(bf16[16,2,32,256]{3,2,1,0:T(8,128)(2,1)} %shard_map.107), calls=%async_computation.3 | async-start | bytes 1048576 | tf_op jit(solution)/shard_map/all_to_all | solution.py:352
  213.9 20.1 %all-to-all-done.3.ret_ref = bf16[16,2,32,256]{3,2,1,0:T(8,128)(2,1)} async-done(((bf16[16,2,32,256]{3,2,1,0:T(8,128)(2,1)}), bf16[16,2,32,256]{3,2,1,0:T(8,128)(2,1)}, u32[]{:S(2)}, u32[]{:S(2)}) %all-to-all-start.3) | async-done | bytes 524320 | tf_op jit(solution)/shard_map/all_to_all | solution.py:352
  234.1 2.1 shard_map.109
  (98 shorter events, 40.4 us)
Async XLA Ops:
  3.0 52.9 %all-to-all-start.1 = ((bf16[16,128,128]{2,1,0:T(8,128)(2,1)}), bf16[16,128,128]{2,1,0:T(8,128)(2,1)S(1)}, u32[]{:S(2)}, u32[]{:S(2)}) async-start(bf16[16,128,128]{2,1,0:T(8,128)(2,1)} %multiply_convert_fusion), calls=%async_computation.1 | async-start | bytes 1048576 | tf_op jit(solution)/shard_map/all_to_all | solution.py:352
  55.9 41.5 %all-to-all-start = ((bf16[16,168,128]{2,1,0:T(8,128)(2,1)}), bf16[16,168,128]{2,1,0:T(8,128)(2,1)}, u32[]{:S(2)}, u32[]{:S(2)}) async-start(bf16[16,168,128]{2,1,0:T(8,128)(2,1)} %shard_map.102), calls=%async_computation | async-start | bytes 1376256 | tf_op jit(solution)/shard_map/all_to_all | solution.py:352
  97.4 68.6 %all-to-all-start.2 = ((bf16[16,64,256]{2,1,0:T(8,128)(2,1)}), bf16[16,64,256]{2,1,0:T(8,128)(2,1)S(1)}, u32[]{:S(2)}, u32[]{:S(2)}) async-start(bf16[16,64,256]{2,1,0:T(8,128)(2,1)} %dynamic-slice_convert_fusion), calls=%async_computation.2 | async-start | bytes 1048576 | tf_op jit(solution)/shard_map/all_to_all | solution.py:352
  105.1 39.4 %collective-permute-start.1 = (bf16[16,128,128]{2,1,0:T(8,128)(2,1)S(1)}, bf16[16,128,128]{2,1,0:T(8,128)(2,1)S(1)}, u32[]{:S(2)}, u32[]{:S(2)}) collective-permute-start(bf16[16,128,128]{2,1,0:T(8,128)(2,1)S(1)} %all-to-all-done.1), channel_id=1, source_target_pairs={{0,128},{128,0},{1,129},{129,1},{2,130},{130,2},{3,131},{131,3},{4... | collective-permute-start | bytes 1572872 | tf_op jit(solution)/shard_map/ppermute | solution.py:24
  108.3 27.2 %collective-permute-start.3 = (bf16[16,32,128]{2,1,0:T(8,128)(2,1)S(1)}, bf16[16,32,128]{2,1,0:T(8,128)(2,1)S(1)}, u32[]{:S(2)}, u32[]{:S(2)}) collective-permute-start(bf16[16,32,128]{2,1,0:T(8,128)(2,1)S(1)} %split.13.refs_0_), channel_id=1, source_target_pairs={{0,8},{8,16},{16,24},{24,0},{32,40},{40,48},{48,56},{56,32},{64,72... | collective-permute-start | bytes 393224 | tf_op jit(solution)/shard_map/ppermute | solution.py:356
  110.0 30.2 %collective-permute-start.4 = (bf16[16,32,128]{2,1,0:T(8,128)(2,1)S(1)}, bf16[16,32,128]{2,1,0:T(8,128)(2,1)S(1)}, u32[]{:S(2)}, u32[]{:S(2)}) collective-permute-start(bf16[16,32,128]{2,1,0:T(8,128)(2,1)S(1)} %split.13.refs_0_), channel_id=1, source_target_pairs={{0,16},{8,24},{16,0},{24,8},{32,48},{40,56},{48,32},{56,40},{64,80... | collective-permute-start | bytes 393224 | tf_op jit(solution)/shard_map/ppermute | solution.py:356
  112.3 27.9 %collective-permute-start.5 = (bf16[16,32,128]{2,1,0:T(8,128)(2,1)S(1)}, bf16[16,32,128]{2,1,0:T(8,128)(2,1)S(1)}, u32[]{:S(2)}, u32[]{:S(2)}) collective-permute-start(bf16[16,32,128]{2,1,0:T(8,128)(2,1)S(1)} %split.13.refs_0_), channel_id=1, source_target_pairs={{0,24},{8,0},{16,8},{24,16},{32,56},{40,32},{48,40},{56,48},{64,88... | collective-permute-start | bytes 393224 | tf_op jit(solution)/shard_map/ppermute | solution.py:356
  142.4 9.1 %collective-permute-start.21 = (bf16[16,64,128]{2,1,0:T(8,128)(2,1)S(1)}, bf16[16,64,128]{2,1,0:T(8,128)(2,1)S(1)}, u32[]{:S(2)}, u32[]{:S(2)}) collective-permute-start(bf16[16,64,128]{2,1,0:T(8,128)(2,1)S(1)} %get-tuple-element.7.refs_0_), channel_id=1, source_target_pairs={{0,6},{2,0},{4,2},{6,4},{1,7},{3,1},{5,3},{7,5},{8,14},{10,8},{12,... | collective-permute-start | bytes 786440 | tf_op jit(solution)/shard_map/ppermute | solution.py:24
  142.8 8.7 %collective-permute-start.23 = (bf16[16,64,128]{2,1,0:T(8,128)(2,1)S(1)}, bf16[16,64,128]{2,1,0:T(8,128)(2,1)S(1)}, u32[]{:S(2)}, u32[]{:S(2)}) collective-permute-start(bf16[16,64,128]{2,1,0:T(8,128)(2,1)S(1)} %get-tuple-element.7.refs_0_), channel_id=1, source_target_pairs={{0,1},{1,0},{2,3},{3,2},{4,5},{5,4},{6,7},{7,6},{8,9},{9,8},{10,11... | collective-permute-start | bytes 786440 | tf_op jit(solution)/shard_map/ppermute | solution.py:24
  142.8 11.6 %collective-permute-start.7 = (bf16[16,64,128]{2,1,0:T(8,128)(2,1)S(1)}, bf16[16,64,128]{2,1,0:T(8,128)(2,1)}, u32[]{:S(2)}, u32[]{:S(2)}) collective-permute-start(bf16[16,64,128]{2,1,0:T(8,128)(2,1)S(1)} %get-tuple-element.6.refs_0_), channel_id=1, source_target_pairs={{0,6},{2,0},{4,2},{6,4},{1,7},{3,1},{5,3},{7,5},{8,14},{10,8},{12,... | collective-permute-start | bytes 786440 | tf_op jit(solution)/shard_map/ppermute | solution.py:24
  145.3 9.3 %collective-permute-start.6 = (bf16[16,64,128]{2,1,0:T(8,128)(2,1)S(1)}, bf16[16,64,128]{2,1,0:T(8,128)(2,1)}, u32[]{:S(2)}, u32[]{:S(2)}) collective-permute-start(bf16[16,64,128]{2,1,0:T(8,128)(2,1)S(1)} %get-tuple-element.6.refs_0_), channel_id=1, source_target_pairs={{0,2},{2,4},{4,6},{6,0},{1,3},{3,5},{5,7},{7,1},{8,10},{10,12},{12... | collective-permute-start | bytes 786440 | tf_op jit(solution)/shard_map/ppermute | solution.py:24
  147.2 12.3 %collective-permute-start.22 = (bf16[16,64,128]{2,1,0:T(8,128)(2,1)S(1)}, bf16[16,64,128]{2,1,0:T(8,128)(2,1)S(1)}, u32[]{:S(2)}, u32[]{:S(2)}) collective-permute-start(bf16[16,64,128]{2,1,0:T(8,128)(2,1)S(1)} %collective-permute-done.20.refs_1_), channel_id=1, source_target_pairs={{0,2},{2,4},{4,6},{6,0},{1,3},{3,5},{5,7},{7,1},{8,10},{10,12},{12... | collective-permute-start | bytes 786440 | tf_op jit(solution)/shard_map/ppermute | solution.py:24
  151.5 8.0 %collective-permute-start.24 = (bf16[16,64,128]{2,1,0:T(8,128)(2,1)S(1)}, bf16[16,64,128]{2,1,0:T(8,128)(2,1)S(1)}, u32[]{:S(2)}, u32[]{:S(2)}) collective-permute-start(bf16[16,64,128]{2,1,0:T(8,128)(2,1)S(1)} %collective-permute-done.20.refs_1_), channel_id=1, source_target_pairs={{0,1},{1,0},{2,3},{3,2},{4,5},{5,4},{6,7},{7,6},{8,9},{9,8},{10,11... | collective-permute-start | bytes 786440 | tf_op jit(solution)/shard_map/ppermute | solution.py:24
  151.5 16.7 %collective-permute-start = (bf16[16,128,128]{2,1,0:T(8,128)(2,1)}, bf16[16,128,128]{2,1,0:T(8,128)(2,1)}, u32[]{:S(2)}, u32[]{:S(2)}) collective-permute-start(bf16[16,128,128]{2,1,0:T(8,128)(2,1)} %split.12), channel_id=1, source_target_pairs={{0,128},{128,0},{1,129},{129,1},{2,130},{130,2},{3,131},{131,3},{4... | collective-permute-start | bytes 1572872 | tf_op jit(solution)/shard_map/ppermute | solution.py:24
  154.6 8.9 %collective-permute-start.8 = (bf16[16,64,128]{2,1,0:T(8,128)(2,1)}, bf16[16,64,128]{2,1,0:T(8,128)(2,1)}, u32[]{:S(2)}, u32[]{:S(2)}) collective-permute-start(bf16[16,64,128]{2,1,0:T(8,128)(2,1)} %collective-permute-done.7.refs_2_), channel_id=1, source_target_pairs={{0,6},{2,0},{4,2},{6,4},{1,7},{3,1},{5,3},{7,5},{8,14},{10,8},{12,... | collective-permute-start | bytes 786440 | tf_op jit(solution)/shard_map/ppermute | solution.py:24
  160.0 9.6 %collective-permute-start.11 = (bf16[16,64,128]{2,1,0:T(8,128)(2,1)}, bf16[16,64,128]{2,1,0:T(8,128)(2,1)}, u32[]{:S(2)}, u32[]{:S(2)}) collective-permute-start(bf16[16,64,128]{2,1,0:T(8,128)(2,1)} %collective-permute-done.7.refs_2_), channel_id=1, source_target_pairs={{0,1},{1,0},{2,3},{3,2},{4,5},{5,4},{6,7},{7,6},{8,9},{9,8},{10,11... | collective-permute-start | bytes 786440 | tf_op jit(solution)/shard_map/ppermute | solution.py:24
  163.5 6.8 %collective-permute-start.10 = (bf16[16,64,128]{2,1,0:T(8,128)(2,1)}, bf16[16,64,128]{2,1,0:T(8,128)(2,1)}, u32[]{:S(2)}, u32[]{:S(2)}) collective-permute-start(bf16[16,64,128]{2,1,0:T(8,128)(2,1)} %collective-permute-done.6.refs_1_), channel_id=1, source_target_pairs={{0,1},{1,0},{2,3},{3,2},{4,5},{5,4},{6,7},{7,6},{8,9},{9,8},{10,11... | collective-permute-start | bytes 786440 | tf_op jit(solution)/shard_map/ppermute | solution.py:24
  166.0 23.7 %collective-permute-start.2 = (bf16[16,64,256]{2,1,0:T(8,128)(2,1)S(1)}, bf16[16,64,256]{2,1,0:T(8,128)(2,1)S(1)}, u32[]{:S(2)}, u32[]{:S(2)}) collective-permute-start(bf16[16,64,256]{2,1,0:T(8,128)(2,1)S(1)} %all-to-all-done.2), channel_id=1, source_target_pairs={{0,128},{128,0},{1,129},{129,1},{2,130},{130,2},{3,131},{131,3},{4... | collective-permute-start | bytes 1572872 | tf_op jit(solution)/shard_map/ppermute | solution.py:24
  168.2 8.4 %collective-permute-start.27 = (bf16[512,128]{1,0:T(8,128)(2,1)S(1)}, bf16[512,128]{1,0:T(8,128)(2,1)S(1)}, u32[]{:S(2)}, u32[]{:S(2)}) collective-permute-start(bf16[512,128]{1,0:T(8,128)(2,1)S(1)} %shard_map.105.refs_0_), channel_id=1, source_target_pairs={{0,2},{2,4},{4,6},{6,0},{1,3},{3,5},{5,7},{7,1},{8,10},{10,12},{12... | collective-permute-start | bytes 393224 | tf_op jit(solution)/shard_map/ppermute | solution.py:24
  169.6 7.0 %collective-permute-start.28 = (bf16[512,128]{1,0:T(8,128)(2,1)S(1)}, bf16[512,128]{1,0:T(8,128)(2,1)S(1)}, u32[]{:S(2)}, u32[]{:S(2)}) collective-permute-start(bf16[512,128]{1,0:T(8,128)(2,1)S(1)} %shard_map.105.refs_0_), channel_id=1, source_target_pairs={{0,6},{2,0},{4,2},{6,4},{1,7},{3,1},{5,3},{7,5},{8,14},{10,8},{12,... | collective-permute-start | bytes 393224 | tf_op jit(solution)/shard_map/ppermute | solution.py:24
  170.3 7.8 %collective-permute-start.30 = (bf16[512,128]{1,0:T(8,128)(2,1)S(1)}, bf16[512,128]{1,0:T(8,128)(2,1)S(1)}, u32[]{:S(2)}, u32[]{:S(2)}) collective-permute-start(bf16[512,128]{1,0:T(8,128)(2,1)S(1)} %shard_map.105.refs_0_), channel_id=1, source_target_pairs={{0,1},{1,0},{2,3},{3,2},{4,5},{5,4},{6,7},{7,6},{8,9},{9,8},{10,11... | collective-permute-start | bytes 393224 | tf_op jit(solution)/shard_map/ppermute | solution.py:24
  176.6 9.5 %collective-permute-start.29 = (bf16[512,128]{1,0:T(8,128)(2,1)S(1)}, bf16[512,128]{1,0:T(8,128)(2,1)S(1)}, u32[]{:S(2)}, u32[]{:S(2)}) collective-permute-start(bf16[512,128]{1,0:T(8,128)(2,1)S(1)} %collective-permute-done.27.refs_1_), channel_id=1, source_target_pairs={{0,2},{2,4},{4,6},{6,0},{1,3},{3,5},{5,7},{7,1},{8,10},{10,12},{12... | collective-permute-start | bytes 393224 | tf_op jit(solution)/shard_map/ppermute | solution.py:24
  178.1 8.0 %collective-permute-start.31 = (bf16[512,128]{1,0:T(8,128)(2,1)S(1)}, bf16[512,128]{1,0:T(8,128)(2,1)S(1)}, u32[]{:S(2)}, u32[]{:S(2)}) collective-permute-start(bf16[512,128]{1,0:T(8,128)(2,1)S(1)} %collective-permute-done.27.refs_1_), channel_id=1, source_target_pairs={{0,1},{1,0},{2,3},{3,2},{4,5},{5,4},{6,7},{7,6},{8,9},{9,8},{10,11... | collective-permute-start | bytes 393224 | tf_op jit(solution)/shard_map/ppermute | solution.py:24
  192.2 41.9 %all-to-all-start.3 = ((bf16[16,2,32,256]{3,2,1,0:T(8,128)(2,1)}), bf16[16,2,32,256]{3,2,1,0:T(8,128)(2,1)}, u32[]{:S(2)}, u32[]{:S(2)}) async-start(bf16[16,2,32,256]{3,2,1,0:T(8,128)(2,1)} %shard_map.107), calls=%async_computation.3 | async-start | bytes 1048576 | tf_op jit(solution)/shard_map/all_to_all | solution.py:352
  (26 other events, 193.1 us)
